TPU v7x, 32 devices: a whole 2x2x4 slice. The times are simulated.
32 devices in a mesh: sp: 4 (over y, x), dp: 8 (over z, core).
Axes of the slice: x: 2, y: 2, z: 4, core: 2. Of those that a mesh axis runs over, the one named last changes fastest.
Arguments:
- tokens: bfloat16 [8, 1024, 2048], P('dp', 'sp'), may hold values from -6 to 6
- key_weight: bfloat16 [2048, 2048], P('dp'), may hold values from -0.125 to 0.125
- queries: bfloat16 [8, 1024, 16, 128], P('dp', None, 'sp'), may hold values from -1.5 to 1.5
- values: bfloat16 [8, 1024, 16, 256], P('dp', None, 'sp'), may hold values from -1.5 to 1.5
- cotangent: bfloat16 [8, 1024, 4096], P('dp', 'sp'), may hold values from -6 to 6
- log_decay: float32 [16], replicated, may hold values from -0.034 to 0, as said below
Outputs:
- grad_tokens: bfloat16 [8, 1024, 2048], P('dp', 'sp')
- grad_queries: bfloat16 [8, 1024, 16, 128], P('dp', None, 'sp')
- grad_values: bfloat16 [8, 1024, 16, 256], P('dp', None, 'sp')
- grad_key_weight: float32 [2048, 2048], P('dp')
Inputs may be any that keep to these rules, and one draw needn't show every extreme that they name: `log_decay`: every entry is below zero.
All inputs are finite; a program needn't handle non-finite values.
Results may differ from a plain program's by a relative error of at most 0.0075.
Values may be sent and summed in bfloat16 or wider, within the bound.
No kernel may reach another device: no remote copies, remote signals or barrier semaphores. Data moves between devices by JAX's collectives and lax.ppermute only.
A program may use at most 128 MiB of HBM per device.

v0:
```python
import jax
import jax.numpy as jnp
from jax import lax
from jax.experimental import pallas as pl
from jax.experimental.pallas import tpu as pltpu
from jax.sharding import PartitionSpec as P

BLOCK = 128


def product(form, left, right):
    return jnp.einsum(form, left, right, preferred_element_type=jnp.float32)


def rotation(seq_len, half):
    position = jnp.arange(seq_len, dtype=jnp.float32)
    frequency = 10000.0 ** (-jnp.arange(half, dtype=jnp.float32) / half)
    angle = position[:, None] * frequency[None, :]
    return (jnp.cos(angle)[:, None, :], jnp.sin(angle)[:, None, :])


def rotate(vectors, cosine, sine):
    half = vectors.shape[-1] // 2
    front, back = (vectors[..., :half], vectors[..., half:])
    return jnp.concatenate([front * cosine - back * sine, front * sine + back * cosine], axis=-1)


def unrotate(grads, cosine, sine):
    half = grads.shape[-1] // 2
    front, back = (grads[..., :half], grads[..., half:])
    return jnp.concatenate([front * cosine + back * sine, back * cosine - front * sine], axis=-1)


def retention_backward(query_rows, key_rows, value_rows, cotan_rows, head_decay):
    seq_len, heads_here, key_width = query_rows.shape
    nblocks = seq_len // BLOCK
    cosine, sine = rotation(seq_len, key_width // 2)
    factor = key_width ** (-0.5)
    rot_query = rotate(query_rows.astype(jnp.float32), cosine, sine).astype(jnp.bfloat16)
    rot_key = (rotate(key_rows.astype(jnp.float32), cosine, sine) * factor).astype(jnp.bfloat16)

    def blocks(array):
        return array.reshape(nblocks, BLOCK, heads_here, array.shape[-1])

    block_query, block_key = (blocks(rot_query), blocks(rot_key))
    block_value, block_cotan = (blocks(value_rows), blocks(cotan_rows))
    inside = jnp.arange(BLOCK, dtype=jnp.float32)
    offset = inside[:, None] - inside[None, :]
    within = jnp.where(
        offset[None] >= 0, jnp.exp(jnp.maximum(offset, 0.0)[None] * head_decay[:, None, None]), 0.0
    )
    rising = jnp.exp((inside + 1.0)[:, None] * head_decay[None, :])[None, :, :, None]
    falling = jnp.exp((BLOCK - 1.0 - inside)[:, None] * head_decay[None, :])[None, :, :, None]
    scores = (product("nihd,njhd->nhij", block_query, block_key) * within[None]).astype(
        jnp.bfloat16
    )
    mixing = (product("nihe,njhe->nhij", block_cotan, block_value) * within[None]).astype(
        jnp.bfloat16
    )
    decayed_queries = (block_query.astype(jnp.float32) * rising).astype(jnp.bfloat16)
    decayed_keys = (block_key.astype(jnp.float32) * falling).astype(jnp.bfloat16)
    block_states = product("nihd,nihe->nhde", decayed_keys, block_value)
    block_trails = product("nihd,nihe->nhde", decayed_queries, block_cotan)
    block_index = jnp.arange(nblocks, dtype=jnp.float32)
    spacing = block_index[:, None] - block_index[None, :] - 1.0
    earlier = jnp.where(
        spacing[None] >= 0,
        jnp.exp(jnp.maximum(spacing, 0.0)[None] * BLOCK * head_decay[:, None, None]),
        0.0,
    )
    later = jnp.transpose(earlier, (0, 2, 1))
    entering = jnp.einsum(
        "hnm,mhde->nhde", earlier, block_states, precision=lax.Precision.HIGHEST
    ).astype(jnp.bfloat16)
    trailing = jnp.einsum(
        "hnm,mhde->nhde", later, block_trails, precision=lax.Precision.HIGHEST
    ).astype(jnp.bfloat16)
    grad_rq = product("nhij,njhd->nihd", mixing, block_key) + rising * product(
        "nihe,nhde->nihd", block_cotan, entering
    )
    grad_rk = product("nhij,nihd->njhd", mixing, block_query) + falling * product(
        "nihe,nhde->nihd", block_value, trailing
    )
    grad_value = product("nhij,nihe->njhe", scores, block_cotan) + falling * product(
        "nihd,nhde->nihe", block_key, trailing
    )
    grad_rq = grad_rq.reshape(seq_len, heads_here, key_width)
    grad_rk = grad_rk.reshape(seq_len, heads_here, key_width)
    grad_query = unrotate(grad_rq, cosine, sine).astype(jnp.bfloat16)
    grad_key = (unrotate(grad_rk, cosine, sine) * factor).astype(jnp.bfloat16)
    grad_value = grad_value.reshape(seq_len, heads_here, -1).astype(jnp.bfloat16)
    return (grad_query, grad_key, grad_value)


def general_body(tokens, key_weight, queries, values, cotangent, log_decay):
    gathered = lax.all_gather(key_weight, "dp", axis=0, tiled=True)
    token_rows = tokens[0]
    key_proj = jnp.einsum(
        "td,qd->tq", token_rows, gathered, preferred_element_type=jnp.float32
    ).astype(jnp.bfloat16)
    head_keys, head_cotan = (
        lax.all_to_all(key_proj[None], "sp", split_axis=2, concat_axis=1, tiled=True),
        lax.all_to_all(cotangent, "sp", split_axis=2, concat_axis=1, tiled=True),
    )
    seq_len = head_keys.shape[1]
    heads_here = queries.shape[2]
    head_start = lax.axis_index("sp") * heads_here
    head_decay = lax.dynamic_slice_in_dim(log_decay, head_start, heads_here)
    grad_query, grad_key, grad_value = retention_backward(
        queries[0],
        head_keys[0].reshape(seq_len, heads_here, -1),
        values[0],
        head_cotan[0].reshape(seq_len, heads_here, -1),
        head_decay,
    )
    returned = lax.all_to_all(
        grad_key.reshape(1, seq_len, -1), "sp", split_axis=1, concat_axis=2, tiled=True
    )
    key_grads = returned[0]
    grad_tokens = jnp.dot(key_grads, gathered, preferred_element_type=jnp.float32).astype(
        jnp.bfloat16
    )
    width = key_grads.shape[1]
    count_dp = lax.axis_size("dp")
    count_sp = lax.axis_size("sp")
    share = width // (count_sp * count_dp)
    ordered = (
        key_grads.reshape(-1, count_dp, count_sp, share).transpose(0, 2, 1, 3).reshape(-1, width)
    )
    partial_grad = jnp.einsum("tq,td->qd", ordered, token_rows, preferred_element_type=jnp.float32)
    owned = lax.psum_scatter(partial_grad, ("sp", "dp"), scatter_dimension=0, tiled=True)
    weight_grad = lax.all_gather(owned, "sp", axis=0, tiled=True)
    return (grad_tokens[None], grad_query[None], grad_value[None], weight_grad)


INNER = 256
CHUNKS = 1


def swap(array, axis, bit):
    count = lax.axis_size(axis)
    return lax.ppermute(array, axis, [(i, i ^ bit) for i in range(count)])


def step_planes(array):
    count = lax.axis_size("dp")
    return lax.ppermute(array, "dp", [(i, (i + 2) % count) for i in range(count)])


def limit(mib):
    return pltpu.CompilerParams(vmem_limit_bytes=mib * 2**20)


def dot(left, right, left_dim, right_dim):
    return lax.dot_general(
        left, right, (((left_dim,), (right_dim,)), ((), ())), preferred_element_type=jnp.float32
    )


def columns(array, index, width):
    return lax.dynamic_slice_in_dim(array, index * width, width, axis=1)


def cost(flops, moved):
    return pl.CostEstimate(flops=int(flops), bytes_accessed=int(moved), transcendentals=0)


def spec(shape, index):
    return pl.BlockSpec(shape, index)


def decays(rate, size):
    rows = lax.broadcasted_iota(jnp.int32, (size, size), 0)
    cols = lax.broadcasted_iota(jnp.int32, (size, size), 1)
    gap = (rows - cols).astype(jnp.float32)
    within = jnp.where(gap >= 0, jnp.exp(jnp.maximum(gap, 0.0) * rate), 0.0)
    flipped = jnp.where(gap <= 0, jnp.exp(jnp.maximum(-gap, 0.0) * rate), 0.0)
    place = lax.broadcasted_iota(jnp.int32, (size, 1), 0).astype(jnp.float32)
    rising = jnp.exp((place + 1.0) * rate)
    falling = jnp.exp((size - 1.0 - place) * rate)
    whole = jnp.exp(jnp.full((1, 1), float(size), jnp.float32) * rate)
    return within, flipped, rising, falling, whole


def turn(block, cosine, sine):
    half = block.shape[-1] // 2
    return block * cosine + pltpu.roll(block, half, 1) * sine


def turn_back(block, cosine, sine):
    half = block.shape[-1] // 2
    return block * cosine - pltpu.roll(block, half, 1) * sine


def first_kernel(slots, rows, inner, factor):
    def kernel(*refs):
        place, rate_ref, query, value, cosine, sine = refs[:6]
        cotans = refs[6 : 6 + slots]
        outs = refs[6 + slots :]
        grads, turned_grads = outs[:slots], outs[slots : 2 * slots]
        rotated, trailing, cotan, whole_grad, flat_grad = outs[2 * slots :]
        here = place[0]
        rate = rate_ref[pl.program_id(0)]
        for k in range(slots):
            cotan[pl.ds((here ^ k) * rows, rows), :] = cotans[k][...]
        _, flipped, rising, falling, whole = decays(rate, inner)
        seq_len = query.shape[0]
        carry = jnp.zeros((query.shape[1], value.shape[1]), jnp.float32)
        for n in reversed(range(seq_len // inner)):
            at = slice(n * inner, (n + 1) * inner)
            cos, sin = cosine[at, :], sine[at, :]
            turned = turn(query[at, :].astype(jnp.float32), cos, sin).astype(jnp.bfloat16)
            rotated[at, :] = turned
            co, va = cotan[at, :], value[at, :]
            mix = (dot(va, co, 1, 1) * flipped).astype(jnp.bfloat16)
            trail = carry.astype(jnp.bfloat16)
            trailing[0, n] = trail
            grad = dot(mix, turned, 1, 0) + falling * dot(va, trail, 1, 1)
            grad = turn_back(grad, cos, sin) * factor
            whole_grad[at, :] = grad.astype(jnp.bfloat16)
            start = n * inner % rows
            flat_grad[n * inner // rows, :, start : start + inner] = grad.T.astype(jnp.bfloat16)
            decayed = (turned.astype(jnp.float32) * rising).astype(jnp.bfloat16)
            carry = carry * whole + dot(decayed, co, 0, 0)
        for k in range(slots):
            grads[k][...] = whole_grad[pl.ds((here ^ k) * rows, rows), :]
            turned_grads[k][...] = flat_grad[here ^ k]

    return kernel


def second_kernel(slots, rows, inner, factor):
    def kernel(*refs):
        place, rate_ref, rotated, value, cosine, sine, trailing, keys = refs[:8]
        cotans = refs[8 : 8 + slots]
        grad_query, grad_value, cotan, key = refs[8 + slots :]
        here = place[0]
        rate = rate_ref[pl.program_id(0)]
        for k in range(slots):
            at = pl.ds((here ^ k) * rows, rows)
            cotan[at, :] = cotans[k][...]
            key[at, :] = keys[k * rows : (k + 1) * rows, :]
        within, flipped, rising, falling, whole = decays(rate, inner)
        seq_len = rotated.shape[0]
        carry = jnp.zeros((rotated.shape[1], value.shape[1]), jnp.float32)
        for n in range(seq_len // inner):
            at = slice(n * inner, (n + 1) * inner)
            cos, sin = cosine[at, :], sine[at, :]
            rk = (turn(key[at, :].astype(jnp.float32), cos, sin) * factor).astype(jnp.bfloat16)
            rq, co, va = rotated[at, :], cotan[at, :], value[at, :]
            score = (dot(rk, rq, 1, 1) * flipped).astype(jnp.bfloat16)
            entering = carry.astype(jnp.bfloat16)
            mix = (dot(co, va, 1, 1) * within).astype(jnp.bfloat16)
            grad = dot(mix, rk, 1, 0) + rising * dot(co, entering, 1, 1)
            grad_query[at, :] = turn_back(grad, cos, sin).astype(jnp.bfloat16)
            grad_value[at, :] = (
                dot(score, co, 1, 0) + falling * dot(rk, trailing[0, n], 1, 0)
            ).astype(jnp.bfloat16)
            decayed = (rk.astype(jnp.float32) * falling).astype(jnp.bfloat16)
            carry = carry * whole + dot(decayed, va, 0, 0)

    return kernel


def prefetch(*values):
    return jnp.stack([jnp.asarray(v, jnp.int32) for v in values])


def near(count=1):
    return [pl.BlockSpec(memory_space=pltpu.VMEM)] * count


def away(count=1):
    return [pl.BlockSpec(memory_space=pltpu.HBM)] * count


def smem():
    return pl.BlockSpec(memory_space=pltpu.SMEM)


def retention_first(here, rate, query, value, cosine, sine, cotans, key_width):
    slots = len(cotans)
    seq_len, query_width = query.shape
    heads = query_width // key_width
    value_width = value.shape[1] // heads
    rows = cotans[0].shape[0]
    inner = min(INNER, rows)
    nblocks = seq_len // inner
    half = jnp.bfloat16
    full = spec((seq_len, key_width), lambda h: (0, 0))
    head = spec((seq_len, key_width), lambda h: (0, h))
    outs = [pltpu.HBM((rows, query_width), half)] * slots
    outs += [pltpu.HBM((query_width, rows), half)] * slots
    outs += [
        pltpu.HBM((seq_len, query_width), half),
        pltpu.HBM((heads, nblocks, key_width, value_width), half),
    ]
    result = pl.pallas_call(
        first_kernel(slots, rows, inner, key_width**-0.5),
        grid=(heads,),
        in_specs=[smem(), smem(), head, spec((seq_len, value_width), lambda h: (0, h)), full, full]
        + [spec((rows, value_width), lambda h: (0, h))] * slots,
        out_specs=[spec((rows, key_width), lambda h: (0, h))] * slots
        + [spec((key_width, rows), lambda h: (h, 0))] * slots
        + [
            head,
            spec((1, nblocks, key_width, value_width), lambda h: (h, 0, 0, 0)),
        ],
        out_shape=outs,
        scratch_shapes=[
            pltpu.VMEM((seq_len, value_width), half),
            pltpu.VMEM((seq_len, key_width), half),
            pltpu.VMEM((slots, key_width, rows), half),
        ],
        compiler_params=limit(16),
        cost_estimate=cost(6e9, 10e6),
        name="retention_first",
    )(prefetch(here), rate, query, value, cosine, sine, *cotans)
    return list(result[:slots]), list(result[slots : 2 * slots]), *result[2 * slots :]


def retention_second(here, rate, rotated, value, cosine, sine, trailing, keys, cotans):
    slots = len(cotans)
    heads, nblocks, key_width, value_width = trailing.shape
    seq_len = rotated.shape[0]
    inner = seq_len // nblocks
    rows = cotans[0].shape[0]
    half = jnp.bfloat16
    full = spec((seq_len, key_width), lambda h: (0, 0))
    head = spec((seq_len, key_width), lambda h: (0, h))
    wide = spec((seq_len, value_width), lambda h: (0, h))
    return pl.pallas_call(
        second_kernel(slots, rows, inner, key_width**-0.5),
        grid=(heads,),
        in_specs=[
            smem(),
            smem(),
            head,
            wide,
            full,
            full,
            spec((1, nblocks, key_width, value_width), lambda h: (h, 0, 0, 0)),
            spec((slots * rows, key_width), lambda h: (0, h)),
        ]
        + [spec((rows, value_width), lambda h: (0, h))] * slots,
        out_specs=[head, wide],
        out_shape=[
            pltpu.HBM(rotated.shape, half),
            pltpu.HBM(value.shape, half),
        ],
        scratch_shapes=[
            pltpu.VMEM((seq_len, value_width), half),
            pltpu.VMEM((seq_len, key_width), half),
        ],
        compiler_params=limit(16),
        cost_estimate=cost(6e9, 14e6),
        name="retention_second",
    )(prefetch(here), rate, rotated, value, cosine, sine, trailing, keys, *cotans)


def halves(tokens):
    width = sum(part.shape[1] for part in tokens[0])
    found, place = ([], []), 0
    for k, parts in enumerate(tokens):
        for at, part in place_parts(parts):
            for piece in range(2 * part.shape[1] // width):
                found[2 * at // width + piece].append((k, place, piece))
            place += 1
    return found


def key_projection(here, plane, core, tokens, shards):
    slots = len(tokens)
    planes = len(shards)
    parts = [part for slot in tokens for part in slot]
    loads = halves(tokens)
    rows, width = tokens[0][0].shape[0], sum(part.shape[1] for part in tokens[0])
    share = shards[0][0].shape[0]
    half = width // 2

    def kernel(*refs):
        place = refs[0]
        token_refs = refs[1 : 1 + len(parts)]
        shard_refs = refs[1 + len(parts) : 1 + len(parts) + 2 * planes]
        out, weight, token, total, sems = refs[1 + len(parts) + 2 * planes :]
        slot, own = place[0], place[1]

        def weight_copy(r, side, at):
            return pltpu.make_async_copy(
                shard_refs[2 * r + side].at[:, at * half : (at + 1) * half],
                weight.at[at, pl.ds(pl.multiple_of((own ^ side) * share, share), share)],
                sems.at[at, slots + side],
            )

        def token_copy(at, k, index, piece):
            return pltpu.make_async_copy(
                token_refs[index].at[:, piece * half : (piece + 1) * half],
                token.at[at, k * rows : (k + 1) * rows],
                sems.at[at, k],
            )

        for at in range(2):
            for r in range(planes):

                @pl.when(slot == r)
                def _():
                    for side in range(2):
                        weight_copy(r, side, at).start()

            for k, index, piece in loads[at]:
                token_copy(at, k, index, piece).start()
        for at in range(2):
            for side in range(2):
                weight_copy(0, side, at).wait()
            for k, index, piece in loads[at]:
                token_copy(at, k, index, piece).wait()
            term = dot(token[at], weight[at], 1, 1)
            if at == 0:
                total[...] = term
            else:
                out[...] = (total[...] + term).astype(jnp.bfloat16)

    far = len(tokens[-1])
    return pl.pallas_call(
        kernel,
        in_specs=[smem()] + away(len(parts) - far) + near(far) + away(2 * planes),
        out_specs=near()[0],
        out_shape=pltpu.VMEM((slots * rows, 2 * share), jnp.bfloat16),
        scratch_shapes=[
            pltpu.VMEM((2, 2 * share, half), jnp.bfloat16),
            pltpu.VMEM((2, slots * rows, half), jnp.bfloat16),
            pltpu.VMEM((slots * rows, 2 * share), jnp.float32),
            pltpu.SemaphoreType.DMA((2, slots + 2)),
        ],
        compiler_params=limit(20),
        cost_estimate=cost(4e9, 8e6),
        name="key_projection",
    )(
        prefetch((plane - here) % planes, core),
        *parts,
        *[part for pair in shards for part in pair],
    )


def token_gradient(here, plane, core, grads, shards):
    slots = len(grads)
    planes = len(shards)
    rows = grads[0].shape[0]
    share, width = shards[0][0].shape

    def kernel(*refs):
        place = refs[0]
        grad_refs = refs[1 : 1 + slots]
        shard_refs = refs[1 + slots : 1 + slots + 2 * planes]
        out, grad, weight, total, sems = refs[1 + slots + 2 * planes :]
        own = place[2]

        def grad_copy(k):
            return pltpu.make_async_copy(grad_refs[k], grad.at[k], sems.at[2 * planes + k])

        def shard_copy(r, side):
            return pltpu.make_async_copy(
                shard_refs[2 * r + side], weight.at[r, own ^ side], sems.at[2 * r + side]
            )

        for k in range(slots):
            grad_copy(k).start()
        for r in range(planes):
            for side in range(2):
                shard_copy(r, side).start()
        for k in range(slots):
            grad_copy(k).wait()
        for r in range(planes):
            k = ((place[1] + planes - r) % planes) ^ place[0]
            for side in range(2):
                shard_copy(r, side).wait()
            block = grad[k]
            term = dot(block[:, :share], weight[r, 0], 1, 0)
            term += dot(block[:, share:], weight[r, 1], 1, 0)
            if r == 0:
                total[...] = term
            elif r < planes - 1:
                total[...] += term
            else:
                out[...] = (total[...] + term).astype(jnp.bfloat16)

    return pl.pallas_call(
        kernel,
        in_specs=[smem()] + away(slots + 2 * planes),
        out_specs=near()[0],
        out_shape=jax.ShapeDtypeStruct((rows, width), jnp.bfloat16),
        scratch_shapes=[
            pltpu.VMEM((slots, rows, 2 * share), jnp.bfloat16),
            pltpu.VMEM((planes, 2, share, width), jnp.bfloat16),
            pltpu.VMEM((rows, width), jnp.float32),
            pltpu.SemaphoreType.DMA((2 * planes + slots,)),
        ],
        compiler_params=limit(20),
        cost_estimate=cost(5e9, 11e6),
        name="token_gradient",
    )(prefetch(here, plane, core), *grads, *[part for pair in shards for part in pair])


def place_parts(parts):
    at, placed = 0, []
    for part in parts:
        placed.append((at, part))
        at += part.shape[1]
    return placed


def weight_start(grads, tokens):
    slots = len(tokens)
    features, rows = grads[0].shape
    parts = [part for slot in tokens for part in slot]
    loads = halves(tokens)
    width = sum(part.shape[1] for part in tokens[0])
    half = width // 2

    def kernel(*refs):
        grad_refs, token_refs = refs[: slots + 1], refs[slots + 1 : slots + 1 + len(parts)]
        out, last, grad, token, sems, grad_sems = refs[slots + 1 + len(parts) :]

        def fetch(at, k, index, piece):
            return pltpu.make_async_copy(
                token_refs[index].at[:, piece * half : (piece + 1) * half],
                token.at[at, k],
                sems.at[at, k],
            )

        def fetch_grad(k):
            to = grad.at[k] if k < slots else last
            return pltpu.make_async_copy(grad_refs[k], to, grad_sems.at[k])

        for k in range(slots):
            fetch_grad(k).start()
        for at in range(2):
            for load in loads[at]:
                fetch(at, *load).start()
        fetch_grad(slots).start()
        for k in range(slots):
            fetch_grad(k).wait()
        for at in range(2):
            for load in loads[at]:
                fetch(at, *load).wait()
            total = dot(grad[0], token[at, 0], 1, 0)
            for k in range(1, slots):
                total += dot(grad[k], token[at, k], 1, 0)
            out[:, at * half : (at + 1) * half] = total
        fetch_grad(slots).wait()

    return pl.pallas_call(
        kernel,
        in_specs=away(slots + 1 + len(parts)),
        out_specs=near(2),
        out_shape=[
            pltpu.VMEM((features, width), jnp.float32),
            pltpu.VMEM((features, rows), jnp.bfloat16),
        ],
        scratch_shapes=[
            pltpu.VMEM((slots, features, rows), jnp.bfloat16),
            pltpu.VMEM((2, slots, rows, half), jnp.bfloat16),
            pltpu.SemaphoreType.DMA((2, slots)),
            pltpu.SemaphoreType.DMA((slots + 1,)),
        ],
        compiler_params=limit(20),
        cost_estimate=cost(4e9, 6e6),
        name="weight_start",
    )(*grads, *parts)


def weight_end(core, grad, tokens, total):
    features, width = total.shape
    share = features // 2

    def kernel(place, grad_ref, *refs):
        token_refs, (so_far, sent, kept) = refs[: len(tokens)], refs[len(tokens) :]
        own = place[0]
        for (at, part), ref in zip(place_parts(tokens), token_refs):
            to = slice(at, at + part.shape[1])
            rows = pl.ds(pl.multiple_of((own ^ 1) * share, share), share)
            sent[:, to] = (so_far[rows, to] + dot(grad_ref[rows, :], ref[...], 1, 0)).astype(
                jnp.bfloat16
            )
        for (at, part), ref in zip(place_parts(tokens), token_refs):
            to = slice(at, at + part.shape[1])
            rows = pl.ds(pl.multiple_of(own * share, share), share)
            kept[:, to] = so_far[rows, to] + dot(grad_ref[rows, :], ref[...], 1, 0)

    return pl.pallas_call(
        kernel,
        in_specs=[smem()] + near(2 + len(tokens)),
        out_specs=near(2),
        out_shape=[
            pltpu.VMEM((share, width), jnp.bfloat16),
            pltpu.VMEM((share, width), jnp.float32),
        ],
        compiler_params=limit(20),
        cost_estimate=cost(4e9, 6e6),
        name="weight_end",
    )(prefetch(core), grad, *tokens, total)


def weight_pieces(here, slots, kept, received):
    share, width = kept.shape
    tile = width // slots

    def kernel(place, own, other, *outs):
        for k in range(slots):
            at = pl.ds(pl.multiple_of((place[0] ^ k) * tile, tile), tile)
            outs[k][...] = (own[:, at] + other[:, at].astype(jnp.float32)).astype(jnp.bfloat16)

    return pl.pallas_call(
        kernel,
        in_specs=[smem()] + near(2),
        out_specs=near(slots),
        out_shape=[pltpu.VMEM((share, tile), jnp.bfloat16)] * slots,
        compiler_params=limit(12),
        cost_estimate=cost(2e9, 6e6),
        name="weight_pieces",
    )(prefetch(here), kept, received)


def route(here, plane, planes, chunks, pieces):
    slots = len(pieces)
    share, tile = pieces[0].shape
    size = tile // chunks

    def kernel(place, *refs):
        outs, stack = refs[slots:-1], refs[-1]
        for k in range(slots):
            stack[k] = refs[k][...]
        for k in range(planes):
            slot = place[0] ^ place[1] ^ k
            for chunk in range(chunks):
                outs[chunk * planes + k][...] = stack[slot, :, chunk * size : (chunk + 1) * size]

    result = pl.pallas_call(
        kernel,
        in_specs=[smem()] + near(slots),
        out_specs=near(planes * chunks),
        out_shape=[pltpu.VMEM((share, size), jnp.bfloat16)] * (planes * chunks),
        scratch_shapes=[pltpu.VMEM((slots, share, tile), jnp.bfloat16)],
        compiler_params=limit(12),
        cost_estimate=cost(1e9, 2e6),
        name="route",
    )(prefetch(here, plane), *pieces)
    return [result[chunk * planes : (chunk + 1) * planes] for chunk in range(chunks)]


def add_up(terms):
    def kernel(*refs):
        total = refs[0][...].astype(jnp.float32)
        for ref in refs[1:-1]:
            total += ref[...].astype(jnp.float32)
        refs[-1][...] = total.astype(jnp.bfloat16)

    return pl.pallas_call(
        kernel,
        in_specs=near(len(terms)),
        out_specs=near()[0],
        out_shape=pltpu.VMEM(terms[0].shape, jnp.bfloat16),
        compiler_params=limit(12),
        cost_estimate=cost(1e9, 1e6),
        name="add_up",
    )(*terms)


def lay_out(here, pieces, chunk, chunks, out=None):
    slots = len(pieces)
    share, size = pieces[0].shape
    shape = jax.ShapeDtypeStruct((share, size * chunks * slots), jnp.float32)
    given = [] if out is None else [out]

    def kernel(place, *refs):
        target, wide, sems = refs[slots + len(given) :]

        def store(k):
            at = ((place[0] ^ k) * chunks + chunk) * size
            return pltpu.make_async_copy(
                wide.at[k], target.at[:, pl.ds(pl.multiple_of(at, size), size)], sems.at[k]
            )

        for k in range(slots):
            wide[k] = refs[k][...].astype(jnp.float32)
            store(k).start()
        for k in range(slots):
            store(k).wait()

    return pl.pallas_call(
        kernel,
        in_specs=[smem()] + near(slots) + away(len(given)),
        out_specs=away()[0],
        out_shape=shape,
        input_output_aliases={1 + slots: 0} if given else {},
        scratch_shapes=[
            pltpu.VMEM((slots, share, size), jnp.float32),
            pltpu.SemaphoreType.DMA((slots,)),
        ],
        compiler_params=limit(12),
        cost_estimate=cost(1e9, 4e6),
        name="lay_out",
    )(prefetch(here), *pieces, *given)


def gather_slots(array):
    half = array.shape[1] // 2
    low, high = array[:, :half], array[:, half:]
    near_high, next_low = swap(high, "sp", 1), swap(low, "sp", 2)
    near_low, next_high = swap(low, "sp", 1), swap(high, "sp", 2)
    far = [swap(next_low, "sp", 1), swap(near_high, "sp", 2)]
    return [[array], [near_low, near_high], [next_low, next_high], far]


def direct_body(tokens, key_weight, queries, values, cotangent, log_decay):
    return direct_steps(tokens, key_weight, queries, values, cotangent, log_decay)


def direct_steps(tokens, key_weight, queries, values, cotangent, log_decay):
    here, member = lax.axis_index("sp"), lax.axis_index("dp")
    slots = lax.axis_size("sp")
    planes = lax.axis_size("dp") // 2
    plane, core = member // 2, member % 2
    seq_len, heads, key_width = queries.shape[1:]
    value_width = values.shape[3]
    rate = lax.dynamic_slice_in_dim(log_decay, here * heads, heads)
    cosine, sine = rotation(seq_len, key_width // 2)
    cosine, sine = cosine[:, 0], sine[:, 0]
    cosine = jnp.concatenate([cosine, cosine], axis=1)
    sine = jnp.concatenate([-sine, sine], axis=1)

    ring = [key_weight]
    for _ in range(1, planes):
        ring.append(step_planes(ring[-1]))
    shards = [(part, swap(part, "dp", 1)) for part in ring]

    cotans = [columns(cotangent[0], here ^ k, heads * value_width) for k in range(slots)]
    cotans = cotans[:1] + [swap(cotans[k], "sp", k) for k in range(1, slots)]
    token_slots = gather_slots(tokens[0])

    query = queries[0].reshape(seq_len, heads * key_width)
    value = values[0].reshape(seq_len, heads * value_width)
    grads, turned_grads, rotated, trailing = retention_first(
        here, rate, query, value, cosine, sine, cotans, key_width
    )

    total, last = weight_start(turned_grads, token_slots[:-1])
    sent, kept = weight_end(core, last, token_slots[-1], total)
    received = swap(sent, "dp", 1)
    pieces = list(weight_pieces(here, slots, kept, received))
    pieces = pieces[:1] + [swap(pieces[k], "sp", k) for k in range(1, slots)]

    routed = route(here, plane, planes, CHUNKS, pieces)
    grad_weight = None
    for chunk, arrays in enumerate(routed):
        terms = [arrays[0]]
        terms += [swap(arrays[k], "dp", 2 * k) for k in range(1, planes)]
        total = add_up(terms)
        gathered = [total] + [swap(total, "sp", k) for k in range(1, slots)]
        grad_weight = lay_out(here, gathered, chunk, CHUNKS, grad_weight)

    returned = [grads[0]] + [swap(grads[k], "sp", k) for k in range(1, slots)]
    grad_tokens = token_gradient(here, plane, core, returned, shards)

    keys = key_projection(here, plane, core, token_slots, shards)
    grad_query, grad_value = retention_second(
        here, rate, rotated, value, cosine, sine, trailing, keys, cotans
    )
    grad_query = grad_query.reshape(queries.shape)
    grad_value = grad_value.reshape(values.shape)
    return (
        grad_tokens[None],
        grad_query,
        grad_value,
        grad_weight,
    )


def solution(mesh):
    slots, members = mesh.shape["sp"], mesh.shape["dp"]
    direct = members == 2 * slots and slots == 4
    return jax.shard_map(
        direct_body if direct else general_body,
        mesh=mesh,
        in_specs=(
            P("dp", "sp", None),
            P("dp", None),
            P("dp", None, "sp", None),
            P("dp", None, "sp", None),
            P("dp", "sp", None),
            P(),
        ),
        out_specs=(
            P("dp", "sp", None),
            P("dp", None, "sp", None),
            P("dp", None, "sp", None),
            P("dp", None),
        ),
        check_vma=False,
    )
```

profile of v0, /device:TPU:0, one launch (start us, length us, event | category | flops | bytes accessed | tf_op | source)
XLA Modules:
  0.0 187.0 jit_solution(2873138663721154085)
XLA Ops:
  0.7 3.0 %dynamic-slice_bitcast_fusion = (bf16[256,1024]{1,0:T(8,128)(2,1)}, bf16[256,1024]{1,0:T(8,128)(2,1)}, bf16[256,1024]{1,0:T(8,128)(2,1)}, bf16[256,1024]{1,0:T(8,128)(2,1)}) fusion(bf16[1,256,4096]{2,1,0:T(8,128)(2,1)} %param.10, s32[]{:T(128)S(6)} %select_n.36, s32[]{:T(128)S(6)} %select_n.34, s32[]{:T(128)S(6)} %select_n.33, s32[]{:T(128)S(6)} %select_n.35), kind=kLoop, calls=%fused_computation.3 | loop fusion | bytes 4194320 | tf_op jit(solution)/shard_map/dynamic_slice | solution.py:161
  3.6 3.0 %collective-permute-start = (bf16[256,1024]{1,0:T(8,128)(2,1)}, bf16[256,1024]{1,0:T(8,128)(2,1)}, u32[]{:S(2)}, u32[]{:S(2)}) collective-permute-start(bf16[256,1024]{1,0:T(8,128)(2,1)} %get-tuple-element.53), channel_id=1, source_target_pairs={{0,8},{8,0},{16,24},{24,16},{1,9},{9,1},{17,25},{25,17},{2,10},{10... | collective-permute-start | bytes 1572872 | tf_op jit(solution)/shard_map/ppermute | solution.py:142
  6.6 1.5 collective-permute-start.1
  9.2 2.0 %collective-permute-start.15 = (bf16[256,1024]{1,0:T(8,128)(2,1)}, bf16[256,1024]{1,0:T(8,128)(2,1)}, u32[]{:S(2)}, u32[]{:S(2)}) collective-permute-start(bf16[256,1024]{1,0:T(8,128)(2,1)} %get-tuple-element.57), channel_id=1, source_target_pairs={{0,16},{8,24},{16,0},{24,8},{1,17},{9,25},{17,1},{25,9},{2,18},{10... | collective-permute-start | bytes 1572872 | tf_op jit(solution)/shard_map/ppermute | solution.py:142
  13.8 2.1 %copy.11 = bf16[128,8,4,256]{3,1,2,0:T(8,128)(2,1)S(1)} copy(bf16[128,8,4,256]{3,2,1,0:T(4,128)(2,1)} %bitcast.28) | data formatting | bytes 4194304
  16.1 2.0 %fusion.2 = (f32[1024,64]{1,0:T(8,128)S(1)}, f32[1024,64]{1,0:T(8,128)S(1)}, f32[1024,64]{1,0:T(8,128)S(1)}) fusion(f32[64]{0:T(128)S(1)} %multiply_power_fusion), kind=kLoop, calls=%fused_computation.10 | loop fusion | flops 131072 | bytes 786688 | tf_op jit(solution)/shard_map/neg | solution.py:730
  18.0 1.7 collective-permute-done.refs_7_.refs_9_
  19.7 2.1 %collective-permute-start.7 = (bf16[256,2048]{1,0:T(8,128)(2,1)}, bf16[256,2048]{1,0:T(8,128)(2,1)}, u32[]{:S(2)}, u32[]{:S(2)}) collective-permute-start(bf16[256,2048]{1,0:T(8,128)(2,1)} %refs_8_.1), channel_id=1, source_target_pairs={{0,2},{1,3},{2,4},{3,5},{4,6},{5,7},{6,0},{7,1},{8,10},{9,11},{10,... | collective-permute-start | bytes 3145736 | tf_op jit(solution)/shard_map/ppermute | solution.py:147
  22.2 10.8 %collective-permute-done.1.refs_8_.refs_10_ = bf16[256,1024]{1,0:T(8,128)(2,1)} collective-permute-done((bf16[256,1024]{1,0:T(8,128)(2,1)}, bf16[256,1024]{1,0:T(8,128)(2,1)}, u32[]{:S(2)}, u32[]{:S(2)}) %collective-permute-start.1) | collective-permute-done | bytes 524320 | tf_op jit(solution)/shard_map/ppermute | solution.py:142
  33.0 2.1 %collective-permute-start.16 = (bf16[256,1024]{1,0:T(8,128)(2,1)}, bf16[256,1024]{1,0:T(8,128)(2,1)S(1)}, u32[]{:S(2)}, u32[]{:S(2)}) collective-permute-start(bf16[256,1024]{1,0:T(8,128)(2,1)} %get-tuple-element.56), channel_id=1, source_target_pairs={{0,16},{8,24},{16,0},{24,8},{1,17},{9,25},{17,1},{25,9},{2,18},{10... | collective-permute-start | bytes 1572872 | tf_op jit(solution)/shard_map/ppermute | solution.py:142
  35.0 9.2 %collective-permute-done.15.refs_4_.refs_7_ = bf16[256,1024]{1,0:T(8,128)(2,1)} collective-permute-done((bf16[256,1024]{1,0:T(8,128)(2,1)}, bf16[256,1024]{1,0:T(8,128)(2,1)}, u32[]{:S(2)}, u32[]{:S(2)}) %collective-permute-start.15) | collective-permute-done | bytes 524320 | tf_op jit(solution)/shard_map/ppermute | solution.py:142
  44.3 2.0 %collective-permute-start.18 = (bf16[256,1024]{1,0:T(8,128)(2,1)}, bf16[256,1024]{1,0:T(8,128)(2,1)S(1)}, u32[]{:S(2)}, u32[]{:S(2)}) collective-permute-start(bf16[256,1024]{1,0:T(8,128)(2,1)} %collective-permute-done.14.refs_3_.refs_6_), channel_id=1, source_target_pairs={{0,16},{8,24},{16,0},{24,8},{1,17},{9,25},{17,1},{25,9},{2,18},{10... | collective-permute-start | bytes 1572872 | tf_op jit(solution)/shard_map/ppermute | solution.py:142
  46.2 7.5 %retention_first.1 = (bf16[256,512]{1,0:T(8,128)(2,1)}, bf16[256,512]{1,0:T(8,128)(2,1)}, bf16[256,512]{1,0:T(8,128)(2,1)}, bf16[256,512]{1,0:T(8,128)(2,1)}, bf...) custom-call(s32[1]{0:T(128)} %bitcast.refs_0_.place, ...), custom_call_target="tpu_custom_call" | custom-call | flops 6000000000 | bytes 10000000 | tf_op jit(solution)/shard_map/retention_first/pallas_call | solution.py:298
  59.3 3.2 %weight_start.1 = (f32[512,2048]{1,0:T(8,128)S(1)}, bf16[512,256]{1,0:T(8,128)(2,1)S(1)}) custom-call(bf16[512,256]{1,0:T(8,128)(2,1)S(1)} %copy-done.27, bf16[512,256]{1,0:T(8,128)(2,1)S(1)} %copy-done.28, bf16[512,256]{1,0:T(8,128)(2,1)S(1)} %copy-done.29, bf16[512,256]{1,0:T(8,128)(2,1)S(1)} %copy-done.30, bf16[256,2048]{1,0:T(8,128)(2,1)S(1)} %bitcast.25, ...), custom_call_target="tpu_custom_call" | custom-call | flops 4000000000 | bytes 6000000 | tf_op jit(solution)/shard_map/weight_start/pallas_call | solution.py:552
  62.6 1.6 collective-permute-start.9
  66.0 21.2 %collective-permute-done.9.refs_9_.refs_12_ = bf16[256,2048]{1,0:T(8,128)(2,1)} collective-permute-done((bf16[256,2048]{1,0:T(8,128)(2,1)}, bf16[256,2048]{1,0:T(8,128)(2,1)}, u32[]{:S(2)}, u32[]{:S(2)}) %collective-permute-start.9) | collective-permute-done | bytes 1048608 | tf_op jit(solution)/shard_map/ppermute | solution.py:147
  89.5 1.5 collective-permute-start.21
  92.5 4.2 %collective-permute-done.20.refs_1_ = bf16[256,512]{1,0:T(8,128)(2,1)S(1)} collective-permute-done((bf16[256,512]{1,0:T(8,128)(2,1)}, bf16[256,512]{1,0:T(8,128)(2,1)S(1)}, u32[]{:S(2)}, u32[]{:S(2)}) %collective-permute-start.20) | collective-permute-done | bytes 262176 | tf_op jit(solution)/shard_map/ppermute | solution.py:142
  96.7 2.3 %collective-permute-done.21.refs_2_ = bf16[256,512]{1,0:T(8,128)(2,1)} collective-permute-done((bf16[256,512]{1,0:T(8,128)(2,1)}, bf16[256,512]{1,0:T(8,128)(2,1)}, u32[]{:S(2)}, u32[]{:S(2)}) %collective-permute-start.21) | collective-permute-done | bytes 262176 | tf_op jit(solution)/shard_map/ppermute | solution.py:142
  103.6 3.2 %collective-permute-start.24 = (bf16[256,512]{1,0:T(8,128)(2,1)S(1)}, bf16[256,512]{1,0:T(8,128)(2,1)S(1)}, u32[]{:S(2)}, u32[]{:S(2)}) collective-permute-start(bf16[256,512]{1,0:T(8,128)(2,1)S(1)} %get-tuple-element.50), channel_id=1, source_target_pairs={{0,4},{1,5},{2,6},{3,7},{4,0},{5,1},{6,2},{7,3},{8,12},{9,13},{10,... | collective-permute-start | bytes 786440 | tf_op jit(solution)/shard_map/ppermute | solution.py:142
  107.1 17.2 %collective-permute-done.23.refs_1_ = bf16[256,512]{1,0:T(8,128)(2,1)S(1)} collective-permute-done((bf16[256,512]{1,0:T(8,128)(2,1)S(1)}, bf16[256,512]{1,0:T(8,128)(2,1)S(1)}, u32[]{:S(2)}, u32[]{:S(2)}) %collective-permute-start.23) | collective-permute-done | bytes 262176 | tf_op jit(solution)/shard_map/ppermute | solution.py:142
  124.3 4.4 %collective-permute-done.24.refs_2_ = bf16[256,512]{1,0:T(8,128)(2,1)S(1)} collective-permute-done((bf16[256,512]{1,0:T(8,128)(2,1)S(1)}, bf16[256,512]{1,0:T(8,128)(2,1)S(1)}, u32[]{:S(2)}, u32[]{:S(2)}) %collective-permute-start.24) | collective-permute-done | bytes 262176 | tf_op jit(solution)/shard_map/ppermute | solution.py:142
  130.2 7.4 %collective-permute-done.26.refs_1_ = bf16[256,512]{1,0:T(8,128)(2,1)S(1)} collective-permute-done((bf16[256,512]{1,0:T(8,128)(2,1)S(1)}, bf16[256,512]{1,0:T(8,128)(2,1)S(1)}, u32[]{:S(2)}, u32[]{:S(2)}) %collective-permute-start.26) | collective-permute-done | bytes 262176 | tf_op jit(solution)/shard_map/ppermute | solution.py:142
  139.5 6.1 %collective-permute-done.27.refs_2_ = bf16[256,512]{1,0:T(8,128)(2,1)S(1)} collective-permute-done((bf16[256,512]{1,0:T(8,128)(2,1)S(1)}, bf16[256,512]{1,0:T(8,128)(2,1)S(1)}, u32[]{:S(2)}, u32[]{:S(2)}) %collective-permute-start.27) | collective-permute-done | bytes 262176 | tf_op jit(solution)/shard_map/ppermute | solution.py:142
  146.4 1.7 collective-permute-start.28
  148.9 5.0 %collective-permute-done.28.refs_3_ = bf16[256,512]{1,0:T(8,128)(2,1)} collective-permute-done((bf16[256,512]{1,0:T(8,128)(2,1)S(1)}, bf16[256,512]{1,0:T(8,128)(2,1)}, u32[]{:S(2)}, u32[]{:S(2)}) %collective-permute-start.28) | collective-permute-done | bytes 262176 | tf_op jit(solution)/shard_map/ppermute | solution.py:142
  157.5 2.3 %lay_out.1 = f32[256,2048]{1,0:T(8,128)} custom-call(s32[1]{0:T(128)} %bitcast.refs_0_.place, bf16[256,512]{1,0:T(8,128)(2,1)S(1)} %copy-done.17, bf16[256,512]{1,0:T(8,128)(2,1)S(1)} %copy-done.19, bf16[256,512]{1,0:T(8,128)(2,1)S(1)} %copy-done.21, bf16[256,512]{1,0:T(8,128)(2,1)} %collective-permute-done.28.refs_3_), custom_call_target="tpu_custom_call" | custom-call | flops 1000000000 | bytes 4000000 | tf_op jit(solution)/shard_map/lay_out/pallas_call | solution.py:690
  162.8 4.5 %key_projection.1.refs_7_ = bf16[1024,512]{1,0:T(8,128)(2,1)S(1)} custom-call(s32[2]{0:T(128)S(1)} %pad_add_fusion.1.refs_0_, bf16[256,2048]{1,0:T(8,128)(2,1)S(1)} %bitcast.26, bf16[256,1024]{1,0:T(8,128)(2,1)S(1)} %copy-done.9, bf16[256,1024]{1,0:T(8,128)(2,1)} %collective-permute-done.14.refs_3_.refs_6_, ...), custom_call_target="tpu_custom_call" | custom-call | flops 4000000000 | bytes 8000000 | tf_op jit(solution)/shard_map/key_projection/pallas_call | solution.py:424
  167.3 8.5 %retention_second.1 = (bf16[1024,512]{1,0:T(8,128)(2,1)}, bf16[1024,1024]{1,0:T(8,128)(2,1)}) custom-call(s32[1]{0:T(128)} %bitcast.refs_0_.place, f32[4]{0:T(128)S(1)} %dynamic_slice.23.refs_1_, bf16[1024,512]{1,0:T(8,128)(2,1)S(1)} %copy-done.24, bf16[1024,1024]{1,0:T(8,128)(2,1)S(1)} %bitcast.23, f32[1024,128]{1,0:T(8,128)S(1)} %copy-done.3, ...), custom_call_target="tpu_custom_call" | custom-call | flops 6000000000 | bytes 14000000 | tf_op jit(solution)/shard_map/retention_second/pallas_call | solution.py:332
  175.8 2.3 %reshape.24 = bf16[1,1024,4,128]{3,2,1,0:T(4,128)(2,1)} reshape(bf16[1024,512]{1,0:T(8,128)(2,1)} %get-tuple-element.34) | data formatting | bytes 2097152 | tf_op jit(solution)/shard_map/reshape | solution.py:769
  178.1 2.7 %reshape.25 = bf16[1,1024,4,256]{3,2,1,0:T(4,128)(2,1)} reshape(bf16[1024,1024]{1,0:T(8,128)(2,1)S(1)} %copy-done.31) | data formatting | bytes 4194304 | tf_op jit(solution)/shard_map/reshape | solution.py:770
  180.9 6.0 %token_gradient.1 = bf16[256,2048]{1,0:T(8,128)(2,1)} custom-call(s32[3]{0:T(128)S(1)} %pad_add_fusion.refs_0_, bf16[256,512]{1,0:T(8,128)(2,1)S(1)} %copy-done.26, bf16[256,512]{1,0:T(8,128)(2,1)S(1)} %collective-permute-done.3.refs_2_, bf16[256,512]{1,0:T(8,128)(2,1)} %collective-permute-done.4.refs_3_, bf16[256,512]{1,0:T(8,128)(2,1)} %collective-permute-done.5.refs_4_, ...), custom_call_target="tpu_custom_call" | custom-call | flops 5000000000 | bytes 11000000 | tf_op jit(solution)/shard_map/token_gradient/pallas_call | solution.py:487
  (117 shorter events, 31.7 us)
Async XLA Ops:
  3.6 16.1 %collective-permute-start = (bf16[256,1024]{1,0:T(8,128)(2,1)}, bf16[256,1024]{1,0:T(8,128)(2,1)}, u32[]{:S(2)}, u32[]{:S(2)}) collective-permute-start(bf16[256,1024]{1,0:T(8,128)(2,1)} %get-tuple-element.53), channel_id=1, source_target_pairs={{0,8},{8,0},{16,24},{24,16},{1,9},{9,1},{17,25},{25,17},{2,10},{10... | collective-permute-start | bytes 1572872 | tf_op jit(solution)/shard_map/ppermute | solution.py:142
  6.6 26.3 %collective-permute-start.1 = (bf16[256,1024]{1,0:T(8,128)(2,1)}, bf16[256,1024]{1,0:T(8,128)(2,1)}, u32[]{:S(2)}, u32[]{:S(2)}) collective-permute-start(bf16[256,1024]{1,0:T(8,128)(2,1)} %get-tuple-element.55), channel_id=1, source_target_pairs={{0,16},{8,24},{16,0},{24,8},{1,17},{9,25},{17,1},{25,9},{2,18},{10... | collective-permute-start | bytes 1572872 | tf_op jit(solution)/shard_map/ppermute | solution.py:142
  8.1 24.8 %collective-permute-start.2 = (bf16[256,1024]{1,0:T(8,128)(2,1)}, bf16[256,1024]{1,0:T(8,128)(2,1)}, u32[]{:S(2)}, u32[]{:S(2)}) collective-permute-start(bf16[256,1024]{1,0:T(8,128)(2,1)} %get-tuple-element.52), channel_id=1, source_target_pairs={{0,24},{8,16},{16,8},{24,0},{1,25},{9,17},{17,9},{25,1},{2,26},{10... | collective-permute-start | bytes 1572872 | tf_op jit(solution)/shard_map/ppermute | solution.py:142
  9.2 35.0 %collective-permute-start.15 = (bf16[256,1024]{1,0:T(8,128)(2,1)}, bf16[256,1024]{1,0:T(8,128)(2,1)}, u32[]{:S(2)}, u32[]{:S(2)}) collective-permute-start(bf16[256,1024]{1,0:T(8,128)(2,1)} %get-tuple-element.57), channel_id=1, source_target_pairs={{0,16},{8,24},{16,0},{24,8},{1,17},{9,25},{17,1},{25,9},{2,18},{10... | collective-permute-start | bytes 1572872 | tf_op jit(solution)/shard_map/ppermute | solution.py:142
  11.2 33.1 %collective-permute-start.14 = (bf16[256,1024]{1,0:T(8,128)(2,1)}, bf16[256,1024]{1,0:T(8,128)(2,1)}, u32[]{:S(2)}, u32[]{:S(2)}) collective-permute-start(bf16[256,1024]{1,0:T(8,128)(2,1)} %get-tuple-element.56), channel_id=1, source_target_pairs={{0,8},{8,0},{16,24},{24,16},{1,9},{9,1},{17,25},{25,17},{2,10},{10... | collective-permute-start | bytes 1572872 | tf_op jit(solution)/shard_map/ppermute | solution.py:142
  16.1 30.2 %copy-start.6 = (bf16[256,1024]{1,0:T(8,128)(2,1)S(1)}, bf16[256,1024]{1,0:T(8,128)(2,1)}, u32[]{:S(2)}) copy-start(bf16[256,1024]{1,0:T(8,128)(2,1)} %get-tuple-element.54.refs_6_.refs_8_) | copy-start | bytes 1572868
  19.7 42.9 %collective-permute-start.7 = (bf16[256,2048]{1,0:T(8,128)(2,1)}, bf16[256,2048]{1,0:T(8,128)(2,1)}, u32[]{:S(2)}, u32[]{:S(2)}) collective-permute-start(bf16[256,2048]{1,0:T(8,128)(2,1)} %refs_8_.1), channel_id=1, source_target_pairs={{0,2},{1,3},{2,4},{3,5},{4,6},{5,7},{6,0},{7,1},{8,10},{9,11},{10,... | collective-permute-start | bytes 3145736 | tf_op jit(solution)/shard_map/ppermute | solution.py:147
  22.1 31.7 %copy-start.2 = (f32[1024,128]{1,0:T(8,128)}, f32[1024,128]{1,0:T(8,128)S(1)}, u32[]{:S(2)}) copy-start(f32[1024,128]{1,0:T(8,128)S(1)} %get-tuple-element.61.refs_4_) | copy-start | bytes 1572868
  22.2 31.7 %copy-start.4 = (f32[1024,128]{1,0:T(8,128)}, f32[1024,128]{1,0:T(8,128)S(1)}, u32[]{:S(2)}) copy-start(f32[1024,128]{1,0:T(8,128)S(1)} %get-tuple-element.62.refs_5_) | copy-start | bytes 1572868
  32.9 20.9 %collective-permute-start.13 = (bf16[256,1024]{1,0:T(8,128)(2,1)}, bf16[256,1024]{1,0:T(8,128)(2,1)S(1)}, u32[]{:S(2)}, u32[]{:S(2)}) collective-permute-start(bf16[256,1024]{1,0:T(8,128)(2,1)} %get-tuple-element.57), channel_id=1, source_target_pairs={{0,8},{8,0},{16,24},{24,16},{1,9},{9,1},{17,25},{25,17},{2,10},{10... | collective-permute-start | bytes 1572872 | tf_op jit(solution)/shard_map/ppermute | solution.py:142
  33.0 22.4 %collective-permute-start.16 = (bf16[256,1024]{1,0:T(8,128)(2,1)}, bf16[256,1024]{1,0:T(8,128)(2,1)S(1)}, u32[]{:S(2)}, u32[]{:S(2)}) collective-permute-start(bf16[256,1024]{1,0:T(8,128)(2,1)} %get-tuple-element.56), channel_id=1, source_target_pairs={{0,16},{8,24},{16,0},{24,8},{1,17},{9,25},{17,1},{25,9},{2,18},{10... | collective-permute-start | bytes 1572872 | tf_op jit(solution)/shard_map/ppermute | solution.py:142
  44.2 20.0 %collective-permute-start.17 = (bf16[256,1024]{1,0:T(8,128)(2,1)}, bf16[256,1024]{1,0:T(8,128)(2,1)S(1)}, u32[]{:S(2)}, u32[]{:S(2)}) collective-permute-start(bf16[256,1024]{1,0:T(8,128)(2,1)} %collective-permute-done.15.refs_4_.refs_7_), channel_id=1, source_target_pairs={{0,8},{8,0},{16,24},{24,16},{1,9},{9,1},{17,25},{25,17},{2,10},{10... | collective-permute-start | bytes 1572872 | tf_op jit(solution)/shard_map/ppermute | solution.py:142
  44.3 20.9 %collective-permute-start.18 = (bf16[256,1024]{1,0:T(8,128)(2,1)}, bf16[256,1024]{1,0:T(8,128)(2,1)S(1)}, u32[]{:S(2)}, u32[]{:S(2)}) collective-permute-start(bf16[256,1024]{1,0:T(8,128)(2,1)} %collective-permute-done.14.refs_3_.refs_6_), channel_id=1, source_target_pairs={{0,16},{8,24},{16,0},{24,8},{1,17},{9,25},{17,1},{25,9},{2,18},{10... | collective-permute-start | bytes 1572872 | tf_op jit(solution)/shard_map/ppermute | solution.py:142
  62.6 24.6 %collective-permute-start.9 = (bf16[256,2048]{1,0:T(8,128)(2,1)}, bf16[256,2048]{1,0:T(8,128)(2,1)}, u32[]{:S(2)}, u32[]{:S(2)}) collective-permute-start(bf16[256,2048]{1,0:T(8,128)(2,1)} %collective-permute-done.7.refs_7_.refs_10_), channel_id=1, source_target_pairs={{0,2},{1,3},{2,4},{3,5},{4,6},{5,7},{6,0},{7,1},{8,10},{9,11},{10,... | collective-permute-start | bytes 3145736 | tf_op jit(solution)/shard_map/ppermute | solution.py:147
  65.9 21.2 %collective-permute-start.19 = (bf16[256,2048]{1,0:T(8,128)(2,1)S(1)}, bf16[256,2048]{1,0:T(8,128)(2,1)S(1)}, u32[]{:S(2)}, u32[]{:S(2)}) collective-permute-start(bf16[256,2048]{1,0:T(8,128)(2,1)S(1)} %get-tuple-element.43), channel_id=1, source_target_pairs={{0,1},{1,0},{2,3},{3,2},{4,5},{5,4},{6,7},{7,6},{8,9},{9,8},{10,11... | collective-permute-start | bytes 3145736 | tf_op jit(solution)/shard_map/ppermute | solution.py:142
  87.1 41.5 %collective-permute-start.11 = (bf16[256,2048]{1,0:T(8,128)(2,1)}, bf16[256,2048]{1,0:T(8,128)(2,1)}, u32[]{:S(2)}, u32[]{:S(2)}) collective-permute-start(bf16[256,2048]{1,0:T(8,128)(2,1)} %collective-permute-done.9.refs_9_.refs_12_), channel_id=1, source_target_pairs={{0,2},{1,3},{2,4},{3,5},{4,6},{5,7},{6,0},{7,1},{8,10},{9,11},{10,... | collective-permute-start | bytes 3145736 | tf_op jit(solution)/shard_map/ppermute | solution.py:147
  88.9 7.8 %collective-permute-start.20 = (bf16[256,512]{1,0:T(8,128)(2,1)}, bf16[256,512]{1,0:T(8,128)(2,1)S(1)}, u32[]{:S(2)}, u32[]{:S(2)}) collective-permute-start(bf16[256,512]{1,0:T(8,128)(2,1)} %get-tuple-element.45), channel_id=1, source_target_pairs={{0,8},{8,0},{16,24},{24,16},{1,9},{9,1},{17,25},{25,17},{2,10},{10... | collective-permute-start | bytes 786440 | tf_op jit(solution)/shard_map/ppermute | solution.py:142
  89.5 9.5 %collective-permute-start.21 = (bf16[256,512]{1,0:T(8,128)(2,1)}, bf16[256,512]{1,0:T(8,128)(2,1)}, u32[]{:S(2)}, u32[]{:S(2)}) collective-permute-start(bf16[256,512]{1,0:T(8,128)(2,1)} %get-tuple-element.46), channel_id=1, source_target_pairs={{0,16},{8,24},{16,0},{24,8},{1,17},{9,25},{17,1},{25,9},{2,18},{10... | collective-permute-start | bytes 786440 | tf_op jit(solution)/shard_map/ppermute | solution.py:142
  91.0 9.5 %collective-permute-start.22 = (bf16[256,512]{1,0:T(8,128)(2,1)}, bf16[256,512]{1,0:T(8,128)(2,1)}, u32[]{:S(2)}, u32[]{:S(2)}) collective-permute-start(bf16[256,512]{1,0:T(8,128)(2,1)} %get-tuple-element.47), channel_id=1, source_target_pairs={{0,24},{8,16},{16,8},{24,0},{1,25},{9,17},{17,9},{25,1},{2,26},{10... | collective-permute-start | bytes 786440 | tf_op jit(solution)/shard_map/ppermute | solution.py:142
  102.6 21.6 %collective-permute-start.23 = (bf16[256,512]{1,0:T(8,128)(2,1)S(1)}, bf16[256,512]{1,0:T(8,128)(2,1)S(1)}, u32[]{:S(2)}, u32[]{:S(2)}) collective-permute-start(bf16[256,512]{1,0:T(8,128)(2,1)S(1)} %get-tuple-element.49), channel_id=1, source_target_pairs={{0,2},{1,3},{2,0},{3,1},{4,6},{5,7},{6,4},{7,5},{8,10},{9,11},{10,... | collective-permute-start | bytes 786440 | tf_op jit(solution)/shard_map/ppermute | solution.py:142
  103.6 25.0 %collective-permute-start.24 = (bf16[256,512]{1,0:T(8,128)(2,1)S(1)}, bf16[256,512]{1,0:T(8,128)(2,1)S(1)}, u32[]{:S(2)}, u32[]{:S(2)}) collective-permute-start(bf16[256,512]{1,0:T(8,128)(2,1)S(1)} %get-tuple-element.50), channel_id=1, source_target_pairs={{0,4},{1,5},{2,6},{3,7},{4,0},{5,1},{6,2},{7,3},{8,12},{9,13},{10,... | collective-permute-start | bytes 786440 | tf_op jit(solution)/shard_map/ppermute | solution.py:142
  106.8 22.4 %collective-permute-start.25 = (bf16[256,512]{1,0:T(8,128)(2,1)S(1)}, bf16[256,512]{1,0:T(8,128)(2,1)S(1)}, u32[]{:S(2)}, u32[]{:S(2)}) collective-permute-start(bf16[256,512]{1,0:T(8,128)(2,1)S(1)} %get-tuple-element.51), channel_id=1, source_target_pairs={{0,6},{1,7},{2,4},{3,5},{4,2},{5,3},{6,0},{7,1},{8,14},{9,15},{10,... | collective-permute-start | bytes 786440 | tf_op jit(solution)/shard_map/ppermute | solution.py:142
  107.1 52.8 %collective-permute-start.6 = (bf16[256,2048]{1,0:T(8,128)(2,1)}, bf16[256,2048]{1,0:T(8,128)(2,1)}, u32[]{:S(2)}, u32[]{:S(2)}) collective-permute-start(bf16[256,2048]{1,0:T(8,128)(2,1)} %refs_8_.1), channel_id=1, source_target_pairs={{0,1},{1,0},{2,3},{3,2},{4,5},{5,4},{6,7},{7,6},{8,9},{9,8},{10,11... | collective-permute-start | bytes 3145736 | tf_op jit(solution)/shard_map/ppermute | solution.py:142
  124.3 37.1 %collective-permute-start.8 = (bf16[256,2048]{1,0:T(8,128)(2,1)}, bf16[256,2048]{1,0:T(8,128)(2,1)}, u32[]{:S(2)}, u32[]{:S(2)}) collective-permute-start(bf16[256,2048]{1,0:T(8,128)(2,1)} %collective-permute-done.7.refs_7_.refs_10_), channel_id=1, source_target_pairs={{0,1},{1,0},{2,3},{3,2},{4,5},{5,4},{6,7},{7,6},{8,9},{9,8},{10,11... | collective-permute-start | bytes 3145736 | tf_op jit(solution)/shard_map/ppermute | solution.py:142
  128.7 34.1 %collective-permute-start.10 = (bf16[256,2048]{1,0:T(8,128)(2,1)}, bf16[256,2048]{1,0:T(8,128)(2,1)}, u32[]{:S(2)}, u32[]{:S(2)}) collective-permute-start(bf16[256,2048]{1,0:T(8,128)(2,1)} %collective-permute-done.9.refs_9_.refs_12_), channel_id=1, source_target_pairs={{0,1},{1,0},{2,3},{3,2},{4,5},{5,4},{6,7},{7,6},{8,9},{9,8},{10,11... | collective-permute-start | bytes 3145736 | tf_op jit(solution)/shard_map/ppermute | solution.py:142
  128.7 34.1 %collective-permute-start.12 = (bf16[256,2048]{1,0:T(8,128)(2,1)}, bf16[256,2048]{1,0:T(8,128)(2,1)}, u32[]{:S(2)}, u32[]{:S(2)}) collective-permute-start(bf16[256,2048]{1,0:T(8,128)(2,1)} %collective-permute-done.11.refs_11_.refs_14_), channel_id=1, source_target_pairs={{0,1},{1,0},{2,3},{3,2},{4,5},{5,4},{6,7},{7,6},{8,9},{9,8},{10,11... | collective-permute-start | bytes 3145736 | tf_op jit(solution)/shard_map/ppermute | solution.py:142
  129.3 8.3 %collective-permute-start.26 = (bf16[256,512]{1,0:T(8,128)(2,1)S(1)}, bf16[256,512]{1,0:T(8,128)(2,1)S(1)}, u32[]{:S(2)}, u32[]{:S(2)}) collective-permute-start(bf16[256,512]{1,0:T(8,128)(2,1)S(1)} %add_up.1.refs_0_), channel_id=1, source_target_pairs={{0,8},{8,0},{16,24},{24,16},{1,9},{9,1},{17,25},{25,17},{2,10},{10... | collective-permute-start | bytes 786440 | tf_op jit(solution)/shard_map/ppermute | solution.py:142
  138.3 7.4 %collective-permute-start.27 = (bf16[256,512]{1,0:T(8,128)(2,1)S(1)}, bf16[256,512]{1,0:T(8,128)(2,1)S(1)}, u32[]{:S(2)}, u32[]{:S(2)}) collective-permute-start(bf16[256,512]{1,0:T(8,128)(2,1)S(1)} %add_up.1.refs_0_), channel_id=1, source_target_pairs={{0,16},{8,24},{16,0},{24,8},{1,17},{9,25},{17,1},{25,9},{2,18},{10... | collective-permute-start | bytes 786440 | tf_op jit(solution)/shard_map/ppermute | solution.py:142
  146.4 7.5 %collective-permute-start.28 = (bf16[256,512]{1,0:T(8,128)(2,1)S(1)}, bf16[256,512]{1,0:T(8,128)(2,1)}, u32[]{:S(2)}, u32[]{:S(2)}) collective-permute-start(bf16[256,512]{1,0:T(8,128)(2,1)S(1)} %add_up.1.refs_0_), channel_id=1, source_target_pairs={{0,24},{8,16},{16,8},{24,0},{1,25},{9,17},{17,9},{25,1},{2,26},{10... | collective-permute-start | bytes 786440 | tf_op jit(solution)/shard_map/ppermute | solution.py:142
  153.9 26.9 %collective-permute-start.3 = (bf16[256,512]{1,0:T(8,128)(2,1)}, bf16[256,512]{1,0:T(8,128)(2,1)S(1)}, u32[]{:S(2)}, u32[]{:S(2)}) collective-permute-start(bf16[256,512]{1,0:T(8,128)(2,1)} %get-tuple-element.29), channel_id=1, source_target_pairs={{0,8},{8,0},{16,24},{24,16},{1,9},{9,1},{17,25},{25,17},{2,10},{10... | collective-permute-start | bytes 786440 | tf_op jit(solution)/shard_map/ppermute | solution.py:142
  159.9 21.0 %collective-permute-start.4 = (bf16[256,512]{1,0:T(8,128)(2,1)}, bf16[256,512]{1,0:T(8,128)(2,1)}, u32[]{:S(2)}, u32[]{:S(2)}) collective-permute-start(bf16[256,512]{1,0:T(8,128)(2,1)} %get-tuple-element.30), channel_id=1, source_target_pairs={{0,16},{8,24},{16,0},{24,8},{1,17},{9,25},{17,1},{25,9},{2,18},{10... | collective-permute-start | bytes 786440 | tf_op jit(solution)/shard_map/ppermute | solution.py:142
  161.4 19.4 %collective-permute-start.5 = (bf16[256,512]{1,0:T(8,128)(2,1)}, bf16[256,512]{1,0:T(8,128)(2,1)}, u32[]{:S(2)}, u32[]{:S(2)}) collective-permute-start(bf16[256,512]{1,0:T(8,128)(2,1)} %get-tuple-element.31), channel_id=1, source_target_pairs={{0,24},{8,16},{16,8},{24,0},{1,25},{9,17},{17,9},{25,1},{2,26},{10... | collective-permute-start | bytes 786440 | tf_op jit(solution)/shard_map/ppermute | solution.py:142
  (31 other events, 168.6 us)
where the time goes:
time: 188 us; the launch traced here: 187 us
  waiting for transfers between devices  93.4 us (50%)
  Pallas kernels  35.1 us (19%)
  starting transfers between devices  31.7 us (17%)
  local copies, waits for them, and re-layouts  23.1 us (12%)
  other arithmetic  2.53 us (1%)
    ppermute x26, waiting for transfers between devices, swap(): return lax.ppermute(array, axis, [(i, i ^ bit) for i in range(count)])  72.2 us
    ppermute x26, starting transfers between devices, swap(): return lax.ppermute(array, axis, [(i, i ^ bit) for i in range(count)])  27.9 us
    ppermute x3, waiting for transfers between devices, step_planes(): lax.ppermute(array, 'dp', [(i, (i + 2) % count) for i in range(count)])  21.2 us
    unnamed x70, local copies, waits for them, and re-layouts  14 us
    pallas_call x1, Pallas kernels, retention_second(): pl.pallas_call(second_kernel(slots, rows, inner, key_width ** (-0.5)), gr...  8.46 us
    pallas_call x1, Pallas kernels, retention_first(): pl.pallas_call(first_kernel(slots, rows, inner, key_width ** (-0.5)), gri...  7.55 us
    pallas_call x1, Pallas kernels, token_gradient(): pl.pallas_call(kernel, in_specs=[smem()] + away(slots + 2 * planes), out_...  5.97 us
    pallas_call x1, Pallas kernels, key_projection(): pl.pallas_call(kernel, in_specs=[smem()] + away(len(parts) - far) + near(...  4.5 us
  transfers between devices with their start and end apart: 29, of which 14 were waited for; matrix products, arithmetic and copies ran while one was open for 6% of the time, Pallas kernels for 16%

commit v1 on v0

--- a/solution.py
+++ b/solution.py
@@ -134,7 +134,7 @@
 
 
 INNER = 256
-CHUNKS = 1
+CHUNKS = 2
 
 
 def swap(array, axis, bit):
@@ -569,117 +569,112 @@
     )(*grads, *parts)
 
 
-def weight_end(core, grad, tokens, total):
+def weight_end(side, grad, tokens, total, kind):
     features, width = total.shape
     share = features // 2
 
     def kernel(place, grad_ref, *refs):
-        token_refs, (so_far, sent, kept) = refs[: len(tokens)], refs[len(tokens) :]
-        own = place[0]
+        token_refs, (so_far, out) = refs[: len(tokens)], refs[len(tokens) :]
+        rows = pl.ds(pl.multiple_of(place[0] * share, share), share)
         for (at, part), ref in zip(place_parts(tokens), token_refs):
             to = slice(at, at + part.shape[1])
-            rows = pl.ds(pl.multiple_of((own ^ 1) * share, share), share)
-            sent[:, to] = (so_far[rows, to] + dot(grad_ref[rows, :], ref[...], 1, 0)).astype(
-                jnp.bfloat16
-            )
-        for (at, part), ref in zip(place_parts(tokens), token_refs):
-            to = slice(at, at + part.shape[1])
-            rows = pl.ds(pl.multiple_of(own * share, share), share)
-            kept[:, to] = so_far[rows, to] + dot(grad_ref[rows, :], ref[...], 1, 0)
+            term = dot(grad_ref[rows, :], ref[...], 1, 0)
+            out[:, to] = (so_far[rows, to] + term).astype(kind)
 
     return pl.pallas_call(
         kernel,
         in_specs=[smem()] + near(2 + len(tokens)),
-        out_specs=near(2),
-        out_shape=[
-            pltpu.VMEM((share, width), jnp.bfloat16),
-            pltpu.VMEM((share, width), jnp.float32),
-        ],
+        out_specs=near()[0],
+        out_shape=pltpu.VMEM((share, width), kind),
         compiler_params=limit(20),
-        cost_estimate=cost(4e9, 6e6),
+        cost_estimate=cost(2e9, 6e6),
         name="weight_end",
-    )(prefetch(core), grad, *tokens, total)
-
-
-def weight_pieces(here, slots, kept, received):
+    )(prefetch(side), grad, *tokens, total)
+
+
+def weight_pieces(here, slots, chunks, kept, received):
     share, width = kept.shape
     tile = width // slots
+    size = tile // chunks
 
     def kernel(place, own, other, *outs):
         for k in range(slots):
-            at = pl.ds(pl.multiple_of((place[0] ^ k) * tile, tile), tile)
-            outs[k][...] = (own[:, at] + other[:, at].astype(jnp.float32)).astype(jnp.bfloat16)
-
-    return pl.pallas_call(
+            for chunk in range(chunks):
+                start = pl.multiple_of((place[0] ^ k) * tile + chunk * size, size)
+                at = pl.ds(start, size)
+                total = own[:, at] + other[:, at].astype(jnp.float32)
+                outs[chunk * slots + k][...] = total.astype(jnp.bfloat16)
+
+    result = pl.pallas_call(
         kernel,
         in_specs=[smem()] + near(2),
-        out_specs=near(slots),
-        out_shape=[pltpu.VMEM((share, tile), jnp.bfloat16)] * slots,
+        out_specs=near(slots * chunks),
+        out_shape=([pltpu.HBM((share, size), jnp.bfloat16)] + [pltpu.VMEM((share, size), jnp.bfloat16)] * (slots - 1)) * chunks,
         compiler_params=limit(12),
         cost_estimate=cost(2e9, 6e6),
         name="weight_pieces",
     )(prefetch(here), kept, received)
-
-
-def route(here, plane, planes, chunks, pieces):
+    return [result[chunk * slots : (chunk + 1) * slots] for chunk in range(chunks)]
+
+
+def route(here, plane, planes, pieces):
     slots = len(pieces)
-    share, tile = pieces[0].shape
-    size = tile // chunks
+    shape = pieces[0].shape
 
     def kernel(place, *refs):
-        outs, stack = refs[slots:-1], refs[-1]
-        for k in range(slots):
+        outs, (stack, sem) = refs[slots:-2], refs[-2:]
+        own = pltpu.make_async_copy(refs[0], stack.at[0], sem)
+        own.start()
+        for k in range(1, slots):
             stack[k] = refs[k][...]
+        own.wait()
         for k in range(planes):
-            slot = place[0] ^ place[1] ^ k
-            for chunk in range(chunks):
-                outs[chunk * planes + k][...] = stack[slot, :, chunk * size : (chunk + 1) * size]
-
-    result = pl.pallas_call(
+            outs[k][...] = stack[place[0] ^ place[1] ^ k]
+
+    return pl.pallas_call(
         kernel,
-        in_specs=[smem()] + near(slots),
-        out_specs=near(planes * chunks),
-        out_shape=[pltpu.VMEM((share, size), jnp.bfloat16)] * (planes * chunks),
-        scratch_shapes=[pltpu.VMEM((slots, share, tile), jnp.bfloat16)],
+        in_specs=[smem()] + away() + near(slots - 1),
+        out_specs=near(planes),
+        out_shape=[pltpu.VMEM(shape, jnp.bfloat16)] * planes,
+        scratch_shapes=[pltpu.VMEM((slots, *shape), jnp.bfloat16), pltpu.SemaphoreType.DMA],
         compiler_params=limit(12),
         cost_estimate=cost(1e9, 2e6),
         name="route",
     )(prefetch(here, plane), *pieces)
-    return [result[chunk * planes : (chunk + 1) * planes] for chunk in range(chunks)]
-
-
-def add_up(terms):
+
+
+def add_up(groups):
+    count, (rows, size) = len(groups[0]), groups[0][0].shape
+
     def kernel(*refs):
-        total = refs[0][...].astype(jnp.float32)
-        for ref in refs[1:-1]:
-            total += ref[...].astype(jnp.float32)
-        refs[-1][...] = total.astype(jnp.bfloat16)
+        for side in range(len(groups)):
+            terms = refs[side * count : (side + 1) * count]
+            total = terms[0][...].astype(jnp.float32)
+            for ref in terms[1:]:
+                total += ref[...].astype(jnp.float32)
+            refs[-1][:, side * size : (side + 1) * size] = total.astype(jnp.bfloat16)
 
     return pl.pallas_call(
         kernel,
-        in_specs=near(len(terms)),
+        in_specs=near(count * len(groups)),
         out_specs=near()[0],
-        out_shape=pltpu.VMEM(terms[0].shape, jnp.bfloat16),
+        out_shape=pltpu.VMEM((rows, size * len(groups)), jnp.bfloat16),
         compiler_params=limit(12),
         cost_estimate=cost(1e9, 1e6),
         name="add_up",
-    )(*terms)
-
-
-def lay_out(here, pieces, chunk, chunks, out=None):
+    )(*[term for group in groups for term in group])
+
+
+def lay_out(here, pieces):
     slots = len(pieces)
     share, size = pieces[0].shape
-    shape = jax.ShapeDtypeStruct((share, size * chunks * slots), jnp.float32)
-    given = [] if out is None else [out]
 
     def kernel(place, *refs):
-        target, wide, sems = refs[slots + len(given) :]
+        out, wide, sems = refs[slots:]
 
         def store(k):
-            at = ((place[0] ^ k) * chunks + chunk) * size
-            return pltpu.make_async_copy(
-                wide.at[k], target.at[:, pl.ds(pl.multiple_of(at, size), size)], sems.at[k]
-            )
+            at = pl.ds(pl.multiple_of((place[0] ^ k) * size, size), size)
+            return pltpu.make_async_copy(wide.at[k], out.at[:, at], sems.at[k])
 
         for k in range(slots):
             wide[k] = refs[k][...].astype(jnp.float32)
@@ -689,10 +684,9 @@
 
     return pl.pallas_call(
         kernel,
-        in_specs=[smem()] + near(slots) + away(len(given)),
+        in_specs=[smem()] + near(slots),
         out_specs=away()[0],
-        out_shape=shape,
-        input_output_aliases={1 + slots: 0} if given else {},
+        out_shape=jax.ShapeDtypeStruct((share, size * slots), jnp.float32),
         scratch_shapes=[
             pltpu.VMEM((slots, share, size), jnp.float32),
             pltpu.SemaphoreType.DMA((slots,)),
@@ -700,7 +694,7 @@
         compiler_params=limit(12),
         cost_estimate=cost(1e9, 4e6),
         name="lay_out",
-    )(prefetch(here), *pieces, *given)
+    )(prefetch(here), *pieces)
 
 
 def gather_slots(array):
@@ -745,19 +739,19 @@
     )
 
     total, last = weight_start(turned_grads, token_slots[:-1])
-    sent, kept = weight_end(core, last, token_slots[-1], total)
+    sent = weight_end(core ^ 1, last, token_slots[-1], total, jnp.bfloat16)
     received = swap(sent, "dp", 1)
-    pieces = list(weight_pieces(here, slots, kept, received))
-    pieces = pieces[:1] + [swap(pieces[k], "sp", k) for k in range(1, slots)]
-
-    routed = route(here, plane, planes, CHUNKS, pieces)
-    grad_weight = None
-    for chunk, arrays in enumerate(routed):
-        terms = [arrays[0]]
-        terms += [swap(arrays[k], "dp", 2 * k) for k in range(1, planes)]
-        total = add_up(terms)
-        gathered = [total] + [swap(total, "sp", k) for k in range(1, slots)]
-        grad_weight = lay_out(here, gathered, chunk, CHUNKS, grad_weight)
+    kept = weight_end(core, last, token_slots[-1], total, jnp.float32)
+    chunks = weight_pieces(here, slots, CHUNKS, kept, received)
+    groups = []
+    for pieces in chunks:
+        came = [pieces[0]] + [swap(pieces[k], "sp", k) for k in range(1, slots)]
+        terms = route(here, plane, planes, came)
+        others = [swap(terms[k], "dp", 2 * k) for k in range(1, planes)]
+        groups.append([terms[0]] + others)
+    total = add_up(groups)
+    gathered = [total] + [swap(total, "sp", k) for k in range(1, slots)]
+    grad_weight = lay_out(here, gathered)
 
     returned = [grads[0]] + [swap(grads[k], "sp", k) for k in range(1, slots)]
     grad_tokens = token_gradient(here, plane, core, returned, shards)

time: 188 us -> 181 us (0.963)
  waiting for transfers between devices: 93.4 us -> 78.6 us
  starting transfers between devices: 31.7 us -> 39.2 us
    ppermute x3, waiting for transfers between devices: 21.2 us -> 12.2 us  [step_planes(): lax.ppermute(array, 'dp', [(i, (i + 2) % count) for i in range(count)])]
    ppermute x26 -> x32, starting transfers between devices: 27.9 us -> 35.2 us  [swap(): return lax.ppermute(array, axis, [(i, i ^ bit) for i in range(count)])]
    ppermute x26 -> x32, waiting for transfers between devices: 72.2 us -> 66.4 us  [swap(): return lax.ppermute(array, axis, [(i, i ^ bit) for i in range(count)])]
    pallas_call x4 -> x5, Pallas kernels: 4.65 us -> 5.5 us  [the longest x1 2.33 us: lay_out(): pl.pallas_call(kernel, in_specs=[smem()] + near(slots), out_specs=away()[...]
  transfers between devices with their start and end apart: 29 -> 35, of which waited for: 14 -> 14; matrix products, arithmetic and copies ran while one was open for 6% -> 7% of each run, Pallas kernels for 16% -> 17%
where the time goes in v1:
time: 181 us; the launch traced here: 180 us
  waiting for transfers between devices  78.6 us (43%)
  starting transfers between devices  39.2 us (22%)
  Pallas kernels  36.1 us (20%)
  local copies, waits for them, and re-layouts  22.4 us (12%)
  other arithmetic  2.54 us (1%)
    ppermute x32, waiting for transfers between devices, swap(): return lax.ppermute(array, axis, [(i, i ^ bit) for i in range(count)])  66.4 us
    ppermute x32, starting transfers between devices, swap(): return lax.ppermute(array, axis, [(i, i ^ bit) for i in range(count)])  35.2 us
    unnamed x70, local copies, waits for them, and re-layouts  13.2 us
    ppermute x3, waiting for transfers between devices, step_planes(): lax.ppermute(array, 'dp', [(i, (i + 2) % count) for i in range(count)])  12.2 us
    pallas_call x1, Pallas kernels, retention_second(): pl.pallas_call(second_kernel(slots, rows, inner, key_width ** (-0.5)), gr...  8.46 us
    pallas_call x1, Pallas kernels, retention_first(): pl.pallas_call(first_kernel(slots, rows, inner, key_width ** (-0.5)), gri...  7.55 us
    pallas_call x1, Pallas kernels, token_gradient(): pl.pallas_call(kernel, in_specs=[smem()] + away(slots + 2 * planes), out_...  5.97 us
    pallas_call x1, Pallas kernels, key_projection(): pl.pallas_call(kernel, in_specs=[smem()] + away(len(parts) - far) + near(...  4.5 us
  transfers between devices with their start and end apart: 35, of which 14 were waited for; matrix products, arithmetic and copies ran while one was open for 7% of the time, Pallas kernels for 17%

profile of v1, /device:TPU:0, one launch (start us, length us, event | category | flops | bytes accessed | tf_op | source)
XLA Modules:
  0.0 180.0 jit_solution(5738001353313667816)
XLA Ops:
  0.7 3.0 %dynamic-slice_bitcast_fusion = (bf16[256,1024]{1,0:T(8,128)(2,1)}, bf16[256,1024]{1,0:T(8,128)(2,1)}, bf16[256,1024]{1,0:T(8,128)(2,1)}, bf16[256,1024]{1,0:T(8,128)(2,1)}) fusion(bf16[1,256,4096]{2,1,0:T(8,128)(2,1)} %param.10, s32[]{:T(128)S(6)} %select_n.36, s32[]{:T(128)S(6)} %select_n.34, s32[]{:T(128)S(6)} %select_n.33, s32[]{:T(128)S(6)} %select_n.35), kind=kLoop, calls=%fused_computation.3 | loop fusion | bytes 4194320 | tf_op jit(solution)/shard_map/dynamic_slice | solution.py:161
  3.6 3.0 %collective-permute-start = (bf16[256,1024]{1,0:T(8,128)(2,1)}, bf16[256,1024]{1,0:T(8,128)(2,1)}, u32[]{:S(2)}, u32[]{:S(2)}) collective-permute-start(bf16[256,1024]{1,0:T(8,128)(2,1)} %get-tuple-element.65), channel_id=1, source_target_pairs={{0,8},{8,0},{16,24},{24,16},{1,9},{9,1},{17,25},{25,17},{2,10},{10... | collective-permute-start | bytes 1572872 | tf_op jit(solution)/shard_map/ppermute | solution.py:142
  9.2 2.0 %collective-permute-start.15 = (bf16[256,1024]{1,0:T(8,128)(2,1)}, bf16[256,1024]{1,0:T(8,128)(2,1)}, u32[]{:S(2)}, u32[]{:S(2)}) collective-permute-start(bf16[256,1024]{1,0:T(8,128)(2,1)} %get-tuple-element.69), channel_id=1, source_target_pairs={{0,16},{8,24},{16,0},{24,8},{1,17},{9,25},{17,1},{25,9},{2,18},{10... | collective-permute-start | bytes 1572872 | tf_op jit(solution)/shard_map/ppermute | solution.py:142
  13.8 2.1 %copy.11 = bf16[128,8,4,256]{3,1,2,0:T(8,128)(2,1)S(1)} copy(bf16[128,8,4,256]{3,2,1,0:T(4,128)(2,1)} %bitcast.29) | data formatting | bytes 4194304
  16.0 3.6 %collective-permute-done.refs_7_.refs_9_ = bf16[256,1024]{1,0:T(8,128)(2,1)} collective-permute-done((bf16[256,1024]{1,0:T(8,128)(2,1)}, bf16[256,1024]{1,0:T(8,128)(2,1)}, u32[]{:S(2)}, u32[]{:S(2)}) %collective-permute-start) | collective-permute-done | bytes 524320 | tf_op jit(solution)/shard_map/ppermute | solution.py:142
  19.7 2.1 %collective-permute-start.7 = (bf16[256,2048]{1,0:T(8,128)(2,1)}, bf16[256,2048]{1,0:T(8,128)(2,1)}, u32[]{:S(2)}, u32[]{:S(2)}) collective-permute-start(bf16[256,2048]{1,0:T(8,128)(2,1)} %refs_8_.1), channel_id=1, source_target_pairs={{0,2},{1,3},{2,4},{3,5},{4,6},{5,7},{6,0},{7,1},{8,10},{9,11},{10,... | collective-permute-start | bytes 3145736 | tf_op jit(solution)/shard_map/ppermute | solution.py:147
  21.8 2.0 %fusion.2 = (f32[1024,64]{1,0:T(8,128)S(1)}, f32[1024,64]{1,0:T(8,128)S(1)}, f32[1024,64]{1,0:T(8,128)S(1)}) fusion(f32[64]{0:T(128)S(1)} %multiply_power_fusion), kind=kLoop, calls=%fused_computation.10 | loop fusion | flops 131072 | bytes 786688 | tf_op jit(solution)/shard_map/neg | solution.py:724
  24.1 8.8 %collective-permute-done.1.refs_8_.refs_10_ = bf16[256,1024]{1,0:T(8,128)(2,1)} collective-permute-done((bf16[256,1024]{1,0:T(8,128)(2,1)}, bf16[256,1024]{1,0:T(8,128)(2,1)}, u32[]{:S(2)}, u32[]{:S(2)}) %collective-permute-start.1) | collective-permute-done | bytes 524320 | tf_op jit(solution)/shard_map/ppermute | solution.py:142
  33.0 2.1 %collective-permute-start.16 = (bf16[256,1024]{1,0:T(8,128)(2,1)}, bf16[256,1024]{1,0:T(8,128)(2,1)S(1)}, u32[]{:S(2)}, u32[]{:S(2)}) collective-permute-start(bf16[256,1024]{1,0:T(8,128)(2,1)} %get-tuple-element.68), channel_id=1, source_target_pairs={{0,16},{8,24},{16,0},{24,8},{1,17},{9,25},{17,1},{25,9},{2,18},{10... | collective-permute-start | bytes 1572872 | tf_op jit(solution)/shard_map/ppermute | solution.py:142
  35.0 9.2 %collective-permute-done.15.refs_4_.refs_7_ = bf16[256,1024]{1,0:T(8,128)(2,1)} collective-permute-done((bf16[256,1024]{1,0:T(8,128)(2,1)}, bf16[256,1024]{1,0:T(8,128)(2,1)}, u32[]{:S(2)}, u32[]{:S(2)}) %collective-permute-start.15) | collective-permute-done | bytes 524320 | tf_op jit(solution)/shard_map/ppermute | solution.py:142
  44.3 2.0 %collective-permute-start.18 = (bf16[256,1024]{1,0:T(8,128)(2,1)}, bf16[256,1024]{1,0:T(8,128)(2,1)S(1)}, u32[]{:S(2)}, u32[]{:S(2)}) collective-permute-start(bf16[256,1024]{1,0:T(8,128)(2,1)} %collective-permute-done.14.refs_3_.refs_6_), channel_id=1, source_target_pairs={{0,16},{8,24},{16,0},{24,8},{1,17},{9,25},{17,1},{25,9},{2,18},{10... | collective-permute-start | bytes 1572872 | tf_op jit(solution)/shard_map/ppermute | solution.py:142
  46.2 7.6 %retention_first.1 = (bf16[256,512]{1,0:T(8,128)(2,1)}, bf16[256,512]{1,0:T(8,128)(2,1)}, bf16[256,512]{1,0:T(8,128)(2,1)}, bf16[256,512]{1,0:T(8,128)(2,1)}, bf...) custom-call(s32[1]{0:T(128)} %bitcast.refs_0_.place, ...), custom_call_target="tpu_custom_call" | custom-call | flops 6000000000 | bytes 10000000 | tf_op jit(solution)/shard_map/retention_first/pallas_call | solution.py:298
  53.8 1.6 collective-permute-start.9
  59.5 3.2 %weight_start.1 = (f32[512,2048]{1,0:T(8,128)S(1)}, bf16[512,256]{1,0:T(8,128)(2,1)S(1)}) custom-call(bf16[512,256]{1,0:T(8,128)(2,1)S(1)} %copy-done.27, bf16[512,256]{1,0:T(8,128)(2,1)S(1)} %copy-done.28, bf16[512,256]{1,0:T(8,128)(2,1)S(1)} %copy-done.29, bf16[512,256]{1,0:T(8,128)(2,1)S(1)} %copy-done.30, bf16[256,2048]{1,0:T(8,128)(2,1)S(1)} %bitcast.26, ...), custom_call_target="tpu_custom_call" | custom-call | flops 4000000000 | bytes 6000000 | tf_op jit(solution)/shard_map/weight_start/pallas_call | solution.py:552
  65.7 12.2 %collective-permute-done.9.refs_9_.refs_12_ = bf16[256,2048]{1,0:T(8,128)(2,1)} collective-permute-done((bf16[256,2048]{1,0:T(8,128)(2,1)}, bf16[256,2048]{1,0:T(8,128)(2,1)}, u32[]{:S(2)}, u32[]{:S(2)}) %collective-permute-start.9) | collective-permute-done | bytes 1048608 | tf_op jit(solution)/shard_map/ppermute | solution.py:147
  83.2 1.5 collective-permute-start.26
  86.2 3.0 %collective-permute-done.21.refs_2_ = bf16[256,256]{1,0:T(8,128)(2,1)} collective-permute-done((bf16[256,256]{1,0:T(8,128)(2,1)}, bf16[256,256]{1,0:T(8,128)(2,1)}, u32[]{:S(2)}, u32[]{:S(2)}) %collective-permute-start.21) | collective-permute-done | bytes 131104 | tf_op jit(solution)/shard_map/ppermute | solution.py:142
  91.5 2.0 %collective-permute-start.23 = (bf16[256,256]{1,0:T(8,128)(2,1)S(1)}, bf16[256,256]{1,0:T(8,128)(2,1)S(1)}, u32[]{:S(2)}, u32[]{:S(2)}) collective-permute-start(bf16[256,256]{1,0:T(8,128)(2,1)S(1)} %get-tuple-element.53), channel_id=1, source_target_pairs={{0,2},{1,3},{2,0},{3,1},{4,6},{5,7},{6,4},{7,5},{8,10},{9,11},{10,... | collective-permute-start | bytes 393224 | tf_op jit(solution)/shard_map/ppermute | solution.py:142
  93.5 2.1 %collective-permute-start.24 = (bf16[256,256]{1,0:T(8,128)(2,1)S(1)}, bf16[256,256]{1,0:T(8,128)(2,1)S(1)}, u32[]{:S(2)}, u32[]{:S(2)}) collective-permute-start(bf16[256,256]{1,0:T(8,128)(2,1)S(1)} %get-tuple-element.54), channel_id=1, source_target_pairs={{0,4},{1,5},{2,6},{3,7},{4,0},{5,1},{6,2},{7,3},{8,12},{9,13},{10,... | collective-permute-start | bytes 393224 | tf_op jit(solution)/shard_map/ppermute | solution.py:142
  98.0 10.0 %collective-permute-done.23.refs_1_ = bf16[256,256]{1,0:T(8,128)(2,1)S(1)} collective-permute-done((bf16[256,256]{1,0:T(8,128)(2,1)S(1)}, bf16[256,256]{1,0:T(8,128)(2,1)S(1)}, u32[]{:S(2)}, u32[]{:S(2)}) %collective-permute-start.23) | collective-permute-done | bytes 131104 | tf_op jit(solution)/shard_map/ppermute | solution.py:142
  108.6 3.3 %collective-permute-start.31 = (bf16[256,256]{1,0:T(8,128)(2,1)S(1)}, bf16[256,256]{1,0:T(8,128)(2,1)S(1)}, u32[]{:S(2)}, u32[]{:S(2)}) collective-permute-start(bf16[256,256]{1,0:T(8,128)(2,1)S(1)} %get-tuple-element.63), channel_id=1, source_target_pairs={{0,6},{1,7},{2,4},{3,5},{4,2},{5,3},{6,0},{7,1},{8,14},{9,15},{10,... | collective-permute-start | bytes 393224 | tf_op jit(solution)/shard_map/ppermute | solution.py:142
  112.4 9.2 %collective-permute-done.30.refs_6_ = bf16[256,256]{1,0:T(8,128)(2,1)S(1)} collective-permute-done((bf16[256,256]{1,0:T(8,128)(2,1)S(1)}, bf16[256,256]{1,0:T(8,128)(2,1)S(1)}, u32[]{:S(2)}, u32[]{:S(2)}) %collective-permute-start.30) | collective-permute-done | bytes 131104 | tf_op jit(solution)/shard_map/ppermute | solution.py:142
  123.6 7.0 %collective-permute-done.32.refs_1_ = bf16[256,512]{1,0:T(8,128)(2,1)S(1)} collective-permute-done((bf16[256,512]{1,0:T(8,128)(2,1)S(1)}, bf16[256,512]{1,0:T(8,128)(2,1)S(1)}, u32[]{:S(2)}, u32[]{:S(2)}) %collective-permute-start.32) | collective-permute-done | bytes 262176 | tf_op jit(solution)/shard_map/ppermute | solution.py:142
  132.3 6.4 %collective-permute-done.33.refs_2_ = bf16[256,512]{1,0:T(8,128)(2,1)S(1)} collective-permute-done((bf16[256,512]{1,0:T(8,128)(2,1)S(1)}, bf16[256,512]{1,0:T(8,128)(2,1)S(1)}, u32[]{:S(2)}, u32[]{:S(2)}) %collective-permute-start.33) | collective-permute-done | bytes 262176 | tf_op jit(solution)/shard_map/ppermute | solution.py:142
  139.4 1.6 collective-permute-start.34
  141.9 5.0 %collective-permute-done.34.refs_3_ = bf16[256,512]{1,0:T(8,128)(2,1)} collective-permute-done((bf16[256,512]{1,0:T(8,128)(2,1)S(1)}, bf16[256,512]{1,0:T(8,128)(2,1)}, u32[]{:S(2)}, u32[]{:S(2)}) %collective-permute-start.34) | collective-permute-done | bytes 262176 | tf_op jit(solution)/shard_map/ppermute | solution.py:142
  151.0 2.3 %lay_out.1 = f32[256,2048]{1,0:T(8,128)} custom-call(s32[1]{0:T(128)} %bitcast.refs_0_.place, bf16[256,512]{1,0:T(8,128)(2,1)S(1)} %copy-done.17, bf16[256,512]{1,0:T(8,128)(2,1)S(1)} %copy-done.19, bf16[256,512]{1,0:T(8,128)(2,1)S(1)} %copy-done.21, bf16[256,512]{1,0:T(8,128)(2,1)} %collective-permute-done.34.refs_3_), custom_call_target="tpu_custom_call" | custom-call | flops 1000000000 | bytes 4000000 | tf_op jit(solution)/shard_map/lay_out/pallas_call | solution.py:685
  155.8 4.5 %key_projection.1.refs_7_ = bf16[1024,512]{1,0:T(8,128)(2,1)S(1)} custom-call(s32[2]{0:T(128)S(1)} %pad_add_fusion.1.refs_0_, bf16[256,2048]{1,0:T(8,128)(2,1)S(1)} %bitcast.27, bf16[256,1024]{1,0:T(8,128)(2,1)S(1)} %copy-done.13, bf16[256,1024]{1,0:T(8,128)(2,1)} %collective-permute-done.14.refs_3_.refs_6_, ...), custom_call_target="tpu_custom_call" | custom-call | flops 4000000000 | bytes 8000000 | tf_op jit(solution)/shard_map/key_projection/pallas_call | solution.py:424
  160.3 8.5 %retention_second.1 = (bf16[1024,512]{1,0:T(8,128)(2,1)}, bf16[1024,1024]{1,0:T(8,128)(2,1)}) custom-call(s32[1]{0:T(128)} %bitcast.refs_0_.place, f32[4]{0:T(128)S(1)} %dynamic_slice.23.refs_1_, bf16[1024,512]{1,0:T(8,128)(2,1)S(1)} %copy-done.24, bf16[1024,1024]{1,0:T(8,128)(2,1)S(1)} %bitcast.24, f32[1024,128]{1,0:T(8,128)S(1)} %copy-done.3, ...), custom_call_target="tpu_custom_call" | custom-call | flops 6000000000 | bytes 14000000 | tf_op jit(solution)/shard_map/retention_second/pallas_call | solution.py:332
  168.8 2.3 %reshape.24 = bf16[1,1024,4,128]{3,2,1,0:T(4,128)(2,1)} reshape(bf16[1024,512]{1,0:T(8,128)(2,1)} %get-tuple-element.40) | data formatting | bytes 2097152 | tf_op jit(solution)/shard_map/reshape | solution.py:763
  171.1 2.7 %reshape.25 = bf16[1,1024,4,256]{3,2,1,0:T(4,128)(2,1)} reshape(bf16[1024,1024]{1,0:T(8,128)(2,1)S(1)} %copy-done.31) | data formatting | bytes 4194304 | tf_op jit(solution)/shard_map/reshape | solution.py:764
  173.8 6.0 %token_gradient.1 = bf16[256,2048]{1,0:T(8,128)(2,1)} custom-call(s32[3]{0:T(128)S(1)} %pad_add_fusion.refs_0_, bf16[256,512]{1,0:T(8,128)(2,1)S(1)} %copy-done.26, bf16[256,512]{1,0:T(8,128)(2,1)S(1)} %collective-permute-done.3.refs_2_, bf16[256,512]{1,0:T(8,128)(2,1)} %collective-permute-done.4.refs_3_, bf16[256,512]{1,0:T(8,128)(2,1)} %collective-permute-done.5.refs_4_, ...), custom_call_target="tpu_custom_call" | custom-call | flops 5000000000 | bytes 11000000 | tf_op jit(solution)/shard_map/token_gradient/pallas_call | solution.py:487
  (131 shorter events, 36.9 us)
Async XLA Ops:
  3.6 16.1 %collective-permute-start = (bf16[256,1024]{1,0:T(8,128)(2,1)}, bf16[256,1024]{1,0:T(8,128)(2,1)}, u32[]{:S(2)}, u32[]{:S(2)}) collective-permute-start(bf16[256,1024]{1,0:T(8,128)(2,1)} %get-tuple-element.65), channel_id=1, source_target_pairs={{0,8},{8,0},{16,24},{24,16},{1,9},{9,1},{17,25},{25,17},{2,10},{10... | collective-permute-start | bytes 1572872 | tf_op jit(solution)/shard_map/ppermute | solution.py:142
  6.6 26.3 %collective-permute-start.1 = (bf16[256,1024]{1,0:T(8,128)(2,1)}, bf16[256,1024]{1,0:T(8,128)(2,1)}, u32[]{:S(2)}, u32[]{:S(2)}) collective-permute-start(bf16[256,1024]{1,0:T(8,128)(2,1)} %get-tuple-element.67), channel_id=1, source_target_pairs={{0,16},{8,24},{16,0},{24,8},{1,17},{9,25},{17,1},{25,9},{2,18},{10... | collective-permute-start | bytes 1572872 | tf_op jit(solution)/shard_map/ppermute | solution.py:142
  8.1 24.8 %collective-permute-start.2 = (bf16[256,1024]{1,0:T(8,128)(2,1)}, bf16[256,1024]{1,0:T(8,128)(2,1)}, u32[]{:S(2)}, u32[]{:S(2)}) collective-permute-start(bf16[256,1024]{1,0:T(8,128)(2,1)} %get-tuple-element.64), channel_id=1, source_target_pairs={{0,24},{8,16},{16,8},{24,0},{1,25},{9,17},{17,9},{25,1},{2,26},{10... | collective-permute-start | bytes 1572872 | tf_op jit(solution)/shard_map/ppermute | solution.py:142
  9.2 35.0 %collective-permute-start.15 = (bf16[256,1024]{1,0:T(8,128)(2,1)}, bf16[256,1024]{1,0:T(8,128)(2,1)}, u32[]{:S(2)}, u32[]{:S(2)}) collective-permute-start(bf16[256,1024]{1,0:T(8,128)(2,1)} %get-tuple-element.69), channel_id=1, source_target_pairs={{0,16},{8,24},{16,0},{24,8},{1,17},{9,25},{17,1},{25,9},{2,18},{10... | collective-permute-start | bytes 1572872 | tf_op jit(solution)/shard_map/ppermute | solution.py:142
  11.2 33.1 %collective-permute-start.14 = (bf16[256,1024]{1,0:T(8,128)(2,1)}, bf16[256,1024]{1,0:T(8,128)(2,1)}, u32[]{:S(2)}, u32[]{:S(2)}) collective-permute-start(bf16[256,1024]{1,0:T(8,128)(2,1)} %get-tuple-element.68), channel_id=1, source_target_pairs={{0,8},{8,0},{16,24},{24,16},{1,9},{9,1},{17,25},{25,17},{2,10},{10... | collective-permute-start | bytes 1572872 | tf_op jit(solution)/shard_map/ppermute | solution.py:142
  19.7 34.1 %collective-permute-start.7 = (bf16[256,2048]{1,0:T(8,128)(2,1)}, bf16[256,2048]{1,0:T(8,128)(2,1)}, u32[]{:S(2)}, u32[]{:S(2)}) collective-permute-start(bf16[256,2048]{1,0:T(8,128)(2,1)} %refs_8_.1), channel_id=1, source_target_pairs={{0,2},{1,3},{2,4},{3,5},{4,6},{5,7},{6,0},{7,1},{8,10},{9,11},{10,... | collective-permute-start | bytes 3145736 | tf_op jit(solution)/shard_map/ppermute | solution.py:147
  32.9 22.5 %collective-permute-start.13 = (bf16[256,1024]{1,0:T(8,128)(2,1)}, bf16[256,1024]{1,0:T(8,128)(2,1)S(1)}, u32[]{:S(2)}, u32[]{:S(2)}) collective-permute-start(bf16[256,1024]{1,0:T(8,128)(2,1)} %get-tuple-element.69), channel_id=1, source_target_pairs={{0,8},{8,0},{16,24},{24,16},{1,9},{9,1},{17,25},{25,17},{2,10},{10... | collective-permute-start | bytes 1572872 | tf_op jit(solution)/shard_map/ppermute | solution.py:142
  33.0 22.5 %collective-permute-start.16 = (bf16[256,1024]{1,0:T(8,128)(2,1)}, bf16[256,1024]{1,0:T(8,128)(2,1)S(1)}, u32[]{:S(2)}, u32[]{:S(2)}) collective-permute-start(bf16[256,1024]{1,0:T(8,128)(2,1)} %get-tuple-element.68), channel_id=1, source_target_pairs={{0,16},{8,24},{16,0},{24,8},{1,17},{9,25},{17,1},{25,9},{2,18},{10... | collective-permute-start | bytes 1572872 | tf_op jit(solution)/shard_map/ppermute | solution.py:142
  44.2 19.5 %collective-permute-start.17 = (bf16[256,1024]{1,0:T(8,128)(2,1)}, bf16[256,1024]{1,0:T(8,128)(2,1)S(1)}, u32[]{:S(2)}, u32[]{:S(2)}) collective-permute-start(bf16[256,1024]{1,0:T(8,128)(2,1)} %collective-permute-done.15.refs_4_.refs_7_), channel_id=1, source_target_pairs={{0,8},{8,0},{16,24},{24,16},{1,9},{9,1},{17,25},{25,17},{2,10},{10... | collective-permute-start | bytes 1572872 | tf_op jit(solution)/shard_map/ppermute | solution.py:142
  44.3 20.9 %collective-permute-start.18 = (bf16[256,1024]{1,0:T(8,128)(2,1)}, bf16[256,1024]{1,0:T(8,128)(2,1)S(1)}, u32[]{:S(2)}, u32[]{:S(2)}) collective-permute-start(bf16[256,1024]{1,0:T(8,128)(2,1)} %collective-permute-done.14.refs_3_.refs_6_), channel_id=1, source_target_pairs={{0,16},{8,24},{16,0},{24,8},{1,17},{9,25},{17,1},{25,9},{2,18},{10... | collective-permute-start | bytes 1572872 | tf_op jit(solution)/shard_map/ppermute | solution.py:142
  53.8 24.0 %collective-permute-start.9 = (bf16[256,2048]{1,0:T(8,128)(2,1)}, bf16[256,2048]{1,0:T(8,128)(2,1)}, u32[]{:S(2)}, u32[]{:S(2)}) collective-permute-start(bf16[256,2048]{1,0:T(8,128)(2,1)} %collective-permute-done.7.refs_7_.refs_10_), channel_id=1, source_target_pairs={{0,2},{1,3},{2,4},{3,5},{4,6},{5,7},{6,0},{7,1},{8,10},{9,11},{10,... | collective-permute-start | bytes 3145736 | tf_op jit(solution)/shard_map/ppermute | solution.py:147
  65.6 13.0 %collective-permute-start.19 = (bf16[256,2048]{1,0:T(8,128)(2,1)S(1)}, bf16[256,2048]{1,0:T(8,128)(2,1)S(1)}, u32[]{:S(2)}, u32[]{:S(2)}) collective-permute-start(bf16[256,2048]{1,0:T(8,128)(2,1)S(1)} %weight_end.3), channel_id=1, source_target_pairs={{0,1},{1,0},{2,3},{3,2},{4,5},{5,4},{6,7},{7,6},{8,9},{9,8},{10,11... | collective-permute-start | bytes 3145736 | tf_op jit(solution)/shard_map/ppermute | solution.py:142
  77.9 43.8 %collective-permute-start.11 = (bf16[256,2048]{1,0:T(8,128)(2,1)}, bf16[256,2048]{1,0:T(8,128)(2,1)}, u32[]{:S(2)}, u32[]{:S(2)}) collective-permute-start(bf16[256,2048]{1,0:T(8,128)(2,1)} %collective-permute-done.9.refs_9_.refs_12_), channel_id=1, source_target_pairs={{0,2},{1,3},{2,4},{3,5},{4,6},{5,7},{6,0},{7,1},{8,10},{9,11},{10,... | collective-permute-start | bytes 3145736 | tf_op jit(solution)/shard_map/ppermute | solution.py:147
  81.1 8.1 %collective-permute-start.21 = (bf16[256,256]{1,0:T(8,128)(2,1)}, bf16[256,256]{1,0:T(8,128)(2,1)}, u32[]{:S(2)}, u32[]{:S(2)}) collective-permute-start(bf16[256,256]{1,0:T(8,128)(2,1)} %get-tuple-element.50), channel_id=1, source_target_pairs={{0,16},{8,24},{16,0},{24,8},{1,17},{9,25},{17,1},{25,9},{2,18},{10... | collective-permute-start | bytes 393224 | tf_op jit(solution)/shard_map/ppermute | solution.py:142
  81.6 7.7 %collective-permute-start.22 = (bf16[256,256]{1,0:T(8,128)(2,1)}, bf16[256,256]{1,0:T(8,128)(2,1)}, u32[]{:S(2)}, u32[]{:S(2)}) collective-permute-start(bf16[256,256]{1,0:T(8,128)(2,1)} %get-tuple-element.51), channel_id=1, source_target_pairs={{0,24},{8,16},{16,8},{24,0},{1,25},{9,17},{17,9},{25,1},{2,26},{10... | collective-permute-start | bytes 393224 | tf_op jit(solution)/shard_map/ppermute | solution.py:142
  83.2 10.3 %collective-permute-start.26 = (bf16[256,256]{1,0:T(8,128)(2,1)S(1)}, bf16[256,256]{1,0:T(8,128)(2,1)S(1)}, u32[]{:S(2)}, u32[]{:S(2)}) collective-permute-start(bf16[256,256]{1,0:T(8,128)(2,1)S(1)} %get-tuple-element.57), channel_id=1, source_target_pairs={{0,8},{8,0},{16,24},{24,16},{1,9},{9,1},{17,25},{25,17},{2,10},{10... | collective-permute-start | bytes 393224 | tf_op jit(solution)/shard_map/ppermute | solution.py:142
  86.2 9.4 %collective-permute-start.27 = (bf16[256,256]{1,0:T(8,128)(2,1)S(1)}, bf16[256,256]{1,0:T(8,128)(2,1)S(1)}, u32[]{:S(2)}, u32[]{:S(2)}) collective-permute-start(bf16[256,256]{1,0:T(8,128)(2,1)S(1)} %get-tuple-element.58), channel_id=1, source_target_pairs={{0,16},{8,24},{16,0},{24,8},{1,17},{9,25},{17,1},{25,9},{2,18},{10... | collective-permute-start | bytes 393224 | tf_op jit(solution)/shard_map/ppermute | solution.py:142
  91.5 16.5 %collective-permute-start.23 = (bf16[256,256]{1,0:T(8,128)(2,1)S(1)}, bf16[256,256]{1,0:T(8,128)(2,1)S(1)}, u32[]{:S(2)}, u32[]{:S(2)}) collective-permute-start(bf16[256,256]{1,0:T(8,128)(2,1)S(1)} %get-tuple-element.53), channel_id=1, source_target_pairs={{0,2},{1,3},{2,0},{3,1},{4,6},{5,7},{6,4},{7,5},{8,10},{9,11},{10,... | collective-permute-start | bytes 393224 | tf_op jit(solution)/shard_map/ppermute | solution.py:142
  93.5 15.1 %collective-permute-start.24 = (bf16[256,256]{1,0:T(8,128)(2,1)S(1)}, bf16[256,256]{1,0:T(8,128)(2,1)S(1)}, u32[]{:S(2)}, u32[]{:S(2)}) collective-permute-start(bf16[256,256]{1,0:T(8,128)(2,1)S(1)} %get-tuple-element.54), channel_id=1, source_target_pairs={{0,4},{1,5},{2,6},{3,7},{4,0},{5,1},{6,2},{7,3},{8,12},{9,13},{10,... | collective-permute-start | bytes 393224 | tf_op jit(solution)/shard_map/ppermute | solution.py:142
  95.6 16.3 %collective-permute-start.25 = (bf16[256,256]{1,0:T(8,128)(2,1)S(1)}, bf16[256,256]{1,0:T(8,128)(2,1)S(1)}, u32[]{:S(2)}, u32[]{:S(2)}) collective-permute-start(bf16[256,256]{1,0:T(8,128)(2,1)S(1)} %get-tuple-element.55), channel_id=1, source_target_pairs={{0,6},{1,7},{2,4},{3,5},{4,2},{5,3},{6,0},{7,1},{8,14},{9,15},{10,... | collective-permute-start | bytes 393224 | tf_op jit(solution)/shard_map/ppermute | solution.py:142
  96.8 15.3 %collective-permute-start.29 = (bf16[256,256]{1,0:T(8,128)(2,1)S(1)}, bf16[256,256]{1,0:T(8,128)(2,1)S(1)}, u32[]{:S(2)}, u32[]{:S(2)}) collective-permute-start(bf16[256,256]{1,0:T(8,128)(2,1)S(1)} %get-tuple-element.61), channel_id=1, source_target_pairs={{0,2},{1,3},{2,0},{3,1},{4,6},{5,7},{6,4},{7,5},{8,10},{9,11},{10,... | collective-permute-start | bytes 393224 | tf_op jit(solution)/shard_map/ppermute | solution.py:142
  108.0 13.6 %collective-permute-start.30 = (bf16[256,256]{1,0:T(8,128)(2,1)S(1)}, bf16[256,256]{1,0:T(8,128)(2,1)S(1)}, u32[]{:S(2)}, u32[]{:S(2)}) collective-permute-start(bf16[256,256]{1,0:T(8,128)(2,1)S(1)} %get-tuple-element.62), channel_id=1, source_target_pairs={{0,4},{1,5},{2,6},{3,7},{4,0},{5,1},{6,2},{7,3},{8,12},{9,13},{10,... | collective-permute-start | bytes 393224 | tf_op jit(solution)/shard_map/ppermute | solution.py:142
  108.6 13.6 %collective-permute-start.31 = (bf16[256,256]{1,0:T(8,128)(2,1)S(1)}, bf16[256,256]{1,0:T(8,128)(2,1)S(1)}, u32[]{:S(2)}, u32[]{:S(2)}) collective-permute-start(bf16[256,256]{1,0:T(8,128)(2,1)S(1)} %get-tuple-element.63), channel_id=1, source_target_pairs={{0,6},{1,7},{2,4},{3,5},{4,2},{5,3},{6,0},{7,1},{8,14},{9,15},{10,... | collective-permute-start | bytes 393224 | tf_op jit(solution)/shard_map/ppermute | solution.py:142
  111.9 41.4 %collective-permute-start.6 = (bf16[256,2048]{1,0:T(8,128)(2,1)}, bf16[256,2048]{1,0:T(8,128)(2,1)}, u32[]{:S(2)}, u32[]{:S(2)}) collective-permute-start(bf16[256,2048]{1,0:T(8,128)(2,1)} %refs_8_.1), channel_id=1, source_target_pairs={{0,1},{1,0},{2,3},{3,2},{4,5},{5,4},{6,7},{7,6},{8,9},{9,8},{10,11... | collective-permute-start | bytes 3145736 | tf_op jit(solution)/shard_map/ppermute | solution.py:142
  112.1 42.2 %collective-permute-start.8 = (bf16[256,2048]{1,0:T(8,128)(2,1)}, bf16[256,2048]{1,0:T(8,128)(2,1)}, u32[]{:S(2)}, u32[]{:S(2)}) collective-permute-start(bf16[256,2048]{1,0:T(8,128)(2,1)} %collective-permute-done.7.refs_7_.refs_10_), channel_id=1, source_target_pairs={{0,1},{1,0},{2,3},{3,2},{4,5},{5,4},{6,7},{7,6},{8,9},{9,8},{10,11... | collective-permute-start | bytes 3145736 | tf_op jit(solution)/shard_map/ppermute | solution.py:142
  121.6 34.1 %collective-permute-start.10 = (bf16[256,2048]{1,0:T(8,128)(2,1)}, bf16[256,2048]{1,0:T(8,128)(2,1)}, u32[]{:S(2)}, u32[]{:S(2)}) collective-permute-start(bf16[256,2048]{1,0:T(8,128)(2,1)} %collective-permute-done.9.refs_9_.refs_12_), channel_id=1, source_target_pairs={{0,1},{1,0},{2,3},{3,2},{4,5},{5,4},{6,7},{7,6},{8,9},{9,8},{10,11... | collective-permute-start | bytes 3145736 | tf_op jit(solution)/shard_map/ppermute | solution.py:142
  121.6 34.1 %collective-permute-start.12 = (bf16[256,2048]{1,0:T(8,128)(2,1)}, bf16[256,2048]{1,0:T(8,128)(2,1)}, u32[]{:S(2)}, u32[]{:S(2)}) collective-permute-start(bf16[256,2048]{1,0:T(8,128)(2,1)} %collective-permute-done.11.refs_11_.refs_14_), channel_id=1, source_target_pairs={{0,1},{1,0},{2,3},{3,2},{4,5},{5,4},{6,7},{7,6},{8,9},{9,8},{10,11... | collective-permute-start | bytes 3145736 | tf_op jit(solution)/shard_map/ppermute | solution.py:142
  122.3 8.3 %collective-permute-start.32 = (bf16[256,512]{1,0:T(8,128)(2,1)S(1)}, bf16[256,512]{1,0:T(8,128)(2,1)S(1)}, u32[]{:S(2)}, u32[]{:S(2)}) collective-permute-start(bf16[256,512]{1,0:T(8,128)(2,1)S(1)} %add_up.1.refs_0_), channel_id=1, source_target_pairs={{0,8},{8,0},{16,24},{24,16},{1,9},{9,1},{17,25},{25,17},{2,10},{10... | collective-permute-start | bytes 786440 | tf_op jit(solution)/shard_map/ppermute | solution.py:142
  139.4 7.5 %collective-permute-start.34 = (bf16[256,512]{1,0:T(8,128)(2,1)S(1)}, bf16[256,512]{1,0:T(8,128)(2,1)}, u32[]{:S(2)}, u32[]{:S(2)}) collective-permute-start(bf16[256,512]{1,0:T(8,128)(2,1)S(1)} %add_up.1.refs_0_), channel_id=1, source_target_pairs={{0,24},{8,16},{16,8},{24,0},{1,25},{9,17},{17,9},{25,1},{2,26},{10... | collective-permute-start | bytes 786440 | tf_op jit(solution)/shard_map/ppermute | solution.py:142
  146.9 26.9 %collective-permute-start.3 = (bf16[256,512]{1,0:T(8,128)(2,1)}, bf16[256,512]{1,0:T(8,128)(2,1)S(1)}, u32[]{:S(2)}, u32[]{:S(2)}) collective-permute-start(bf16[256,512]{1,0:T(8,128)(2,1)} %get-tuple-element.35), channel_id=1, source_target_pairs={{0,8},{8,0},{16,24},{24,16},{1,9},{9,1},{17,25},{25,17},{2,10},{10... | collective-permute-start | bytes 786440 | tf_op jit(solution)/shard_map/ppermute | solution.py:142
  153.3 20.5 %collective-permute-start.4 = (bf16[256,512]{1,0:T(8,128)(2,1)}, bf16[256,512]{1,0:T(8,128)(2,1)}, u32[]{:S(2)}, u32[]{:S(2)}) collective-permute-start(bf16[256,512]{1,0:T(8,128)(2,1)} %get-tuple-element.36), channel_id=1, source_target_pairs={{0,16},{8,24},{16,0},{24,8},{1,17},{9,25},{17,1},{25,9},{2,18},{10... | collective-permute-start | bytes 786440 | tf_op jit(solution)/shard_map/ppermute | solution.py:142
  154.4 19.4 %collective-permute-start.5 = (bf16[256,512]{1,0:T(8,128)(2,1)}, bf16[256,512]{1,0:T(8,128)(2,1)}, u32[]{:S(2)}, u32[]{:S(2)}) collective-permute-start(bf16[256,512]{1,0:T(8,128)(2,1)} %get-tuple-element.37), channel_id=1, source_target_pairs={{0,24},{8,16},{16,8},{24,0},{1,25},{9,17},{17,9},{25,1},{2,26},{10... | collective-permute-start | bytes 786440 | tf_op jit(solution)/shard_map/ppermute | solution.py:142
  (37 other events, 303.5 us)

commit v2 on v1

--- a/solution.py
+++ b/solution.py
@@ -290,7 +290,7 @@
     full = spec((seq_len, key_width), lambda h: (0, 0))
     head = spec((seq_len, key_width), lambda h: (0, h))
     outs = [pltpu.HBM((rows, query_width), half)] * slots
-    outs += [pltpu.HBM((query_width, rows), half)] * slots
+    outs += [pltpu.VMEM((query_width, rows), half)] * slots
     outs += [
         pltpu.HBM((seq_len, query_width), half),
         pltpu.HBM((heads, nblocks, key_width, value_width), half),
@@ -518,8 +518,8 @@
     half = width // 2
 
     def kernel(*refs):
-        grad_refs, token_refs = refs[: slots + 1], refs[slots + 1 : slots + 1 + len(parts)]
-        out, last, grad, token, sems, grad_sems = refs[slots + 1 + len(parts) :]
+        grad_refs, token_refs = refs[:slots], refs[slots : slots + len(parts)]
+        out, token, sems = refs[slots + len(parts) :]
 
         def fetch(at, k, index, piece):
             return pltpu.make_async_copy(
@@ -528,40 +528,25 @@
                 sems.at[at, k],
             )
 
-        def fetch_grad(k):
-            to = grad.at[k] if k < slots else last
-            return pltpu.make_async_copy(grad_refs[k], to, grad_sems.at[k])
-
-        for k in range(slots):
-            fetch_grad(k).start()
         for at in range(2):
             for load in loads[at]:
                 fetch(at, *load).start()
-        fetch_grad(slots).start()
-        for k in range(slots):
-            fetch_grad(k).wait()
         for at in range(2):
             for load in loads[at]:
                 fetch(at, *load).wait()
-            total = dot(grad[0], token[at, 0], 1, 0)
+            total = dot(grad_refs[0][...], token[at, 0], 1, 0)
             for k in range(1, slots):
-                total += dot(grad[k], token[at, k], 1, 0)
+                total += dot(grad_refs[k][...], token[at, k], 1, 0)
             out[:, at * half : (at + 1) * half] = total
-        fetch_grad(slots).wait()
 
     return pl.pallas_call(
         kernel,
-        in_specs=away(slots + 1 + len(parts)),
-        out_specs=near(2),
-        out_shape=[
-            pltpu.VMEM((features, width), jnp.float32),
-            pltpu.VMEM((features, rows), jnp.bfloat16),
-        ],
+        in_specs=near(slots) + away(len(parts)),
+        out_specs=near()[0],
+        out_shape=pltpu.VMEM((features, width), jnp.float32),
         scratch_shapes=[
-            pltpu.VMEM((slots, features, rows), jnp.bfloat16),
             pltpu.VMEM((2, slots, rows, half), jnp.bfloat16),
             pltpu.SemaphoreType.DMA((2, slots)),
-            pltpu.SemaphoreType.DMA((slots + 1,)),
         ],
         compiler_params=limit(20),
         cost_estimate=cost(4e9, 6e6),
@@ -699,11 +684,9 @@
 
 def gather_slots(array):
     half = array.shape[1] // 2
-    low, high = array[:, :half], array[:, half:]
-    near_high, next_low = swap(high, "sp", 1), swap(low, "sp", 2)
-    near_low, next_high = swap(low, "sp", 1), swap(high, "sp", 2)
-    far = [swap(next_low, "sp", 1), swap(near_high, "sp", 2)]
-    return [[array], [near_low, near_high], [next_low, next_high], far]
+    near_one, next_one = swap(array, "sp", 1), swap(array, "sp", 2)
+    far = [swap(next_one[:, :half], "sp", 1), swap(near_one[:, half:], "sp", 2)]
+    return [[array], [near_one], [next_one], far]
 
 
 def direct_body(tokens, key_weight, queries, values, cotangent, log_decay):
@@ -738,10 +721,10 @@
         here, rate, query, value, cosine, sine, cotans, key_width
     )
 
-    total, last = weight_start(turned_grads, token_slots[:-1])
-    sent = weight_end(core ^ 1, last, token_slots[-1], total, jnp.bfloat16)
+    total = weight_start(turned_grads[:-1], token_slots[:-1])
+    sent = weight_end(core ^ 1, turned_grads[-1], token_slots[-1], total, jnp.bfloat16)
     received = swap(sent, "dp", 1)
-    kept = weight_end(core, last, token_slots[-1], total, jnp.float32)
+    kept = weight_end(core, turned_grads[-1], token_slots[-1], total, jnp.float32)
     chunks = weight_pieces(here, slots, CHUNKS, kept, received)
     groups = []
     for pieces in chunks:

time: 181 us -> 188 us (1.039)
  waiting for transfers between devices: 78.6 us -> 89 us
  local copies, waits for them, and re-layouts: 22.4 us -> 18.8 us
    ppermute x3, waiting for transfers between devices: 12.2 us -> 19.2 us  [step_planes(): lax.ppermute(array, 'dp', [(i, (i + 2) % count) for i in range(count)])]
    unnamed x70 -> x54, local copies, waits for them, and re-layouts: 13.2 us -> 8.23 us
    ppermute x32 -> x30, waiting for transfers between devices: 66.4 us -> 69.8 us  [swap(): return lax.ppermute(array, axis, [(i, i ^ bit) for i in range(count)])]
    ppermute x32 -> x30, starting transfers between devices: 35.2 us -> 35.7 us  [swap(): return lax.ppermute(array, axis, [(i, i ^ bit) for i in range(count)])]
  transfers between devices with their start and end apart: 35 -> 33, of which waited for: 14 -> 12; matrix products, arithmetic and copies ran while one was open for 7% -> 8% of each run, Pallas kernels for 17% -> 16%
where the time goes in v2:
time: 188 us; the launch traced here: 187 us
  waiting for transfers between devices  89 us (47%)
  starting transfers between devices  39.8 us (21%)
  Pallas kernels  35.7 us (19%)
  local copies, waits for them, and re-layouts  18.8 us (10%)
  other arithmetic  2.54 us (1%)
    ppermute x30, waiting for transfers between devices, swap(): return lax.ppermute(array, axis, [(i, i ^ bit) for i in range(count)])  69.8 us
    ppermute x30, starting transfers between devices, swap(): return lax.ppermute(array, axis, [(i, i ^ bit) for i in range(count)])  35.7 us
    ppermute x3, waiting for transfers between devices, step_planes(): lax.ppermute(array, 'dp', [(i, (i + 2) % count) for i in range(count)])  19.2 us
    pallas_call x1, Pallas kernels, retention_second(): pl.pallas_call(second_kernel(slots, rows, inner, key_width ** (-0.5)), gr...  8.46 us
    unnamed x54, local copies, waits for them, and re-layouts  8.23 us
    pallas_call x1, Pallas kernels, retention_first(): pl.pallas_call(first_kernel(slots, rows, inner, key_width ** (-0.5)), gri...  7.52 us
    pallas_call x1, Pallas kernels, token_gradient(): pl.pallas_call(kernel, in_specs=[smem()] + away(slots + 2 * planes), out_...  5.97 us
    pallas_call x1, Pallas kernels, key_projection(): pl.pallas_call(kernel, in_specs=[smem()] + away(len(parts) - far) + near(...  4.64 us
  transfers between devices with their start and end apart: 33, of which 12 were waited for; matrix products, arithmetic and copies ran while one was open for 8% of the time, Pallas kernels for 16%

profile of v2, /device:TPU:0, one launch (start us, length us, event | category | flops | bytes accessed | tf_op | source)
XLA Modules:
  0.0 187.1 jit_solution(4764972638613882797)
XLA Ops:
  0.6 3.1 %collective-permute-start.14 = (bf16[256,2048]{1,0:T(8,128)(2,1)}, bf16[256,2048]{1,0:T(8,128)(2,1)}, u32[]{:S(2)}, u32[]{:S(2)}) collective-permute-start(bf16[256,2048]{1,0:T(8,128)(2,1)} %bitcast.26), channel_id=1, source_target_pairs={{0,16},{8,24},{16,0},{24,8},{1,17},{9,25},{17,1},{25,9},{2,18},{10... | collective-permute-start | bytes 3145736 | tf_op jit(solution)/shard_map/ppermute | solution.py:142
  5.2 3.0 %dynamic-slice_bitcast_fusion = (bf16[256,1024]{1,0:T(8,128)(2,1)}, bf16[256,1024]{1,0:T(8,128)(2,1)}, bf16[256,1024]{1,0:T(8,128)(2,1)}, bf16[256,1024]{1,0:T(8,128)(2,1)}) fusion(bf16[1,256,4096]{2,1,0:T(8,128)(2,1)} %param.10, s32[]{:T(128)S(6)} %select_n.36, s32[]{:T(128)S(6)} %select_n.34, s32[]{:T(128)S(6)} %select_n.33, s32[]{:T(128)S(6)} %select_n.35), kind=kLoop, calls=%fused_computation.3 | loop fusion | bytes 4194320 | tf_op jit(solution)/shard_map/dynamic_slice | solution.py:161
  8.8 2.9 %collective-permute-start.2 = (bf16[256,1024]{1,0:T(8,128)(2,1)}, bf16[256,1024]{1,0:T(8,128)(2,1)}, u32[]{:S(2)}, u32[]{:S(2)}) collective-permute-start(bf16[256,1024]{1,0:T(8,128)(2,1)} %get-tuple-element.60), channel_id=1, source_target_pairs={{0,24},{8,16},{16,8},{24,0},{1,25},{9,17},{17,9},{25,1},{2,26},{10... | collective-permute-start | bytes 1572872 | tf_op jit(solution)/shard_map/ppermute | solution.py:142
  11.8 2.1 %copy.11 = bf16[128,8,4,256]{3,1,2,0:T(8,128)(2,1)S(1)} copy(bf16[128,8,4,256]{3,2,1,0:T(4,128)(2,1)} %bitcast.30) | data formatting | bytes 4194304
  14.0 14.0 %collective-permute-done.14.refs_3_.refs_5_ = bf16[256,2048]{1,0:T(8,128)(2,1)} collective-permute-done((bf16[256,2048]{1,0:T(8,128)(2,1)}, bf16[256,2048]{1,0:T(8,128)(2,1)}, u32[]{:S(2)}, u32[]{:S(2)}) %collective-permute-start.14) | collective-permute-done | bytes 1048608 | tf_op jit(solution)/shard_map/ppermute | solution.py:142
  28.0 2.1 %collective-permute-start.7 = (bf16[256,2048]{1,0:T(8,128)(2,1)}, bf16[256,2048]{1,0:T(8,128)(2,1)}, u32[]{:S(2)}, u32[]{:S(2)}) collective-permute-start(bf16[256,2048]{1,0:T(8,128)(2,1)} %refs_6_.1), channel_id=1, source_target_pairs={{0,2},{1,3},{2,4},{3,5},{4,6},{5,7},{6,0},{7,1},{8,10},{9,11},{10,... | collective-permute-start | bytes 3145736 | tf_op jit(solution)/shard_map/ppermute | solution.py:147
  30.1 2.0 %fusion.2 = (f32[1024,64]{1,0:T(8,128)S(1)}, f32[1024,64]{1,0:T(8,128)S(1)}, f32[1024,64]{1,0:T(8,128)S(1)}) fusion(f32[64]{0:T(128)S(1)} %multiply_power_fusion), kind=kLoop, calls=%fused_computation.10 | loop fusion | flops 131072 | bytes 786688 | tf_op jit(solution)/shard_map/neg | solution.py:707
  33.9 1.6 collective-permute-start.15
  36.6 4.7 %collective-permute-done.refs_7_.refs_9_ = bf16[256,1024]{1,0:T(8,128)(2,1)} collective-permute-done((bf16[256,1024]{1,0:T(8,128)(2,1)}, bf16[256,1024]{1,0:T(8,128)(2,1)}, u32[]{:S(2)}, u32[]{:S(2)}) %collective-permute-start) | collective-permute-done | bytes 524320 | tf_op jit(solution)/shard_map/ppermute | solution.py:142
  41.4 10.7 %collective-permute-done.2.refs_9_.refs_11_ = bf16[256,1024]{1,0:T(8,128)(2,1)} collective-permute-done((bf16[256,1024]{1,0:T(8,128)(2,1)}, bf16[256,1024]{1,0:T(8,128)(2,1)}, u32[]{:S(2)}, u32[]{:S(2)}) %collective-permute-start.2) | collective-permute-done | bytes 524320 | tf_op jit(solution)/shard_map/ppermute | solution.py:142
  52.1 7.5 %retention_first.1 = (bf16[256,512]{1,0:T(8,128)(2,1)}, bf16[256,512]{1,0:T(8,128)(2,1)}, bf16[256,512]{1,0:T(8,128)(2,1)}, bf16[256,512]{1,0:T(8,128)(2,1)}, bf...) custom-call(s32[1]{0:T(128)} %bitcast.refs_0_.place, ...), custom_call_target="tpu_custom_call" | custom-call | flops 6000000000 | bytes 10000000 | tf_op jit(solution)/shard_map/retention_first/pallas_call | solution.py:298
  59.6 2.1 %collective-permute-start.9 = (bf16[256,2048]{1,0:T(8,128)(2,1)}, bf16[256,2048]{1,0:T(8,128)(2,1)}, u32[]{:S(2)}, u32[]{:S(2)}) collective-permute-start(bf16[256,2048]{1,0:T(8,128)(2,1)} %collective-permute-done.7.refs_7_.refs_8_), channel_id=1, source_target_pairs={{0,2},{1,3},{2,4},{3,5},{4,6},{5,7},{6,0},{7,1},{8,10},{9,11},{10,... | collective-permute-start | bytes 3145736 | tf_op jit(solution)/shard_map/ppermute | solution.py:147
  61.7 3.3 %weight_start.1.refs_2_ = f32[512,2048]{1,0:T(8,128)S(1)} custom-call(bf16[512,256]{1,0:T(8,128)(2,1)S(1)} %get-tuple-element.41.refs_0_, bf16[512,256]{1,0:T(8,128)(2,1)S(1)} %get-tuple-element.42.refs_1_, bf16[512,256]{1,0:T(8,128)(2,1)S(1)} %get-tuple-element.43.refs_2_, bf16[256,2048]{1,0:T(8,128)(2,1)S(1)} %bitcast.28, ...), custom_call_target="tpu_custom_call" | custom-call | flops 4000000000 | bytes 6000000 | tf_op jit(solution)/shard_map/weight_start/pallas_call | solution.py:542
  65.5 19.2 %collective-permute-done.9.refs_9_.refs_10_ = bf16[256,2048]{1,0:T(8,128)(2,1)} collective-permute-done((bf16[256,2048]{1,0:T(8,128)(2,1)}, bf16[256,2048]{1,0:T(8,128)(2,1)}, u32[]{:S(2)}, u32[]{:S(2)}) %collective-permute-start.9) | collective-permute-done | bytes 1048608 | tf_op jit(solution)/shard_map/ppermute | solution.py:147
  87.5 1.5 collective-permute-start.19
  91.8 2.2 %collective-permute-start.25 = (bf16[256,256]{1,0:T(8,128)(2,1)S(1)}, bf16[256,256]{1,0:T(8,128)(2,1)S(1)}, u32[]{:S(2)}, u32[]{:S(2)}) collective-permute-start(bf16[256,256]{1,0:T(8,128)(2,1)S(1)} %get-tuple-element.54), channel_id=1, source_target_pairs={{0,16},{8,24},{16,0},{24,8},{1,17},{9,25},{17,1},{25,9},{2,18},{10... | collective-permute-start | bytes 393224 | tf_op jit(solution)/shard_map/ppermute | solution.py:142
  93.9 3.1 %collective-permute-start.26 = (bf16[256,256]{1,0:T(8,128)(2,1)S(1)}, bf16[256,256]{1,0:T(8,128)(2,1)S(1)}, u32[]{:S(2)}, u32[]{:S(2)}) collective-permute-start(bf16[256,256]{1,0:T(8,128)(2,1)S(1)} %get-tuple-element.55), channel_id=1, source_target_pairs={{0,24},{8,16},{16,8},{24,0},{1,25},{9,17},{17,9},{25,1},{2,26},{10... | collective-permute-start | bytes 393224 | tf_op jit(solution)/shard_map/ppermute | solution.py:142
  98.7 1.8 collective-permute-start.21
  100.5 2.4 %collective-permute-start.22 = (bf16[256,256]{1,0:T(8,128)(2,1)S(1)}, bf16[256,256]{1,0:T(8,128)(2,1)S(1)}, u32[]{:S(2)}, u32[]{:S(2)}) collective-permute-start(bf16[256,256]{1,0:T(8,128)(2,1)S(1)} %get-tuple-element.50), channel_id=1, source_target_pairs={{0,4},{1,5},{2,6},{3,7},{4,0},{5,1},{6,2},{7,3},{8,12},{9,13},{10,... | collective-permute-start | bytes 393224 | tf_op jit(solution)/shard_map/ppermute | solution.py:142
  104.9 10.8 %collective-permute-done.21.refs_1_ = bf16[256,256]{1,0:T(8,128)(2,1)S(1)} collective-permute-done((bf16[256,256]{1,0:T(8,128)(2,1)S(1)}, bf16[256,256]{1,0:T(8,128)(2,1)S(1)}, u32[]{:S(2)}, u32[]{:S(2)}) %collective-permute-start.21) | collective-permute-done | bytes 131104 | tf_op jit(solution)/shard_map/ppermute | solution.py:142
  119.8 8.7 %collective-permute-done.28.refs_6_ = bf16[256,256]{1,0:T(8,128)(2,1)S(1)} collective-permute-done((bf16[256,256]{1,0:T(8,128)(2,1)S(1)}, bf16[256,256]{1,0:T(8,128)(2,1)S(1)}, u32[]{:S(2)}, u32[]{:S(2)}) %collective-permute-start.28) | collective-permute-done | bytes 131104 | tf_op jit(solution)/shard_map/ppermute | solution.py:142
  129.2 1.5 collective-permute-start.30
  130.7 6.8 %collective-permute-done.30.refs_1_ = bf16[256,512]{1,0:T(8,128)(2,1)S(1)} collective-permute-done((bf16[256,512]{1,0:T(8,128)(2,1)S(1)}, bf16[256,512]{1,0:T(8,128)(2,1)S(1)}, u32[]{:S(2)}, u32[]{:S(2)}) %collective-permute-start.30) | collective-permute-done | bytes 262176 | tf_op jit(solution)/shard_map/ppermute | solution.py:142
  139.2 6.4 %collective-permute-done.31.refs_2_ = bf16[256,512]{1,0:T(8,128)(2,1)S(1)} collective-permute-done((bf16[256,512]{1,0:T(8,128)(2,1)S(1)}, bf16[256,512]{1,0:T(8,128)(2,1)S(1)}, u32[]{:S(2)}, u32[]{:S(2)}) %collective-permute-start.31) | collective-permute-done | bytes 262176 | tf_op jit(solution)/shard_map/ppermute | solution.py:142
  146.3 1.9 %collective-permute-start.32 = (bf16[256,512]{1,0:T(8,128)(2,1)S(1)}, bf16[256,512]{1,0:T(8,128)(2,1)}, u32[]{:S(2)}, u32[]{:S(2)}) collective-permute-start(bf16[256,512]{1,0:T(8,128)(2,1)S(1)} %add_up.1.refs_0_), channel_id=1, source_target_pairs={{0,24},{8,16},{16,8},{24,0},{1,25},{9,17},{17,9},{25,1},{2,26},{10... | collective-permute-start | bytes 786440 | tf_op jit(solution)/shard_map/ppermute | solution.py:142
  149.1 4.8 %collective-permute-done.32.refs_3_ = bf16[256,512]{1,0:T(8,128)(2,1)} collective-permute-done((bf16[256,512]{1,0:T(8,128)(2,1)S(1)}, bf16[256,512]{1,0:T(8,128)(2,1)}, u32[]{:S(2)}, u32[]{:S(2)}) %collective-permute-start.32) | collective-permute-done | bytes 262176 | tf_op jit(solution)/shard_map/ppermute | solution.py:142
  158.1 2.3 %lay_out.1 = f32[256,2048]{1,0:T(8,128)} custom-call(s32[1]{0:T(128)} %bitcast.refs_0_.place, bf16[256,512]{1,0:T(8,128)(2,1)S(1)} %copy-done.13, bf16[256,512]{1,0:T(8,128)(2,1)S(1)} %copy-done.15, bf16[256,512]{1,0:T(8,128)(2,1)S(1)} %copy-done.17, bf16[256,512]{1,0:T(8,128)(2,1)} %collective-permute-done.32.refs_3_), custom_call_target="tpu_custom_call" | custom-call | flops 1000000000 | bytes 4000000 | tf_op jit(solution)/shard_map/lay_out/pallas_call | solution.py:670
  162.7 4.6 %key_projection.1.refs_7_ = bf16[1024,512]{1,0:T(8,128)(2,1)S(1)} custom-call(s32[2]{0:T(128)S(1)} %pad_add_fusion.1.refs_0_, bf16[256,2048]{1,0:T(8,128)(2,1)S(1)} %bitcast.29, bf16[256,2048]{1,0:T(8,128)(2,1)} %collective-permute-done.13.refs_2_.refs_4_, bf16[256,2048]{1,0:T(8,128)(2,1)} %collective-permute-done.14.refs_3_.refs_5_, ...), custom_call_target="tpu_custom_call" | custom-call | flops 4000000000 | bytes 8000000 | tf_op jit(solution)/shard_map/key_projection/pallas_call | solution.py:424
  167.4 8.5 %retention_second.1 = (bf16[1024,512]{1,0:T(8,128)(2,1)}, bf16[1024,1024]{1,0:T(8,128)(2,1)}) custom-call(s32[1]{0:T(128)} %bitcast.refs_0_.place, f32[4]{0:T(128)S(1)} %dynamic_slice.23.refs_1_, bf16[1024,512]{1,0:T(8,128)(2,1)S(1)} %copy-done.20, bf16[1024,1024]{1,0:T(8,128)(2,1)S(1)} %bitcast.24, f32[1024,128]{1,0:T(8,128)S(1)} %copy-done.1, ...), custom_call_target="tpu_custom_call" | custom-call | flops 6000000000 | bytes 14000000 | tf_op jit(solution)/shard_map/retention_second/pallas_call | solution.py:332
  175.9 2.3 %reshape.24 = bf16[1,1024,4,128]{3,2,1,0:T(4,128)(2,1)} reshape(bf16[1024,512]{1,0:T(8,128)(2,1)} %get-tuple-element.38) | data formatting | bytes 2097152 | tf_op jit(solution)/shard_map/reshape | solution.py:746
  178.2 2.7 %reshape.25 = bf16[1,1024,4,256]{3,2,1,0:T(4,128)(2,1)} reshape(bf16[1024,1024]{1,0:T(8,128)(2,1)S(1)} %copy-done.23) | data formatting | bytes 4194304 | tf_op jit(solution)/shard_map/reshape | solution.py:747
  180.9 6.0 %token_gradient.1 = bf16[256,2048]{1,0:T(8,128)(2,1)} custom-call(s32[3]{0:T(128)S(1)} %pad_add_fusion.refs_0_, bf16[256,512]{1,0:T(8,128)(2,1)S(1)} %copy-done.22, bf16[256,512]{1,0:T(8,128)(2,1)S(1)} %collective-permute-done.3.refs_2_, bf16[256,512]{1,0:T(8,128)(2,1)} %collective-permute-done.4.refs_3_, bf16[256,512]{1,0:T(8,128)(2,1)} %collective-permute-done.5.refs_4_, ...), custom_call_target="tpu_custom_call" | custom-call | flops 5000000000 | bytes 11000000 | tf_op jit(solution)/shard_map/token_gradient/pallas_call | solution.py:487
  (112 shorter events, 29.6 us)
Async XLA Ops:
  0.6 27.4 %collective-permute-start.14 = (bf16[256,2048]{1,0:T(8,128)(2,1)}, bf16[256,2048]{1,0:T(8,128)(2,1)}, u32[]{:S(2)}, u32[]{:S(2)}) collective-permute-start(bf16[256,2048]{1,0:T(8,128)(2,1)} %bitcast.26), channel_id=1, source_target_pairs={{0,16},{8,24},{16,0},{24,8},{1,17},{9,25},{17,1},{25,9},{2,18},{10... | collective-permute-start | bytes 3145736 | tf_op jit(solution)/shard_map/ppermute | solution.py:142
  3.7 30.2 %collective-permute-start.13 = (bf16[256,2048]{1,0:T(8,128)(2,1)}, bf16[256,2048]{1,0:T(8,128)(2,1)}, u32[]{:S(2)}, u32[]{:S(2)}) collective-permute-start(bf16[256,2048]{1,0:T(8,128)(2,1)} %bitcast.27), channel_id=1, source_target_pairs={{0,8},{8,0},{16,24},{24,16},{1,9},{9,1},{17,25},{25,17},{2,10},{10... | collective-permute-start | bytes 3145736 | tf_op jit(solution)/shard_map/ppermute | solution.py:142
  8.1 33.1 %collective-permute-start = (bf16[256,1024]{1,0:T(8,128)(2,1)}, bf16[256,1024]{1,0:T(8,128)(2,1)}, u32[]{:S(2)}, u32[]{:S(2)}) collective-permute-start(bf16[256,1024]{1,0:T(8,128)(2,1)} %get-tuple-element.61), channel_id=1, source_target_pairs={{0,8},{8,0},{16,24},{24,16},{1,9},{9,1},{17,25},{25,17},{2,10},{10... | collective-permute-start | bytes 1572872 | tf_op jit(solution)/shard_map/ppermute | solution.py:142
  8.7 32.7 %collective-permute-start.1 = (bf16[256,1024]{1,0:T(8,128)(2,1)}, bf16[256,1024]{1,0:T(8,128)(2,1)}, u32[]{:S(2)}, u32[]{:S(2)}) collective-permute-start(bf16[256,1024]{1,0:T(8,128)(2,1)} %get-tuple-element.63), channel_id=1, source_target_pairs={{0,16},{8,24},{16,0},{24,8},{1,17},{9,25},{17,1},{25,9},{2,18},{10... | collective-permute-start | bytes 1572872 | tf_op jit(solution)/shard_map/ppermute | solution.py:142
  8.8 43.3 %collective-permute-start.2 = (bf16[256,1024]{1,0:T(8,128)(2,1)}, bf16[256,1024]{1,0:T(8,128)(2,1)}, u32[]{:S(2)}, u32[]{:S(2)}) collective-permute-start(bf16[256,1024]{1,0:T(8,128)(2,1)} %get-tuple-element.60), channel_id=1, source_target_pairs={{0,24},{8,16},{16,8},{24,0},{1,25},{9,17},{17,9},{25,1},{2,26},{10... | collective-permute-start | bytes 1572872 | tf_op jit(solution)/shard_map/ppermute | solution.py:142
  28.0 31.6 %collective-permute-start.7 = (bf16[256,2048]{1,0:T(8,128)(2,1)}, bf16[256,2048]{1,0:T(8,128)(2,1)}, u32[]{:S(2)}, u32[]{:S(2)}) collective-permute-start(bf16[256,2048]{1,0:T(8,128)(2,1)} %refs_6_.1), channel_id=1, source_target_pairs={{0,2},{1,3},{2,4},{3,5},{4,6},{5,7},{6,0},{7,1},{8,10},{9,11},{10,... | collective-permute-start | bytes 3145736 | tf_op jit(solution)/shard_map/ppermute | solution.py:147
  33.9 31.0 %collective-permute-start.15 = (bf16[256,1024]{1,0:T(8,128)(2,1)S(1)}, bf16[256,1024]{1,0:T(8,128)(2,1)S(1)}, u32[]{:S(2)}, u32[]{:S(2)}) collective-permute-start(bf16[256,1024]{1,0:T(8,128)(2,1)S(1)} %slice.8), channel_id=1, source_target_pairs={{0,8},{8,0},{16,24},{24,16},{1,9},{9,1},{17,25},{25,17},{2,10},{10... | collective-permute-start | bytes 1572872 | tf_op jit(solution)/shard_map/ppermute | solution.py:142
  41.3 23.7 %collective-permute-start.16 = (bf16[256,1024]{1,0:T(8,128)(2,1)S(1)}, bf16[256,1024]{1,0:T(8,128)(2,1)S(1)}, u32[]{:S(2)}, u32[]{:S(2)}) collective-permute-start(bf16[256,1024]{1,0:T(8,128)(2,1)S(1)} %slice.9), channel_id=1, source_target_pairs={{0,16},{8,24},{16,0},{24,8},{1,17},{9,25},{17,1},{25,9},{2,18},{10... | collective-permute-start | bytes 1572872 | tf_op jit(solution)/shard_map/ppermute | solution.py:142
  59.6 25.1 %collective-permute-start.9 = (bf16[256,2048]{1,0:T(8,128)(2,1)}, bf16[256,2048]{1,0:T(8,128)(2,1)}, u32[]{:S(2)}, u32[]{:S(2)}) collective-permute-start(bf16[256,2048]{1,0:T(8,128)(2,1)} %collective-permute-done.7.refs_7_.refs_8_), channel_id=1, source_target_pairs={{0,2},{1,3},{2,4},{3,5},{4,6},{5,7},{6,0},{7,1},{8,10},{9,11},{10,... | collective-permute-start | bytes 3145736 | tf_op jit(solution)/shard_map/ppermute | solution.py:147
  65.4 19.7 %collective-permute-start.17 = (bf16[256,2048]{1,0:T(8,128)(2,1)S(1)}, bf16[256,2048]{1,0:T(8,128)(2,1)S(1)}, u32[]{:S(2)}, u32[]{:S(2)}) collective-permute-start(bf16[256,2048]{1,0:T(8,128)(2,1)S(1)} %weight_end.3), channel_id=1, source_target_pairs={{0,1},{1,0},{2,3},{3,2},{4,5},{5,4},{6,7},{7,6},{8,9},{9,8},{10,11... | collective-permute-start | bytes 3145736 | tf_op jit(solution)/shard_map/ppermute | solution.py:142
  84.7 43.9 %collective-permute-start.11 = (bf16[256,2048]{1,0:T(8,128)(2,1)}, bf16[256,2048]{1,0:T(8,128)(2,1)}, u32[]{:S(2)}, u32[]{:S(2)}) collective-permute-start(bf16[256,2048]{1,0:T(8,128)(2,1)} %collective-permute-done.9.refs_9_.refs_10_), channel_id=1, source_target_pairs={{0,2},{1,3},{2,4},{3,5},{4,6},{5,7},{6,0},{7,1},{8,10},{9,11},{10,... | collective-permute-start | bytes 3145736 | tf_op jit(solution)/shard_map/ppermute | solution.py:147
  87.5 6.4 %collective-permute-start.19 = (bf16[256,256]{1,0:T(8,128)(2,1)S(1)}, bf16[256,256]{1,0:T(8,128)(2,1)S(1)}, u32[]{:S(2)}, u32[]{:S(2)}) collective-permute-start(bf16[256,256]{1,0:T(8,128)(2,1)S(1)} %get-tuple-element.46), channel_id=1, source_target_pairs={{0,16},{8,24},{16,0},{24,8},{1,17},{9,25},{17,1},{25,9},{2,18},{10... | collective-permute-start | bytes 393224 | tf_op jit(solution)/shard_map/ppermute | solution.py:142
  89.1 8.0 %collective-permute-start.20 = (bf16[256,256]{1,0:T(8,128)(2,1)S(1)}, bf16[256,256]{1,0:T(8,128)(2,1)S(1)}, u32[]{:S(2)}, u32[]{:S(2)}) collective-permute-start(bf16[256,256]{1,0:T(8,128)(2,1)S(1)} %get-tuple-element.47), channel_id=1, source_target_pairs={{0,24},{8,16},{16,8},{24,0},{1,25},{9,17},{17,9},{25,1},{2,26},{10... | collective-permute-start | bytes 393224 | tf_op jit(solution)/shard_map/ppermute | solution.py:142
  89.7 10.8 %collective-permute-start.24 = (bf16[256,256]{1,0:T(8,128)(2,1)S(1)}, bf16[256,256]{1,0:T(8,128)(2,1)S(1)}, u32[]{:S(2)}, u32[]{:S(2)}) collective-permute-start(bf16[256,256]{1,0:T(8,128)(2,1)S(1)} %get-tuple-element.53), channel_id=1, source_target_pairs={{0,8},{8,0},{16,24},{24,16},{1,9},{9,1},{17,25},{25,17},{2,10},{10... | collective-permute-start | bytes 393224 | tf_op jit(solution)/shard_map/ppermute | solution.py:142
  91.8 11.1 %collective-permute-start.25 = (bf16[256,256]{1,0:T(8,128)(2,1)S(1)}, bf16[256,256]{1,0:T(8,128)(2,1)S(1)}, u32[]{:S(2)}, u32[]{:S(2)}) collective-permute-start(bf16[256,256]{1,0:T(8,128)(2,1)S(1)} %get-tuple-element.54), channel_id=1, source_target_pairs={{0,16},{8,24},{16,0},{24,8},{1,17},{9,25},{17,1},{25,9},{2,18},{10... | collective-permute-start | bytes 393224 | tf_op jit(solution)/shard_map/ppermute | solution.py:142
  93.9 9.2 %collective-permute-start.26 = (bf16[256,256]{1,0:T(8,128)(2,1)S(1)}, bf16[256,256]{1,0:T(8,128)(2,1)S(1)}, u32[]{:S(2)}, u32[]{:S(2)}) collective-permute-start(bf16[256,256]{1,0:T(8,128)(2,1)S(1)} %get-tuple-element.55), channel_id=1, source_target_pairs={{0,24},{8,16},{16,8},{24,0},{1,25},{9,17},{17,9},{25,1},{2,26},{10... | collective-permute-start | bytes 393224 | tf_op jit(solution)/shard_map/ppermute | solution.py:142
  98.7 17.0 %collective-permute-start.21 = (bf16[256,256]{1,0:T(8,128)(2,1)S(1)}, bf16[256,256]{1,0:T(8,128)(2,1)S(1)}, u32[]{:S(2)}, u32[]{:S(2)}) collective-permute-start(bf16[256,256]{1,0:T(8,128)(2,1)S(1)} %get-tuple-element.49), channel_id=1, source_target_pairs={{0,2},{1,3},{2,0},{3,1},{4,6},{5,7},{6,4},{7,5},{8,10},{9,11},{10,... | collective-permute-start | bytes 393224 | tf_op jit(solution)/shard_map/ppermute | solution.py:142
  100.5 15.7 %collective-permute-start.22 = (bf16[256,256]{1,0:T(8,128)(2,1)S(1)}, bf16[256,256]{1,0:T(8,128)(2,1)S(1)}, u32[]{:S(2)}, u32[]{:S(2)}) collective-permute-start(bf16[256,256]{1,0:T(8,128)(2,1)S(1)} %get-tuple-element.50), channel_id=1, source_target_pairs={{0,4},{1,5},{2,6},{3,7},{4,0},{5,1},{6,2},{7,3},{8,12},{9,13},{10,... | collective-permute-start | bytes 393224 | tf_op jit(solution)/shard_map/ppermute | solution.py:142
  102.9 16.2 %collective-permute-start.23 = (bf16[256,256]{1,0:T(8,128)(2,1)S(1)}, bf16[256,256]{1,0:T(8,128)(2,1)S(1)}, u32[]{:S(2)}, u32[]{:S(2)}) collective-permute-start(bf16[256,256]{1,0:T(8,128)(2,1)S(1)} %get-tuple-element.51), channel_id=1, source_target_pairs={{0,6},{1,7},{2,4},{3,5},{4,2},{5,3},{6,0},{7,1},{8,14},{9,15},{10,... | collective-permute-start | bytes 393224 | tf_op jit(solution)/shard_map/ppermute | solution.py:142
  104.0 15.8 %collective-permute-start.27 = (bf16[256,256]{1,0:T(8,128)(2,1)S(1)}, bf16[256,256]{1,0:T(8,128)(2,1)S(1)}, u32[]{:S(2)}, u32[]{:S(2)}) collective-permute-start(bf16[256,256]{1,0:T(8,128)(2,1)S(1)} %get-tuple-element.57), channel_id=1, source_target_pairs={{0,2},{1,3},{2,0},{3,1},{4,6},{5,7},{6,4},{7,5},{8,10},{9,11},{10,... | collective-permute-start | bytes 393224 | tf_op jit(solution)/shard_map/ppermute | solution.py:142
  115.7 12.9 %collective-permute-start.28 = (bf16[256,256]{1,0:T(8,128)(2,1)S(1)}, bf16[256,256]{1,0:T(8,128)(2,1)S(1)}, u32[]{:S(2)}, u32[]{:S(2)}) collective-permute-start(bf16[256,256]{1,0:T(8,128)(2,1)S(1)} %get-tuple-element.58), channel_id=1, source_target_pairs={{0,4},{1,5},{2,6},{3,7},{4,0},{5,1},{6,2},{7,3},{8,12},{9,13},{10,... | collective-permute-start | bytes 393224 | tf_op jit(solution)/shard_map/ppermute | solution.py:142
  116.2 12.9 %collective-permute-start.29 = (bf16[256,256]{1,0:T(8,128)(2,1)S(1)}, bf16[256,256]{1,0:T(8,128)(2,1)S(1)}, u32[]{:S(2)}, u32[]{:S(2)}) collective-permute-start(bf16[256,256]{1,0:T(8,128)(2,1)S(1)} %get-tuple-element.59), channel_id=1, source_target_pairs={{0,6},{1,7},{2,4},{3,5},{4,2},{5,3},{6,0},{7,1},{8,14},{9,15},{10,... | collective-permute-start | bytes 393224 | tf_op jit(solution)/shard_map/ppermute | solution.py:142
  119.1 41.4 %collective-permute-start.6 = (bf16[256,2048]{1,0:T(8,128)(2,1)}, bf16[256,2048]{1,0:T(8,128)(2,1)}, u32[]{:S(2)}, u32[]{:S(2)}) collective-permute-start(bf16[256,2048]{1,0:T(8,128)(2,1)} %refs_6_.1), channel_id=1, source_target_pairs={{0,1},{1,0},{2,3},{3,2},{4,5},{5,4},{6,7},{7,6},{8,9},{9,8},{10,11... | collective-permute-start | bytes 3145736 | tf_op jit(solution)/shard_map/ppermute | solution.py:142
  119.8 41.8 %collective-permute-start.8 = (bf16[256,2048]{1,0:T(8,128)(2,1)}, bf16[256,2048]{1,0:T(8,128)(2,1)}, u32[]{:S(2)}, u32[]{:S(2)}) collective-permute-start(bf16[256,2048]{1,0:T(8,128)(2,1)} %collective-permute-done.7.refs_7_.refs_8_), channel_id=1, source_target_pairs={{0,1},{1,0},{2,3},{3,2},{4,5},{5,4},{6,7},{7,6},{8,9},{9,8},{10,11... | collective-permute-start | bytes 3145736 | tf_op jit(solution)/shard_map/ppermute | solution.py:142
  128.6 34.1 %collective-permute-start.10 = (bf16[256,2048]{1,0:T(8,128)(2,1)}, bf16[256,2048]{1,0:T(8,128)(2,1)}, u32[]{:S(2)}, u32[]{:S(2)}) collective-permute-start(bf16[256,2048]{1,0:T(8,128)(2,1)} %collective-permute-done.9.refs_9_.refs_10_), channel_id=1, source_target_pairs={{0,1},{1,0},{2,3},{3,2},{4,5},{5,4},{6,7},{7,6},{8,9},{9,8},{10,11... | collective-permute-start | bytes 3145736 | tf_op jit(solution)/shard_map/ppermute | solution.py:142
  128.6 34.1 %collective-permute-start.12 = (bf16[256,2048]{1,0:T(8,128)(2,1)}, bf16[256,2048]{1,0:T(8,128)(2,1)}, u32[]{:S(2)}, u32[]{:S(2)}) collective-permute-start(bf16[256,2048]{1,0:T(8,128)(2,1)} %collective-permute-done.11.refs_11_.refs_12_), channel_id=1, source_target_pairs={{0,1},{1,0},{2,3},{3,2},{4,5},{5,4},{6,7},{7,6},{8,9},{9,8},{10,11... | collective-permute-start | bytes 3145736 | tf_op jit(solution)/shard_map/ppermute | solution.py:142
  129.2 8.3 %collective-permute-start.30 = (bf16[256,512]{1,0:T(8,128)(2,1)S(1)}, bf16[256,512]{1,0:T(8,128)(2,1)S(1)}, u32[]{:S(2)}, u32[]{:S(2)}) collective-permute-start(bf16[256,512]{1,0:T(8,128)(2,1)S(1)} %add_up.1.refs_0_), channel_id=1, source_target_pairs={{0,8},{8,0},{16,24},{24,16},{1,9},{9,1},{17,25},{25,17},{2,10},{10... | collective-permute-start | bytes 786440 | tf_op jit(solution)/shard_map/ppermute | solution.py:142
  138.2 7.4 %collective-permute-start.31 = (bf16[256,512]{1,0:T(8,128)(2,1)S(1)}, bf16[256,512]{1,0:T(8,128)(2,1)S(1)}, u32[]{:S(2)}, u32[]{:S(2)}) collective-permute-start(bf16[256,512]{1,0:T(8,128)(2,1)S(1)} %add_up.1.refs_0_), channel_id=1, source_target_pairs={{0,16},{8,24},{16,0},{24,8},{1,17},{9,25},{17,1},{25,9},{2,18},{10... | collective-permute-start | bytes 786440 | tf_op jit(solution)/shard_map/ppermute | solution.py:142
  146.3 7.5 %collective-permute-start.32 = (bf16[256,512]{1,0:T(8,128)(2,1)S(1)}, bf16[256,512]{1,0:T(8,128)(2,1)}, u32[]{:S(2)}, u32[]{:S(2)}) collective-permute-start(bf16[256,512]{1,0:T(8,128)(2,1)S(1)} %add_up.1.refs_0_), channel_id=1, source_target_pairs={{0,24},{8,16},{16,8},{24,0},{1,25},{9,17},{17,9},{25,1},{2,26},{10... | collective-permute-start | bytes 786440 | tf_op jit(solution)/shard_map/ppermute | solution.py:142
  153.8 27.1 %collective-permute-start.3 = (bf16[256,512]{1,0:T(8,128)(2,1)}, bf16[256,512]{1,0:T(8,128)(2,1)S(1)}, u32[]{:S(2)}, u32[]{:S(2)}) collective-permute-start(bf16[256,512]{1,0:T(8,128)(2,1)} %get-tuple-element.33), channel_id=1, source_target_pairs={{0,8},{8,0},{16,24},{24,16},{1,9},{9,1},{17,25},{25,17},{2,10},{10... | collective-permute-start | bytes 786440 | tf_op jit(solution)/shard_map/ppermute | solution.py:142
  160.5 20.4 %collective-permute-start.4 = (bf16[256,512]{1,0:T(8,128)(2,1)}, bf16[256,512]{1,0:T(8,128)(2,1)}, u32[]{:S(2)}, u32[]{:S(2)}) collective-permute-start(bf16[256,512]{1,0:T(8,128)(2,1)} %get-tuple-element.34), channel_id=1, source_target_pairs={{0,16},{8,24},{16,0},{24,8},{1,17},{9,25},{17,1},{25,9},{2,18},{10... | collective-permute-start | bytes 786440 | tf_op jit(solution)/shard_map/ppermute | solution.py:142
  161.6 19.3 %collective-permute-start.5 = (bf16[256,512]{1,0:T(8,128)(2,1)}, bf16[256,512]{1,0:T(8,128)(2,1)}, u32[]{:S(2)}, u32[]{:S(2)}) collective-permute-start(bf16[256,512]{1,0:T(8,128)(2,1)} %get-tuple-element.35), channel_id=1, source_target_pairs={{0,24},{8,16},{16,8},{24,0},{1,25},{9,17},{17,9},{25,1},{2,26},{10... | collective-permute-start | bytes 786440 | tf_op jit(solution)/shard_map/ppermute | solution.py:142
  (27 other events, 275.6 us)

commit v3 on v2

--- a/solution.py
+++ b/solution.py
@@ -442,17 +442,25 @@
     )
 
 
-def token_gradient(here, plane, core, grads, shards):
+def token_gradient(here, plane, core, grads, shards, flats, heads):
     slots = len(grads)
     planes = len(shards)
     rows = grads[0].shape[0]
     share, width = shards[0][0].shape
+    seq_len = flats[0].shape[0]
+    block = seq_len // planes
+    widths = [flat.shape[1] // heads for flat in flats]
+    count = len(flats)
 
     def kernel(*refs):
         place = refs[0]
         grad_refs = refs[1 : 1 + slots]
         shard_refs = refs[1 + slots : 1 + slots + 2 * planes]
-        out, grad, weight, total, sems = refs[1 + slots + 2 * planes :]
+        rest = refs[1 + slots + 2 * planes :]
+        flat_refs, out, open_refs = rest[:count], rest[count], rest[count + 1 : 2 * count + 1]
+        grad, weight, total = rest[2 * count + 1 : 2 * count + 4]
+        flat_blocks, open_blocks = rest[2 * count + 4 : 3 * count + 4], rest[3 * count + 4 : -2]
+        sems, flat_sems = rest[-2:]
         own = place[2]
 
         def grad_copy(k):
@@ -463,42 +471,69 @@
                 shard_refs[2 * r + side], weight.at[r, own ^ side], sems.at[2 * r + side]
             )
 
+        def flat_copy(i, r):
+            part = flat_refs[i].at[r * block : (r + 1) * block]
+            return pltpu.make_async_copy(part, flat_blocks[i].at[r], flat_sems.at[0, i, r])
+
+        def open_copy(i, r):
+            part = open_refs[i].at[r * block : (r + 1) * block]
+            return pltpu.make_async_copy(open_blocks[i].at[r], part, flat_sems.at[1, i, r])
+
+        for i in range(count):
+            flat_copy(i, 0).start()
         for k in range(slots):
             grad_copy(k).start()
         for r in range(planes):
             for side in range(2):
                 shard_copy(r, side).start()
+            if r + 1 < planes:
+                for i in range(count):
+                    flat_copy(i, r + 1).start()
         for k in range(slots):
             grad_copy(k).wait()
         for r in range(planes):
+            for i in range(count):
+                flat_copy(i, r).wait()
+                opened = flat_blocks[i][r].reshape(block, heads, widths[i])
+                open_blocks[i][r] = opened
+                open_copy(i, r).start()
             k = ((place[1] + planes - r) % planes) ^ place[0]
             for side in range(2):
                 shard_copy(r, side).wait()
-            block = grad[k]
-            term = dot(block[:, :share], weight[r, 0], 1, 0)
-            term += dot(block[:, share:], weight[r, 1], 1, 0)
+            piece = grad[k]
+            term = dot(piece[:, :share], weight[r, 0], 1, 0)
+            term += dot(piece[:, share:], weight[r, 1], 1, 0)
             if r == 0:
                 total[...] = term
             elif r < planes - 1:
                 total[...] += term
             else:
                 out[...] = (total[...] + term).astype(jnp.bfloat16)
+        for r in range(planes):
+            for i in range(count):
+                open_copy(i, r).wait()
 
     return pl.pallas_call(
         kernel,
-        in_specs=[smem()] + away(slots + 2 * planes),
-        out_specs=near()[0],
-        out_shape=jax.ShapeDtypeStruct((rows, width), jnp.bfloat16),
+        in_specs=[smem()] + away(slots + 2 * planes + count),
+        out_specs=near() + away(count),
+        out_shape=[jax.ShapeDtypeStruct((rows, width), jnp.bfloat16)]
+        + [jax.ShapeDtypeStruct((seq_len, heads, size), jnp.bfloat16) for size in widths],
         scratch_shapes=[
             pltpu.VMEM((slots, rows, 2 * share), jnp.bfloat16),
             pltpu.VMEM((planes, 2, share, width), jnp.bfloat16),
             pltpu.VMEM((rows, width), jnp.float32),
+        ]
+        + [pltpu.VMEM((planes, block, heads * size), jnp.bfloat16) for size in widths]
+        + [pltpu.VMEM((planes, block, heads, size), jnp.bfloat16) for size in widths]
+        + [
             pltpu.SemaphoreType.DMA((2 * planes + slots,)),
+            pltpu.SemaphoreType.DMA((2, count, planes)),
         ],
-        compiler_params=limit(20),
-        cost_estimate=cost(5e9, 11e6),
+        compiler_params=limit(32),
+        cost_estimate=cost(5e9, 17e6),
         name="token_gradient",
-    )(prefetch(here, plane, core), *grads, *[part for pair in shards for part in pair])
+    )(prefetch(here, plane, core), *grads, *[part for pair in shards for part in pair], *flats)
 
 
 def place_parts(parts):
@@ -737,14 +772,14 @@
     grad_weight = lay_out(here, gathered)
 
     returned = [grads[0]] + [swap(grads[k], "sp", k) for k in range(1, slots)]
-    grad_tokens = token_gradient(here, plane, core, returned, shards)
-
     keys = key_projection(here, plane, core, token_slots, shards)
     grad_query, grad_value = retention_second(
         here, rate, rotated, value, cosine, sine, trailing, keys, cotans
     )
-    grad_query = grad_query.reshape(queries.shape)
-    grad_value = grad_value.reshape(values.shape)
+    grad_tokens, grad_query, grad_value = token_gradient(
+        here, plane, core, returned, shards, [grad_query, grad_value], heads
+    )
+    grad_query, grad_value = grad_query[None], grad_value[None]
     return (
         grad_tokens[None],
         grad_query,

time: 188 us -> 185 us (0.984)
  local copies, waits for them, and re-layouts: 18.8 us -> 15.4 us
    reshape x2 -> x0, local copies, waits for them, and re-layouts: 5.02 us -> none  [the longest x1 2.74 us: direct_steps(): grad_value = grad_value.reshape(values.shape)]
    unnamed x54 -> x56, local copies, waits for them, and re-layouts: 8.23 us -> 9.91 us
  transfers between devices with their start and end apart: 33 -> 33, of which waited for: 12 -> 12; matrix products, arithmetic and copies ran while one was open for 8% -> 6% of each run, Pallas kernels for 16% -> 16%
where the time goes in v3:
time: 185 us
  waiting for transfers between devices  89.3 us (48%)
  starting transfers between devices  39.8 us (22%)
  Pallas kernels  36.8 us (20%)
  local copies, waits for them, and re-layouts  15.4 us (8%)
  other arithmetic  2.54 us (1%)
    ppermute x30, waiting for transfers between devices, swap(): return lax.ppermute(array, axis, [(i, i ^ bit) for i in range(count)])  70.1 us
    ppermute x30, starting transfers between devices, swap(): return lax.ppermute(array, axis, [(i, i ^ bit) for i in range(count)])  35.7 us
    ppermute x3, waiting for transfers between devices, step_planes(): lax.ppermute(array, 'dp', [(i, (i + 2) % count) for i in range(count)])  19.2 us
    unnamed x56, local copies, waits for them, and re-layouts  9.91 us
    pallas_call x1, Pallas kernels, retention_second(): pl.pallas_call(second_kernel(slots, rows, inner, key_width ** (-0.5)), gr...  8.46 us
    pallas_call x1, Pallas kernels, retention_first(): pl.pallas_call(first_kernel(slots, rows, inner, key_width ** (-0.5)), gri...  7.52 us
    pallas_call x1, Pallas kernels, token_gradient(): pl.pallas_call(kernel, in_specs=[smem()] + away(slots + 2 * planes + coun...  6.98 us
    pallas_call x1, Pallas kernels, key_projection(): pl.pallas_call(kernel, in_specs=[smem()] + away(len(parts) - far) + near(...  4.64 us
  transfers between devices with their start and end apart: 33, of which 12 were waited for; matrix products, arithmetic and copies ran while one was open for 6% of the time, Pallas kernels for 16%

profile of v3, /device:TPU:0, one launch (start us, length us, event | category | flops | bytes accessed | tf_op | source)
XLA Modules:
  0.0 185.0 jit_solution(1952983108285126187)
XLA Ops:
  0.6 3.1 %collective-permute-start.14 = (bf16[256,2048]{1,0:T(8,128)(2,1)}, bf16[256,2048]{1,0:T(8,128)(2,1)}, u32[]{:S(2)}, u32[]{:S(2)}) collective-permute-start(bf16[256,2048]{1,0:T(8,128)(2,1)} %bitcast.28), channel_id=1, source_target_pairs={{0,16},{8,24},{16,0},{24,8},{1,17},{9,25},{17,1},{25,9},{2,18},{10... | collective-permute-start | bytes 3145736 | tf_op jit(solution)/shard_map/ppermute | solution.py:142
  3.7 1.5 collective-permute-start.13
  5.2 2.9 %dynamic-slice_bitcast_fusion = (bf16[256,1024]{1,0:T(8,128)(2,1)}, bf16[256,1024]{1,0:T(8,128)(2,1)}, bf16[256,1024]{1,0:T(8,128)(2,1)}, bf16[256,1024]{1,0:T(8,128)(2,1)}) fusion(bf16[1,256,4096]{2,1,0:T(8,128)(2,1)} %param.10, s32[]{:T(128)S(6)} %select_n.36, s32[]{:T(128)S(6)} %select_n.34, s32[]{:T(128)S(6)} %select_n.33, s32[]{:T(128)S(6)} %select_n.35), kind=kLoop, calls=%fused_computation.3 | loop fusion | bytes 4194320 | tf_op jit(solution)/shard_map/dynamic_slice | solution.py:161
  8.7 2.9 %collective-permute-start.2 = (bf16[256,1024]{1,0:T(8,128)(2,1)}, bf16[256,1024]{1,0:T(8,128)(2,1)}, u32[]{:S(2)}, u32[]{:S(2)}) collective-permute-start(bf16[256,1024]{1,0:T(8,128)(2,1)} %get-tuple-element.66), channel_id=1, source_target_pairs={{0,24},{8,16},{16,8},{24,0},{1,25},{9,17},{17,9},{25,1},{2,26},{10... | collective-permute-start | bytes 1572872 | tf_op jit(solution)/shard_map/ppermute | solution.py:142
  11.5 2.2 %copy.11 = bf16[128,8,4,256]{3,1,2,0:T(8,128)(2,1)S(1)} copy(bf16[128,8,4,256]{3,2,1,0:T(4,128)(2,1)} %bitcast.32) | data formatting | bytes 4194304
  14.5 13.6 %collective-permute-done.14.refs_3_.refs_5_ = bf16[256,2048]{1,0:T(8,128)(2,1)} collective-permute-done((bf16[256,2048]{1,0:T(8,128)(2,1)}, bf16[256,2048]{1,0:T(8,128)(2,1)}, u32[]{:S(2)}, u32[]{:S(2)}) %collective-permute-start.14) | collective-permute-done | bytes 1048608 | tf_op jit(solution)/shard_map/ppermute | solution.py:142
  28.0 2.1 %collective-permute-start.7 = (bf16[256,2048]{1,0:T(8,128)(2,1)}, bf16[256,2048]{1,0:T(8,128)(2,1)}, u32[]{:S(2)}, u32[]{:S(2)}) collective-permute-start(bf16[256,2048]{1,0:T(8,128)(2,1)} %refs_5_.1), channel_id=1, source_target_pairs={{0,2},{1,3},{2,4},{3,5},{4,6},{5,7},{6,0},{7,1},{8,10},{9,11},{10,... | collective-permute-start | bytes 3145736 | tf_op jit(solution)/shard_map/ppermute | solution.py:147
  30.1 2.0 %fusion.2 = (f32[1024,64]{1,0:T(8,128)S(1)}, f32[1024,64]{1,0:T(8,128)S(1)}, f32[1024,64]{1,0:T(8,128)S(1)}) fusion(f32[64]{0:T(128)S(1)} %multiply_power_fusion), kind=kLoop, calls=%fused_computation.10 | loop fusion | flops 131072 | bytes 786688 | tf_op jit(solution)/shard_map/neg | solution.py:742
  33.9 1.6 collective-permute-start.15
  36.6 4.7 %collective-permute-done.refs_7_.refs_9_ = bf16[256,1024]{1,0:T(8,128)(2,1)} collective-permute-done((bf16[256,1024]{1,0:T(8,128)(2,1)}, bf16[256,1024]{1,0:T(8,128)(2,1)}, u32[]{:S(2)}, u32[]{:S(2)}) %collective-permute-start) | collective-permute-done | bytes 524320 | tf_op jit(solution)/shard_map/ppermute | solution.py:142
  41.4 10.7 %collective-permute-done.2.refs_9_.refs_11_ = bf16[256,1024]{1,0:T(8,128)(2,1)} collective-permute-done((bf16[256,1024]{1,0:T(8,128)(2,1)}, bf16[256,1024]{1,0:T(8,128)(2,1)}, u32[]{:S(2)}, u32[]{:S(2)}) %collective-permute-start.2) | collective-permute-done | bytes 524320 | tf_op jit(solution)/shard_map/ppermute | solution.py:142
  52.1 7.5 %retention_first.1 = (bf16[256,512]{1,0:T(8,128)(2,1)}, bf16[256,512]{1,0:T(8,128)(2,1)}, bf16[256,512]{1,0:T(8,128)(2,1)}, bf16[256,512]{1,0:T(8,128)(2,1)}, bf...) custom-call(s32[1]{0:T(128)} %bitcast.refs_0_.place, ...), custom_call_target="tpu_custom_call" | custom-call | flops 6000000000 | bytes 10000000 | tf_op jit(solution)/shard_map/retention_first/pallas_call | solution.py:298
  59.6 2.1 %collective-permute-start.9 = (bf16[256,2048]{1,0:T(8,128)(2,1)}, bf16[256,2048]{1,0:T(8,128)(2,1)}, u32[]{:S(2)}, u32[]{:S(2)}) collective-permute-start(bf16[256,2048]{1,0:T(8,128)(2,1)} %collective-permute-done.7.refs_8_.refs_7_), channel_id=1, source_target_pairs={{0,2},{1,3},{2,4},{3,5},{4,6},{5,7},{6,0},{7,1},{8,10},{9,11},{10,... | collective-permute-start | bytes 3145736 | tf_op jit(solution)/shard_map/ppermute | solution.py:147
  61.7 3.3 %weight_start.1.refs_2_ = f32[512,2048]{1,0:T(8,128)S(1)} custom-call(bf16[512,256]{1,0:T(8,128)(2,1)S(1)} %get-tuple-element.47.refs_0_, bf16[512,256]{1,0:T(8,128)(2,1)S(1)} %get-tuple-element.48.refs_1_, bf16[512,256]{1,0:T(8,128)(2,1)S(1)} %get-tuple-element.49.refs_2_, bf16[256,2048]{1,0:T(8,128)(2,1)S(1)} %bitcast.30, ...), custom_call_target="tpu_custom_call" | custom-call | flops 4000000000 | bytes 6000000 | tf_op jit(solution)/shard_map/weight_start/pallas_call | solution.py:577
  65.5 19.2 %collective-permute-done.9.refs_10_.refs_9_ = bf16[256,2048]{1,0:T(8,128)(2,1)} collective-permute-done((bf16[256,2048]{1,0:T(8,128)(2,1)}, bf16[256,2048]{1,0:T(8,128)(2,1)}, u32[]{:S(2)}, u32[]{:S(2)}) %collective-permute-start.9) | collective-permute-done | bytes 1048608 | tf_op jit(solution)/shard_map/ppermute | solution.py:147
  87.5 1.5 collective-permute-start.25
  91.8 2.2 %collective-permute-start.19 = (bf16[256,256]{1,0:T(8,128)(2,1)S(1)}, bf16[256,256]{1,0:T(8,128)(2,1)S(1)}, u32[]{:S(2)}, u32[]{:S(2)}) collective-permute-start(bf16[256,256]{1,0:T(8,128)(2,1)S(1)} %get-tuple-element.52), channel_id=1, source_target_pairs={{0,16},{8,24},{16,0},{24,8},{1,17},{9,25},{17,1},{25,9},{2,18},{10... | collective-permute-start | bytes 393224 | tf_op jit(solution)/shard_map/ppermute | solution.py:142
  93.9 3.1 %collective-permute-start.20 = (bf16[256,256]{1,0:T(8,128)(2,1)S(1)}, bf16[256,256]{1,0:T(8,128)(2,1)S(1)}, u32[]{:S(2)}, u32[]{:S(2)}) collective-permute-start(bf16[256,256]{1,0:T(8,128)(2,1)S(1)} %get-tuple-element.53), channel_id=1, source_target_pairs={{0,24},{8,16},{16,8},{24,0},{1,25},{9,17},{17,9},{25,1},{2,26},{10... | collective-permute-start | bytes 393224 | tf_op jit(solution)/shard_map/ppermute | solution.py:142
  98.7 1.8 collective-permute-start.27
  100.5 2.4 %collective-permute-start.28 = (bf16[256,256]{1,0:T(8,128)(2,1)S(1)}, bf16[256,256]{1,0:T(8,128)(2,1)S(1)}, u32[]{:S(2)}, u32[]{:S(2)}) collective-permute-start(bf16[256,256]{1,0:T(8,128)(2,1)S(1)} %get-tuple-element.64), channel_id=1, source_target_pairs={{0,4},{1,5},{2,6},{3,7},{4,0},{5,1},{6,2},{7,3},{8,12},{9,13},{10,... | collective-permute-start | bytes 393224 | tf_op jit(solution)/shard_map/ppermute | solution.py:142
  104.9 10.8 %collective-permute-done.27.refs_5_ = bf16[256,256]{1,0:T(8,128)(2,1)S(1)} collective-permute-done((bf16[256,256]{1,0:T(8,128)(2,1)S(1)}, bf16[256,256]{1,0:T(8,128)(2,1)S(1)}, u32[]{:S(2)}, u32[]{:S(2)}) %collective-permute-start.27) | collective-permute-done | bytes 131104 | tf_op jit(solution)/shard_map/ppermute | solution.py:142
  119.8 8.7 %collective-permute-done.22.refs_2_ = bf16[256,256]{1,0:T(8,128)(2,1)S(1)} collective-permute-done((bf16[256,256]{1,0:T(8,128)(2,1)S(1)}, bf16[256,256]{1,0:T(8,128)(2,1)S(1)}, u32[]{:S(2)}, u32[]{:S(2)}) %collective-permute-start.22) | collective-permute-done | bytes 131104 | tf_op jit(solution)/shard_map/ppermute | solution.py:142
  129.2 1.5 collective-permute-start.30
  130.7 6.8 %collective-permute-done.30.refs_1_ = bf16[256,512]{1,0:T(8,128)(2,1)S(1)} collective-permute-done((bf16[256,512]{1,0:T(8,128)(2,1)S(1)}, bf16[256,512]{1,0:T(8,128)(2,1)S(1)}, u32[]{:S(2)}, u32[]{:S(2)}) %collective-permute-start.30) | collective-permute-done | bytes 262176 | tf_op jit(solution)/shard_map/ppermute | solution.py:142
  139.2 6.4 %collective-permute-done.31.refs_2_ = bf16[256,512]{1,0:T(8,128)(2,1)S(1)} collective-permute-done((bf16[256,512]{1,0:T(8,128)(2,1)S(1)}, bf16[256,512]{1,0:T(8,128)(2,1)S(1)}, u32[]{:S(2)}, u32[]{:S(2)}) %collective-permute-start.31) | collective-permute-done | bytes 262176 | tf_op jit(solution)/shard_map/ppermute | solution.py:142
  146.3 1.9 %collective-permute-start.32 = (bf16[256,512]{1,0:T(8,128)(2,1)S(1)}, bf16[256,512]{1,0:T(8,128)(2,1)}, u32[]{:S(2)}, u32[]{:S(2)}) collective-permute-start(bf16[256,512]{1,0:T(8,128)(2,1)S(1)} %add_up.1.refs_0_), channel_id=1, source_target_pairs={{0,24},{8,16},{16,8},{24,0},{1,25},{9,17},{17,9},{25,1},{2,26},{10... | collective-permute-start | bytes 786440 | tf_op jit(solution)/shard_map/ppermute | solution.py:142
  148.3 5.5 %collective-permute-done.32.refs_3_ = bf16[256,512]{1,0:T(8,128)(2,1)} collective-permute-done((bf16[256,512]{1,0:T(8,128)(2,1)S(1)}, bf16[256,512]{1,0:T(8,128)(2,1)}, u32[]{:S(2)}, u32[]{:S(2)}) %collective-permute-start.32) | collective-permute-done | bytes 262176 | tf_op jit(solution)/shard_map/ppermute | solution.py:142
  157.2 2.4 %lay_out.1 = f32[256,2048]{1,0:T(8,128)} custom-call(s32[1]{0:T(128)} %bitcast.refs_0_.place, bf16[256,512]{1,0:T(8,128)(2,1)S(1)} %add_up.1.refs_0_, bf16[256,512]{1,0:T(8,128)(2,1)S(1)} %copy-done.13, bf16[256,512]{1,0:T(8,128)(2,1)S(1)} %copy-done.15, bf16[256,512]{1,0:T(8,128)(2,1)} %collective-permute-done.32.refs_3_), custom_call_target="tpu_custom_call" | custom-call | flops 1000000000 | bytes 4000000 | tf_op jit(solution)/shard_map/lay_out/pallas_call | solution.py:705
  161.8 4.6 %key_projection.1.refs_7_ = bf16[1024,512]{1,0:T(8,128)(2,1)S(1)} custom-call(s32[2]{0:T(128)S(1)} %pad_add_fusion.1.refs_0_, bf16[256,2048]{1,0:T(8,128)(2,1)S(1)} %bitcast.31, bf16[256,2048]{1,0:T(8,128)(2,1)} %collective-permute-done.13.refs_2_.refs_4_, bf16[256,2048]{1,0:T(8,128)(2,1)} %collective-permute-done.14.refs_3_.refs_5_, ...), custom_call_target="tpu_custom_call" | custom-call | flops 4000000000 | bytes 8000000 | tf_op jit(solution)/shard_map/key_projection/pallas_call | solution.py:424
  166.5 8.5 %retention_second.1 = (bf16[1024,512]{1,0:T(8,128)(2,1)}, bf16[1024,1024]{1,0:T(8,128)(2,1)}) custom-call(s32[1]{0:T(128)} %bitcast.refs_0_.place, f32[4]{0:T(128)S(1)} %dynamic_slice.23.refs_1_, bf16[1024,512]{1,0:T(8,128)(2,1)S(1)} %copy-done.21, bf16[1024,1024]{1,0:T(8,128)(2,1)S(1)} %bitcast.26, f32[1024,128]{1,0:T(8,128)S(1)} %copy-done.1, ...), custom_call_target="tpu_custom_call" | custom-call | flops 6000000000 | bytes 14000000 | tf_op jit(solution)/shard_map/retention_second/pallas_call | solution.py:332
  175.1 1.6 copy-done.16
  177.9 7.0 %token_gradient.1 = (bf16[256,2048]{1,0:T(8,128)(2,1)}, bf16[1024,4,128]{2,1,0:T(4,128)(2,1)}, bf16[1024,4,256]{2,1,0:T(4,128)(2,1)}) custom-call(s32[3]{0:T(128)S(1)} %pad_add_fusion.refs_0_, bf16[256,512]{1,0:T(8,128)(2,1)S(1)} %copy-done.20, bf16[256,512]{1,0:T(8,128)(2,1)S(1)} %collective-permute-done.3.refs_2_, ...), custom_call_target="tpu_custom_call" | custom-call | flops 5000000000 | bytes 17000000 | tf_op jit(solution)/shard_map/token_gradient/pallas_call | solution.py:516
  (112 shorter events, 28.2 us)
Async XLA Ops:
  0.6 27.4 %collective-permute-start.14 = (bf16[256,2048]{1,0:T(8,128)(2,1)}, bf16[256,2048]{1,0:T(8,128)(2,1)}, u32[]{:S(2)}, u32[]{:S(2)}) collective-permute-start(bf16[256,2048]{1,0:T(8,128)(2,1)} %bitcast.28), channel_id=1, source_target_pairs={{0,16},{8,24},{16,0},{24,8},{1,17},{9,25},{17,1},{25,9},{2,18},{10... | collective-permute-start | bytes 3145736 | tf_op jit(solution)/shard_map/ppermute | solution.py:142
  3.7 30.2 %collective-permute-start.13 = (bf16[256,2048]{1,0:T(8,128)(2,1)}, bf16[256,2048]{1,0:T(8,128)(2,1)}, u32[]{:S(2)}, u32[]{:S(2)}) collective-permute-start(bf16[256,2048]{1,0:T(8,128)(2,1)} %bitcast.29), channel_id=1, source_target_pairs={{0,8},{8,0},{16,24},{24,16},{1,9},{9,1},{17,25},{25,17},{2,10},{10... | collective-permute-start | bytes 3145736 | tf_op jit(solution)/shard_map/ppermute | solution.py:142
  8.0 33.2 %collective-permute-start = (bf16[256,1024]{1,0:T(8,128)(2,1)}, bf16[256,1024]{1,0:T(8,128)(2,1)}, u32[]{:S(2)}, u32[]{:S(2)}) collective-permute-start(bf16[256,1024]{1,0:T(8,128)(2,1)} %get-tuple-element.67), channel_id=1, source_target_pairs={{0,8},{8,0},{16,24},{24,16},{1,9},{9,1},{17,25},{25,17},{2,10},{10... | collective-permute-start | bytes 1572872 | tf_op jit(solution)/shard_map/ppermute | solution.py:142
  8.6 32.8 %collective-permute-start.1 = (bf16[256,1024]{1,0:T(8,128)(2,1)}, bf16[256,1024]{1,0:T(8,128)(2,1)}, u32[]{:S(2)}, u32[]{:S(2)}) collective-permute-start(bf16[256,1024]{1,0:T(8,128)(2,1)} %get-tuple-element.69), channel_id=1, source_target_pairs={{0,16},{8,24},{16,0},{24,8},{1,17},{9,25},{17,1},{25,9},{2,18},{10... | collective-permute-start | bytes 1572872 | tf_op jit(solution)/shard_map/ppermute | solution.py:142
  8.7 43.4 %collective-permute-start.2 = (bf16[256,1024]{1,0:T(8,128)(2,1)}, bf16[256,1024]{1,0:T(8,128)(2,1)}, u32[]{:S(2)}, u32[]{:S(2)}) collective-permute-start(bf16[256,1024]{1,0:T(8,128)(2,1)} %get-tuple-element.66), channel_id=1, source_target_pairs={{0,24},{8,16},{16,8},{24,0},{1,25},{9,17},{17,9},{25,1},{2,26},{10... | collective-permute-start | bytes 1572872 | tf_op jit(solution)/shard_map/ppermute | solution.py:142
  28.0 31.6 %collective-permute-start.7 = (bf16[256,2048]{1,0:T(8,128)(2,1)}, bf16[256,2048]{1,0:T(8,128)(2,1)}, u32[]{:S(2)}, u32[]{:S(2)}) collective-permute-start(bf16[256,2048]{1,0:T(8,128)(2,1)} %refs_5_.1), channel_id=1, source_target_pairs={{0,2},{1,3},{2,4},{3,5},{4,6},{5,7},{6,0},{7,1},{8,10},{9,11},{10,... | collective-permute-start | bytes 3145736 | tf_op jit(solution)/shard_map/ppermute | solution.py:147
  33.9 31.0 %collective-permute-start.15 = (bf16[256,1024]{1,0:T(8,128)(2,1)S(1)}, bf16[256,1024]{1,0:T(8,128)(2,1)S(1)}, u32[]{:S(2)}, u32[]{:S(2)}) collective-permute-start(bf16[256,1024]{1,0:T(8,128)(2,1)S(1)} %slice.8), channel_id=1, source_target_pairs={{0,8},{8,0},{16,24},{24,16},{1,9},{9,1},{17,25},{25,17},{2,10},{10... | collective-permute-start | bytes 1572872 | tf_op jit(solution)/shard_map/ppermute | solution.py:142
  41.3 23.7 %collective-permute-start.16 = (bf16[256,1024]{1,0:T(8,128)(2,1)S(1)}, bf16[256,1024]{1,0:T(8,128)(2,1)S(1)}, u32[]{:S(2)}, u32[]{:S(2)}) collective-permute-start(bf16[256,1024]{1,0:T(8,128)(2,1)S(1)} %slice.9), channel_id=1, source_target_pairs={{0,16},{8,24},{16,0},{24,8},{1,17},{9,25},{17,1},{25,9},{2,18},{10... | collective-permute-start | bytes 1572872 | tf_op jit(solution)/shard_map/ppermute | solution.py:142
  59.6 25.1 %collective-permute-start.9 = (bf16[256,2048]{1,0:T(8,128)(2,1)}, bf16[256,2048]{1,0:T(8,128)(2,1)}, u32[]{:S(2)}, u32[]{:S(2)}) collective-permute-start(bf16[256,2048]{1,0:T(8,128)(2,1)} %collective-permute-done.7.refs_8_.refs_7_), channel_id=1, source_target_pairs={{0,2},{1,3},{2,4},{3,5},{4,6},{5,7},{6,0},{7,1},{8,10},{9,11},{10,... | collective-permute-start | bytes 3145736 | tf_op jit(solution)/shard_map/ppermute | solution.py:147
  65.4 19.7 %collective-permute-start.17 = (bf16[256,2048]{1,0:T(8,128)(2,1)S(1)}, bf16[256,2048]{1,0:T(8,128)(2,1)S(1)}, u32[]{:S(2)}, u32[]{:S(2)}) collective-permute-start(bf16[256,2048]{1,0:T(8,128)(2,1)S(1)} %weight_end.3), channel_id=1, source_target_pairs={{0,1},{1,0},{2,3},{3,2},{4,5},{5,4},{6,7},{7,6},{8,9},{9,8},{10,11... | collective-permute-start | bytes 3145736 | tf_op jit(solution)/shard_map/ppermute | solution.py:142
  84.7 43.9 %collective-permute-start.11 = (bf16[256,2048]{1,0:T(8,128)(2,1)}, bf16[256,2048]{1,0:T(8,128)(2,1)}, u32[]{:S(2)}, u32[]{:S(2)}) collective-permute-start(bf16[256,2048]{1,0:T(8,128)(2,1)} %collective-permute-done.9.refs_10_.refs_9_), channel_id=1, source_target_pairs={{0,2},{1,3},{2,4},{3,5},{4,6},{5,7},{6,0},{7,1},{8,10},{9,11},{10,... | collective-permute-start | bytes 3145736 | tf_op jit(solution)/shard_map/ppermute | solution.py:147
  87.5 6.4 %collective-permute-start.25 = (bf16[256,256]{1,0:T(8,128)(2,1)S(1)}, bf16[256,256]{1,0:T(8,128)(2,1)S(1)}, u32[]{:S(2)}, u32[]{:S(2)}) collective-permute-start(bf16[256,256]{1,0:T(8,128)(2,1)S(1)} %get-tuple-element.60), channel_id=1, source_target_pairs={{0,16},{8,24},{16,0},{24,8},{1,17},{9,25},{17,1},{25,9},{2,18},{10... | collective-permute-start | bytes 393224 | tf_op jit(solution)/shard_map/ppermute | solution.py:142
  89.1 8.0 %collective-permute-start.26 = (bf16[256,256]{1,0:T(8,128)(2,1)S(1)}, bf16[256,256]{1,0:T(8,128)(2,1)S(1)}, u32[]{:S(2)}, u32[]{:S(2)}) collective-permute-start(bf16[256,256]{1,0:T(8,128)(2,1)S(1)} %get-tuple-element.61), channel_id=1, source_target_pairs={{0,24},{8,16},{16,8},{24,0},{1,25},{9,17},{17,9},{25,1},{2,26},{10... | collective-permute-start | bytes 393224 | tf_op jit(solution)/shard_map/ppermute | solution.py:142
  89.7 10.8 %collective-permute-start.18 = (bf16[256,256]{1,0:T(8,128)(2,1)S(1)}, bf16[256,256]{1,0:T(8,128)(2,1)S(1)}, u32[]{:S(2)}, u32[]{:S(2)}) collective-permute-start(bf16[256,256]{1,0:T(8,128)(2,1)S(1)} %get-tuple-element.51), channel_id=1, source_target_pairs={{0,8},{8,0},{16,24},{24,16},{1,9},{9,1},{17,25},{25,17},{2,10},{10... | collective-permute-start | bytes 393224 | tf_op jit(solution)/shard_map/ppermute | solution.py:142
  91.8 11.1 %collective-permute-start.19 = (bf16[256,256]{1,0:T(8,128)(2,1)S(1)}, bf16[256,256]{1,0:T(8,128)(2,1)S(1)}, u32[]{:S(2)}, u32[]{:S(2)}) collective-permute-start(bf16[256,256]{1,0:T(8,128)(2,1)S(1)} %get-tuple-element.52), channel_id=1, source_target_pairs={{0,16},{8,24},{16,0},{24,8},{1,17},{9,25},{17,1},{25,9},{2,18},{10... | collective-permute-start | bytes 393224 | tf_op jit(solution)/shard_map/ppermute | solution.py:142
  93.9 9.2 %collective-permute-start.20 = (bf16[256,256]{1,0:T(8,128)(2,1)S(1)}, bf16[256,256]{1,0:T(8,128)(2,1)S(1)}, u32[]{:S(2)}, u32[]{:S(2)}) collective-permute-start(bf16[256,256]{1,0:T(8,128)(2,1)S(1)} %get-tuple-element.53), channel_id=1, source_target_pairs={{0,24},{8,16},{16,8},{24,0},{1,25},{9,17},{17,9},{25,1},{2,26},{10... | collective-permute-start | bytes 393224 | tf_op jit(solution)/shard_map/ppermute | solution.py:142
  98.7 17.0 %collective-permute-start.27 = (bf16[256,256]{1,0:T(8,128)(2,1)S(1)}, bf16[256,256]{1,0:T(8,128)(2,1)S(1)}, u32[]{:S(2)}, u32[]{:S(2)}) collective-permute-start(bf16[256,256]{1,0:T(8,128)(2,1)S(1)} %get-tuple-element.63), channel_id=1, source_target_pairs={{0,2},{1,3},{2,0},{3,1},{4,6},{5,7},{6,4},{7,5},{8,10},{9,11},{10,... | collective-permute-start | bytes 393224 | tf_op jit(solution)/shard_map/ppermute | solution.py:142
  100.5 15.7 %collective-permute-start.28 = (bf16[256,256]{1,0:T(8,128)(2,1)S(1)}, bf16[256,256]{1,0:T(8,128)(2,1)S(1)}, u32[]{:S(2)}, u32[]{:S(2)}) collective-permute-start(bf16[256,256]{1,0:T(8,128)(2,1)S(1)} %get-tuple-element.64), channel_id=1, source_target_pairs={{0,4},{1,5},{2,6},{3,7},{4,0},{5,1},{6,2},{7,3},{8,12},{9,13},{10,... | collective-permute-start | bytes 393224 | tf_op jit(solution)/shard_map/ppermute | solution.py:142
  102.9 16.2 %collective-permute-start.29 = (bf16[256,256]{1,0:T(8,128)(2,1)S(1)}, bf16[256,256]{1,0:T(8,128)(2,1)S(1)}, u32[]{:S(2)}, u32[]{:S(2)}) collective-permute-start(bf16[256,256]{1,0:T(8,128)(2,1)S(1)} %get-tuple-element.65), channel_id=1, source_target_pairs={{0,6},{1,7},{2,4},{3,5},{4,2},{5,3},{6,0},{7,1},{8,14},{9,15},{10,... | collective-permute-start | bytes 393224 | tf_op jit(solution)/shard_map/ppermute | solution.py:142
  104.0 15.8 %collective-permute-start.21 = (bf16[256,256]{1,0:T(8,128)(2,1)S(1)}, bf16[256,256]{1,0:T(8,128)(2,1)S(1)}, u32[]{:S(2)}, u32[]{:S(2)}) collective-permute-start(bf16[256,256]{1,0:T(8,128)(2,1)S(1)} %get-tuple-element.55), channel_id=1, source_target_pairs={{0,2},{1,3},{2,0},{3,1},{4,6},{5,7},{6,4},{7,5},{8,10},{9,11},{10,... | collective-permute-start | bytes 393224 | tf_op jit(solution)/shard_map/ppermute | solution.py:142
  115.7 12.9 %collective-permute-start.22 = (bf16[256,256]{1,0:T(8,128)(2,1)S(1)}, bf16[256,256]{1,0:T(8,128)(2,1)S(1)}, u32[]{:S(2)}, u32[]{:S(2)}) collective-permute-start(bf16[256,256]{1,0:T(8,128)(2,1)S(1)} %get-tuple-element.56), channel_id=1, source_target_pairs={{0,4},{1,5},{2,6},{3,7},{4,0},{5,1},{6,2},{7,3},{8,12},{9,13},{10,... | collective-permute-start | bytes 393224 | tf_op jit(solution)/shard_map/ppermute | solution.py:142
  116.2 12.9 %collective-permute-start.23 = (bf16[256,256]{1,0:T(8,128)(2,1)S(1)}, bf16[256,256]{1,0:T(8,128)(2,1)S(1)}, u32[]{:S(2)}, u32[]{:S(2)}) collective-permute-start(bf16[256,256]{1,0:T(8,128)(2,1)S(1)} %get-tuple-element.57), channel_id=1, source_target_pairs={{0,6},{1,7},{2,4},{3,5},{4,2},{5,3},{6,0},{7,1},{8,14},{9,15},{10,... | collective-permute-start | bytes 393224 | tf_op jit(solution)/shard_map/ppermute | solution.py:142
  119.1 40.5 %collective-permute-start.6 = (bf16[256,2048]{1,0:T(8,128)(2,1)}, bf16[256,2048]{1,0:T(8,128)(2,1)}, u32[]{:S(2)}, u32[]{:S(2)}) collective-permute-start(bf16[256,2048]{1,0:T(8,128)(2,1)} %refs_5_.1), channel_id=1, source_target_pairs={{0,1},{1,0},{2,3},{3,2},{4,5},{5,4},{6,7},{7,6},{8,9},{9,8},{10,11... | collective-permute-start | bytes 3145736 | tf_op jit(solution)/shard_map/ppermute | solution.py:142
  119.8 40.9 %collective-permute-start.8 = (bf16[256,2048]{1,0:T(8,128)(2,1)}, bf16[256,2048]{1,0:T(8,128)(2,1)}, u32[]{:S(2)}, u32[]{:S(2)}) collective-permute-start(bf16[256,2048]{1,0:T(8,128)(2,1)} %collective-permute-done.7.refs_8_.refs_7_), channel_id=1, source_target_pairs={{0,1},{1,0},{2,3},{3,2},{4,5},{5,4},{6,7},{7,6},{8,9},{9,8},{10,11... | collective-permute-start | bytes 3145736 | tf_op jit(solution)/shard_map/ppermute | solution.py:142
  128.6 33.2 %collective-permute-start.10 = (bf16[256,2048]{1,0:T(8,128)(2,1)}, bf16[256,2048]{1,0:T(8,128)(2,1)}, u32[]{:S(2)}, u32[]{:S(2)}) collective-permute-start(bf16[256,2048]{1,0:T(8,128)(2,1)} %collective-permute-done.9.refs_10_.refs_9_), channel_id=1, source_target_pairs={{0,1},{1,0},{2,3},{3,2},{4,5},{5,4},{6,7},{7,6},{8,9},{9,8},{10,11... | collective-permute-start | bytes 3145736 | tf_op jit(solution)/shard_map/ppermute | solution.py:142
  128.6 33.2 %collective-permute-start.12 = (bf16[256,2048]{1,0:T(8,128)(2,1)}, bf16[256,2048]{1,0:T(8,128)(2,1)}, u32[]{:S(2)}, u32[]{:S(2)}) collective-permute-start(bf16[256,2048]{1,0:T(8,128)(2,1)} %collective-permute-done.11.refs_12_.refs_11_), channel_id=1, source_target_pairs={{0,1},{1,0},{2,3},{3,2},{4,5},{5,4},{6,7},{7,6},{8,9},{9,8},{10,11... | collective-permute-start | bytes 3145736 | tf_op jit(solution)/shard_map/ppermute | solution.py:142
  129.2 8.3 %collective-permute-start.30 = (bf16[256,512]{1,0:T(8,128)(2,1)S(1)}, bf16[256,512]{1,0:T(8,128)(2,1)S(1)}, u32[]{:S(2)}, u32[]{:S(2)}) collective-permute-start(bf16[256,512]{1,0:T(8,128)(2,1)S(1)} %add_up.1.refs_0_), channel_id=1, source_target_pairs={{0,8},{8,0},{16,24},{24,16},{1,9},{9,1},{17,25},{25,17},{2,10},{10... | collective-permute-start | bytes 786440 | tf_op jit(solution)/shard_map/ppermute | solution.py:142
  138.2 7.4 %collective-permute-start.31 = (bf16[256,512]{1,0:T(8,128)(2,1)S(1)}, bf16[256,512]{1,0:T(8,128)(2,1)S(1)}, u32[]{:S(2)}, u32[]{:S(2)}) collective-permute-start(bf16[256,512]{1,0:T(8,128)(2,1)S(1)} %add_up.1.refs_0_), channel_id=1, source_target_pairs={{0,16},{8,24},{16,0},{24,8},{1,17},{9,25},{17,1},{25,9},{2,18},{10... | collective-permute-start | bytes 786440 | tf_op jit(solution)/shard_map/ppermute | solution.py:142
  146.3 7.5 %collective-permute-start.32 = (bf16[256,512]{1,0:T(8,128)(2,1)S(1)}, bf16[256,512]{1,0:T(8,128)(2,1)}, u32[]{:S(2)}, u32[]{:S(2)}) collective-permute-start(bf16[256,512]{1,0:T(8,128)(2,1)S(1)} %add_up.1.refs_0_), channel_id=1, source_target_pairs={{0,24},{8,16},{16,8},{24,0},{1,25},{9,17},{17,9},{25,1},{2,26},{10... | collective-permute-start | bytes 786440 | tf_op jit(solution)/shard_map/ppermute | solution.py:142
  153.8 21.2 %collective-permute-start.3 = (bf16[256,512]{1,0:T(8,128)(2,1)}, bf16[256,512]{1,0:T(8,128)(2,1)S(1)}, u32[]{:S(2)}, u32[]{:S(2)}) collective-permute-start(bf16[256,512]{1,0:T(8,128)(2,1)} %get-tuple-element.36), channel_id=1, source_target_pairs={{0,8},{8,0},{16,24},{24,16},{1,9},{9,1},{17,25},{25,17},{2,10},{10... | collective-permute-start | bytes 786440 | tf_op jit(solution)/shard_map/ppermute | solution.py:142
  159.6 15.4 %collective-permute-start.4 = (bf16[256,512]{1,0:T(8,128)(2,1)S(1)}, bf16[256,512]{1,0:T(8,128)(2,1)S(1)}, u32[]{:S(2)}, u32[]{:S(2)}) collective-permute-start(bf16[256,512]{1,0:T(8,128)(2,1)S(1)} %copy-done.25), channel_id=1, source_target_pairs={{0,16},{8,24},{16,0},{24,8},{1,17},{9,25},{17,1},{25,9},{2,18},{10... | collective-permute-start | bytes 786440 | tf_op jit(solution)/shard_map/ppermute | solution.py:142
  160.7 14.3 %collective-permute-start.5 = (bf16[256,512]{1,0:T(8,128)(2,1)S(1)}, bf16[256,512]{1,0:T(8,128)(2,1)S(1)}, u32[]{:S(2)}, u32[]{:S(2)}) collective-permute-start(bf16[256,512]{1,0:T(8,128)(2,1)S(1)} %copy-done.24), channel_id=1, source_target_pairs={{0,24},{8,16},{16,8},{24,0},{1,25},{9,17},{17,9},{25,1},{2,26},{10... | collective-permute-start | bytes 786440 | tf_op jit(solution)/shard_map/ppermute | solution.py:142
  (28 other events, 278.5 us)
